TPU v7x, 32 devices: a whole 2x2x4 slice. The times are simulated.
32 devices in a mesh: grp: 2 (over x), ep: 8 (over z, y), tp: 2 (over core).
Axes of the slice: x: 2, y: 2, z: 4, core: 2. Of those that a mesh axis runs over, the one named last changes fastest.
Arguments:
- tokens: bfloat16 [2304, 2048], P(('grp', 'ep')), parts along dimension 0, may hold values from -6 to 6
- norm_gain: bfloat16 [2048], replicated, may hold values from 0.099609375 to 1.8984375
- chosen_rows: int32 [16, 144], P('grp', 'ep'), parts along dimension 0, may hold values from 0 to 1151, as said below
- route_weights: float32 [16, 144], P('grp', 'ep'), parts along dimension 0, may hold values from 0.2 to 1
- gate_weight: bfloat16 [8, 2048, 1536], P('ep', None, 'tp'), may hold values from -0.125 to 0.125
- up_weight: bfloat16 [8, 2048, 1536], P('ep', None, 'tp'), may hold values from -0.125 to 0.125
- down_weight: bfloat16 [8, 1536, 2048], P('ep', 'tp'), may hold values from -0.15625 to 0.15625
Outputs:
- mixed: bfloat16 [2304, 2048], P(('grp', 'ep', 'tp')), parts along dimension 0
There are 2 independent parts, one for each index of `grp`. A program takes and returns all parts, laid end to end along the dimension named above; an argument that names none is the same for every part. Nothing has to cross between parts.
Inputs may be any that keep to these rules, and one draw needn't show every extreme that they name: `chosen_rows`: the columns come in blocks of 18, one block for each index of ep's 144 tokens in order. In every row the first half of a block names distinct tokens of the first half of that block's tokens, and its second half distinct tokens of the second half.
All inputs are finite; a program needn't handle non-finite values.
Results may differ from a plain program's by a relative error of at most 0.01.
Values may be sent and summed in bfloat16 or wider, within the bound.
No kernel may reach another device: no remote copies, remote signals or barrier semaphores. Data moves between devices by JAX's collectives and lax.ppermute only.
A program may use at most 128 MiB of HBM per device.

v0:
```python
import jax
import jax.numpy as jnp
from jax import lax
from jax.sharding import PartitionSpec as P


def rms_apply(values_in, norm_gain):
    values = values_in.astype(jnp.float32)
    scale = lax.rsqrt(jnp.mean(values * values, axis=-1, keepdims=True) + 1e-06)
    return (values * scale * norm_gain.astype(jnp.float32)).astype(jnp.bfloat16)


def local(tokens, norm_gain, chosen_rows, route_weights, gate_weight, up_weight, down_weight):
    tok_rows = tokens.shape[0]
    width = tokens.shape[1]
    experts = chosen_rows.shape[0]
    slots = chosen_rows.shape[1]
    half_slots = slots // 2
    half_rows = tok_rows // 2
    source_id = lax.axis_index("ep")
    core_id = lax.axis_index("tp")
    local_rows = (chosen_rows - source_id * tok_rows).reshape(experts, 2, half_slots)
    source_rows = rms_apply(tokens, norm_gain)
    own_half = lax.dynamic_index_in_dim(local_rows, core_id, 1, keepdims=False)
    outgoing = source_rows[own_half]
    received = lax.all_to_all(outgoing, "ep", split_axis=0, concat_axis=0, tiled=True)
    arrived = lax.all_gather(received[None], "tp", axis=0, tiled=True)
    expert_in = arrived.reshape(-1, width)
    gate_proj = jnp.dot(expert_in, gate_weight[0], preferred_element_type=jnp.float32)
    up_proj = jnp.dot(expert_in, up_weight[0], preferred_element_type=jnp.float32)
    hidden = (jax.nn.silu(gate_proj) * up_proj).astype(jnp.bfloat16)
    summed = lax.psum_scatter(
        jnp.dot(hidden, down_weight[0], preferred_element_type=jnp.float32).astype(jnp.bfloat16),
        "tp",
        scatter_dimension=0,
        tiled=True,
    )
    expert_out = summed.reshape(experts, half_slots, width)
    results = lax.all_to_all(expert_out, "ep", split_axis=0, concat_axis=0, tiled=True)
    row_index = (
        lax.dynamic_index_in_dim(local_rows, core_id, 1, keepdims=False) - core_id * half_rows
    )
    weight_half = lax.dynamic_index_in_dim(
        route_weights.reshape(experts, 2, half_slots), core_id, 1, keepdims=False
    )
    contrib = weight_half.reshape(-1, 1) * results.reshape(-1, width).astype(jnp.float32)
    mixed = jnp.zeros((half_rows, width), jnp.float32).at[row_index.reshape(-1)].add(contrib)
    return mixed.astype(jnp.bfloat16)


def solution(mesh):
    return jax.shard_map(
        local,
        mesh=mesh,
        in_specs=(
            P(("grp", "ep"), None),
            P(),
            P("grp", "ep"),
            P("grp", "ep"),
            P("ep", None, "tp"),
            P("ep", None, "tp"),
            P("ep", "tp", None),
        ),
        out_specs=P(("grp", "ep", "tp"), None),
        check_vma=False,
    )
```

profile of v0, /device:TPU:0, one launch (start us, length us, event | category | flops | bytes accessed | tf_op | source)
XLA Modules:
  0.0 93.9 jit_solution(9900520229802952924)
XLA Ops:
  6.5 0.0 copy-start
  6.5 0.0 reduce-scatter.2.cloned.1.call-start
  6.5 1.4 %fusion.15 = f32[144]{0:T(256)S(1)} fusion(bf16[144,2048]{1,0:T(8,128)(2,1)} %param.7), kind=kLoop, calls=%fused_computation.13 | loop fusion | flops 884592 | bytes 590400 | tf_op jit(solution)/shard_map/reduce_sum | solution.py:9
  8.0 0.7 broadcast_subtract_fusion
  8.7 0.1 reshape.78
  8.8 0.1 reshape.85
  8.9 0.7 convert_element_type.25
  9.6 2.1 %fusion.17 = bf16[144,2048]{1,0:T(8,128)(2,1)} fusion(bf16[144,2048]{1,0:T(8,128)(2,1)} %param.7, f32[2048]{0:T(1024)S(1)} %convert_element_type.25, f32[144]{0:T(256)S(1)} %add_rsqrt_fusion), kind=kLoop, calls=%fused_computation.15 | loop fusion | flops 1179648 | bytes 1188416 | tf_op jit(solution)/shard_map/convert_element_type | solution.py:10
  11.6 2.2 %gather_fusion = bf16[72,2048]{1,0:T(8,128)(2,1)S(1)} fusion(bf16[144,2048]{1,0:T(8,128)(2,1)} %fusion.17, s32[1024]{0:T(1024)S(1)} %pad_clamp_fusion), kind=kCustom, calls=%fused_computation | custom fusion | bytes 590112 | tf_op jit(solution)/shard_map/gather | solution.py:25
  13.8 0.9 reshape.84
  14.7 21.8 %all_to_all.10 = bf16[8,9,2048]{2,1,0:T(8,128)(2,1)S(1)} all-to-all(bf16[8,9,2048]{2,1,0:T(8,128)(2,1)} %reshape.84), channel_id=1, replica_groups=mesh['grp'=2,'ep'=8,'tp'=2] {'ep'}, dimensions={0} | all-to-all | bytes 589824 | tf_op jit(solution)/shard_map/all_to_all | solution.py:26
  36.6 0.2 copy.11
  36.8 2.2 %all-gather = bf16[16,9,2048]{2,0,1:T(8,128)(2,1)S(1)} all-gather(bf16[8,9,2048]{2,0,1:T(8,128)(2,1)S(1)} %copy.11), channel_id=2, replica_groups=mesh['grp'=2,'ep'=8,'tp'=2] {'tp'}, dimensions={0}, use_global_device_ids=true | all-gather | bytes 884736 | tf_op jit(solution)/shard_map/all_gather | solution.py:27
  39.0 1.4 %copy.12 = bf16[16,9,2048]{2,1,0:T(8,128)(2,1)} copy(bf16[16,9,2048]{2,0,1:T(8,128)(2,1)S(1)} %all-gather) | data formatting | bytes 1179648 | tf_op jit(solution)/shard_map/all_gather | solution.py:27
  40.4 2.3 %reshape.80 = bf16[144,2048]{1,0:T(8,128)(2,1)} reshape(bf16[16,9,2048]{2,1,0:T(8,128)(2,1)} %copy.12) | data formatting | bytes 1179648 | tf_op jit(solution)/shard_map/reshape | solution.py:28
  42.7 3.5 %fusion.4 = f32[144,768]{1,0:T(8,128)} fusion(bf16[144,2048]{1,0:T(8,128)(2,1)} %reshape.80, bf16[1,2048,768]{2,1,0:T(8,128)(2,1)} %param.11), kind=kOutput, calls=%fused_computation.6 | convolution fusion | flops 452984832 | bytes 4177920 | tf_op jit(solution)/shard_map/dot_general | solution.py:29
  46.2 0.0 copy-done
  46.2 0.0 copy-start.1
  46.2 4.3 %fusion.6 = bf16[144,2048]{1,0:T(8,128)(2,1)} fusion(bf16[1,768,2048]{2,1,0:T(8,128)(2,1)S(1)} %copy-done, bf16[144,2048]{1,0:T(8,128)(2,1)} %reshape.80, bf16[1,2048,768]{2,1,0:T(8,128)(2,1)} %param.12, f32[144,768]{1,0:T(8,128)} %fusion.4), kind=kOutput, calls=%fused_computation.8 | convolution fusion | flops 906928128 | bytes 7913472 | tf_op jit(solution)/shard_map/dot_general | solution.py:33
  50.5 0.0 reduce-scatter.2.cloned.1.call-update
  50.5 7.2 %reduce-scatter.2.cloned.1.call-done = bf16[72,2048]{1,0:T(8,128)(2,1)} async-done(((bf16[144,2048]{1,0:T(8,128)(2,1)}), bf16[72,2048]{1,0:T(8,128)(2,1)}) %reduce-scatter.2.cloned.1.call-update) | async-done | bytes 294928 | tf_op jit(solution)/shard_map/reduce_scatter | solution.py:32
  57.6 1.9 %reshape.81 = bf16[8,9,2048]{2,1,0:T(8,128)(2,1)} reshape(bf16[72,2048]{1,0:T(8,128)(2,1)} %reduce-scatter.2.cloned.1.call-done) | data formatting | bytes 589824 | tf_op jit(solution)/shard_map/reshape | solution.py:38
  59.5 5.7 %all-to-all-start.1 = ((bf16[8,9,2048]{2,1,0:T(8,128)(2,1)}), bf16[8,9,2048]{2,1,0:T(8,128)(2,1)}, u32[]{:S(2)}, u32[]{:S(2)}) async-start(bf16[8,9,2048]{2,1,0:T(8,128)(2,1)} %reshape.81), calls=%async_computation.2 | async-start | bytes 1048576 | tf_op jit(solution)/shard_map/all_to_all | solution.py:39
  65.2 0.1 sub.27
  65.3 0.0 copy-done.1
  65.3 0.1 reshape.79
  65.4 0.1 mul.44
  65.5 14.8 %all-to-all-done.1 = bf16[8,9,2048]{2,1,0:T(8,128)(2,1)} async-done(((bf16[8,9,2048]{2,1,0:T(8,128)(2,1)}), bf16[8,9,2048]{2,1,0:T(8,128)(2,1)}, u32[]{:S(2)}, u32[]{:S(2)}) %all-to-all-start.1) | async-done | bytes 294944 | tf_op jit(solution)/shard_map/all_to_all | solution.py:39
  80.3 2.0 %reshape.82 = f32[72,2048]{1,0:T(8,128)} reshape(bf16[8,9,2048]{2,1,0:T(8,128)(2,1)} %all-to-all-done.1) | data formatting | bytes 884736 | tf_op jit(solution)/shard_map/convert_element_type | solution.py:46
  82.3 2.9 %scatter_custom_fusion = f32[72,2048]{1,0:T(8,128)} fusion(s32[72]{0:T(128)S(1)} %fusion.30, f32[72,2048]{1,0:T(8,128)} %reshape.82, f32[72]{0:T(128)S(1)} %mul.44, f32[]{:T(128)} %constant.11.clone.1), kind=kCustom, calls=%fused_computation.16 | custom fusion | flops 294912 | bytes 1180164 | tf_op jit(solution)/shard_map/scatter-add | solution.py:47
  85.2 1.8 %convert_element_type.31 = bf16[72,2048]{1,0:T(8,128)(2,1)} convert(f32[72,2048]{1,0:T(8,128)} %scatter_custom_fusion) | non-fusion elementwise | flops 147456 | bytes 884736 | tf_op jit(solution)/shard_map/convert_element_type | solution.py:48
  (6 shorter events, 0.1 us)
Async XLA Ops:
  6.5 39.6 %copy-start = (bf16[1,768,2048]{2,1,0:T(8,128)(2,1)S(1)}, bf16[1,768,2048]{2,1,0:T(8,128)(2,1)}, u32[]{:S(2)}) copy-start(bf16[1,768,2048]{2,1,0:T(8,128)(2,1)} %param.13) | copy-start | bytes 9437188
  6.5 51.1 %reduce-scatter.2.cloned.1.call-start = ((), (), s32[]{:S(2)}) async-start(), calls=%async_computation.3 | async-start | bytes 884736 | tf_op jit(solution)/shard_map/reduce_scatter | solution.py:32
  46.2 19.2 %copy-start.1 = (f32[8,18]{1,0:T(8,128)S(1)}, f32[8,18]{1,0:T(8,128)}, u32[]{:S(2)}) copy-start(f32[8,18]{1,0:T(8,128)} %param.10) | copy-start | bytes 1732
  59.5 20.8 %all-to-all-start.1 = ((bf16[8,9,2048]{2,1,0:T(8,128)(2,1)}), bf16[8,9,2048]{2,1,0:T(8,128)(2,1)}, u32[]{:S(2)}, u32[]{:S(2)}) async-start(bf16[8,9,2048]{2,1,0:T(8,128)(2,1)} %reshape.81), calls=%async_computation.2 | async-start | bytes 1048576 | tf_op jit(solution)/shard_map/all_to_all | solution.py:39
Sparse Core Ops, SparseCore 0:
  50.6 6.9 reduce-scatter.1
where the time goes:
time: 94.5 us; the launch traced here: 93.9 us
  blocking collectives  24.1 us (26%)
  waiting for transfers between devices  22 us (23%)
  between operations  13.4 us (14%)
  local copies, waits for them, and re-layouts  11.2 us (12%)
  other arithmetic  9.62 us (10%)
  matrix products  7.79 us (8%)
  starting transfers between devices  5.73 us (6%)
    all_to_all x1, blocking collectives, local(): lax.all_to_all(outgoing, 'ep', split_axis=0, concat_axis=0, tiled=True)  21.8 us
    all_to_all x1, waiting for transfers between devices, local(): lax.all_to_all(expert_out, 'ep', split_axis=0, concat_axis=0, tiled=True)  14.8 us
    reduce_scatter x1, waiting for transfers between devices, local(): lax.psum_scatter(jnp.dot(hidden, down_weight[0], preferred_element_type=j...  7.16 us
    all_to_all x1, starting transfers between devices, local(): lax.all_to_all(expert_out, 'ep', split_axis=0, concat_axis=0, tiled=True)  5.72 us
    dot_general x1, matrix products, local(): jnp.dot(hidden, down_weight[0], preferred_element_type=jnp.float32)  4.3 us
    dot_general x1, matrix products, local(): jnp.dot(expert_in, gate_weight[0], preferred_element_type=jnp.float32)  3.49 us
    gather x2, local copies, waits for them, and re-layouts, local(): outgoing = source_rows[own_half]  3.1 us
    scatter-add x1, other arithmetic, local(): jnp.zeros((half_rows, width), jnp.float32).at[row_index.reshape(-1)]  2.89 us
  transfers between devices with their start and end apart: 2, of which 2 were waited for; matrix products, arithmetic and copies ran while one was open for 0% of the time, Pallas kernels for 0%

commit v1 on v0

v1 whole, which is shorter than its diff:
```python
import functools

import jax
import jax.numpy as jnp
from jax import lax
from jax.experimental import pallas as pl
from jax.experimental.pallas import tpu as pltpu
from jax.sharding import PartitionSpec as P

LANES = 128
SUB = 8
F32 = jnp.float32
BF16 = jnp.bfloat16
VMEM = pl.BlockSpec(memory_space=pltpu.VMEM)


def cdiv(a, b):
    return (a + b - 1) // b


def pick(values, wanted):
    lane = lax.broadcasted_iota(jnp.int32, values.shape, 1)
    return jnp.sum(jnp.where(lane == wanted, values, 0.0), axis=1, keepdims=True)


def main_slots(n_main, half_slots, slots):
    sub = lax.broadcasted_iota(jnp.int32, (2 * n_main, slots), 0)
    return jnp.where(sub < n_main, sub, sub - n_main + half_slots)


def dispatch_kernel(tok_ref, gain_ref, rows_ref, out_ref, norm_scr, tail_scr):
    tok_rows, width = tok_ref.shape
    n_dest, slots = rows_ref.shape
    half_slots = slots // 2
    n_main = half_slots // SUB * SUB
    n_tail = half_slots - n_main
    half_width = width // 2
    blocks = half_width // LANES
    core = lax.axis_index("tp")
    base = pl.multiple_of(core * half_width, half_width)
    gain = gain_ref[:, pl.ds(base, half_width)].astype(F32)
    step = 16
    for at in range(0, tok_rows, step):
        rows = slice(at, at + step)
        values = tok_ref[rows, :].astype(F32)
        scale = lax.rsqrt(jnp.mean(values * values, axis=-1, keepdims=True) + 1e-06)
        part = tok_ref[rows, pl.ds(base, half_width)].astype(F32)
        norm_scr[rows, :] = (part * scale * gain).astype(BF16)
    normed = norm_scr[...]
    index = (rows_ref[...] - lax.axis_index("ep") * tok_rows).astype(F32)
    wanted = main_slots(n_main, half_slots, slots)
    group = 2 * n_main

    def one_hot(column):
        token = lax.broadcasted_iota(jnp.int32, (column.shape[0], tok_rows), 1)
        return jnp.where(token == column.astype(jnp.int32), 1.0, 0.0).astype(BF16)

    def chosen(column):
        return jnp.dot(one_hot(column), normed, preferred_element_type=F32)

    for first in range(0, n_dest, SUB):
        columns = [
            pick(jnp.broadcast_to(index[d : d + 1, :], (group, slots)), wanted)
            for d in range(first, first + SUB)
        ]
        got = chosen(jnp.concatenate(columns, axis=0))
        for d in range(SUB):
            for j in range(blocks):
                out_ref[first + d, j * group : (j + 1) * group, :] = got[
                    d * group : (d + 1) * group, j * LANES : (j + 1) * LANES
                ].astype(BF16)
    per_dest = 2 * n_tail * blocks
    columns = [
        pick(index, jnp.full((n_dest, slots), h * half_slots + n_main + t, jnp.int32))
        for h in range(2)
        for t in range(n_tail)
    ]
    got = chosen(jnp.concatenate(columns, axis=0))
    for k in range(2 * n_tail):
        for j in range(blocks):
            tail_scr[pl.ds(k * blocks + j, n_dest, stride=per_dest), :] = got[
                k * n_dest : (k + 1) * n_dest, j * LANES : (j + 1) * LANES
            ]
    for d in range(n_dest):
        out_ref[d, group * blocks :, :] = tail_scr[d * per_dest : (d + 1) * per_dest, :].astype(BF16)


def expert_kernel(
    mine_ref, other_ref, gate_ref, up_ref, down_ref, send_ref, keep_ref,
    x_scr, hidden_scr, tail_scr, back_scr, *, n_main, n_tail,
):
    n_src = mine_ref.shape[0]
    _, width, hidden = gate_ref.shape
    half_width = width // 2
    blocks = half_width // LANES
    group = 2 * n_main
    per_src = 2 * n_tail * blocks
    main_rows = n_src * group
    core = lax.axis_index("tp")
    for ref, base in ((mine_ref, core * half_width), (other_ref, (1 - core) * half_width)):
        for s in range(n_src):
            tail_scr[s * per_src : (s + 1) * per_src, :] = ref[s, group * blocks :, :].astype(F32)
        for j in range(blocks):
            lanes = pl.ds(pl.multiple_of(base + j * LANES, LANES), LANES)
            for s in range(n_src):
                x_scr[s * group : (s + 1) * group, lanes] = ref[s, j * group : (j + 1) * group, :]
            rest = [
                tail_scr[pl.ds(k * blocks + j, n_src, stride=per_src), :] for k in range(2 * n_tail)
            ]
            x_scr[main_rows:, lanes] = jnp.concatenate(rest, axis=0).astype(BF16)
    chunk = 2 * LANES
    x = x_scr[...]
    for at in range(0, hidden, chunk):
        cols = slice(at, at + chunk)
        gate = jnp.dot(x, gate_ref[0, :, cols], preferred_element_type=F32)
        up = jnp.dot(x, up_ref[0, :, cols], preferred_element_type=F32)
        hidden_scr[:, cols] = (gate / (1.0 + jnp.exp(-gate)) * up).astype(BF16)
    act = hidden_scr[...]
    first = core == 0
    all_blocks = width // LANES
    per_back = n_tail * all_blocks
    for at in range(0, width, chunk):
        part = jnp.dot(act, down_ref[0, :, at : at + chunk], preferred_element_type=F32)
        j = at // LANES
        for s in range(n_src):
            halves = []
            for h in range(2):
                row = s * group + h * n_main
                halves.append(
                    jnp.concatenate(
                        [part[row : row + n_main, :LANES], part[row : row + n_main, LANES:]], axis=0
                    )
                )
            place = slice(j * n_main, (j + 2) * n_main)
            send_ref[s, place, :] = jnp.where(first, halves[1], halves[0]).astype(BF16)
            keep_ref[s, place, :] = jnp.where(first, halves[0], halves[1]).astype(BF16)
        for b in range(2):
            lanes = slice(b * LANES, (b + 1) * LANES)
            for t in range(n_tail):
                rows = [main_rows + (h * n_tail + t) * n_src for h in range(2)]
                low, high = (part[row : row + n_src, lanes] for row in rows)
                where = pl.ds(t * all_blocks + j + b, n_src, stride=per_back)
                back_scr[0, where, :] = jnp.where(first, high, low)
                back_scr[1, where, :] = jnp.where(first, low, high)
    for s in range(n_src):
        rows = slice(s * per_back, (s + 1) * per_back)
        send_ref[s, n_main * all_blocks :, :] = back_scr[0, rows, :].astype(BF16)
        keep_ref[s, n_main * all_blocks :, :] = back_scr[1, rows, :].astype(BF16)


def combine_kernel(back_ref, rows_ref, weight_ref, out_ref, row_scr, tail_scr):
    n_exp, slots = rows_ref.shape
    half_slots = slots // 2
    n_main = half_slots // SUB * SUB
    n_tail = half_slots - n_main
    out_rows, width = out_ref.shape
    all_blocks = width // LANES
    per_back = n_tail * all_blocks
    main_rows = n_exp * n_main
    core = lax.axis_index("tp")
    start = lax.axis_index("ep") * (2 * out_rows) + core * out_rows
    index = (rows_ref[...] - start).astype(F32)
    weight = weight_ref[...]
    lane0 = core * half_slots
    wanted = lax.broadcasted_iota(jnp.int32, (n_main, slots), 0) + lane0
    pieces = []

    def entry(idx, wgt):
        token = lax.broadcasted_iota(jnp.int32, (idx.shape[0], cdiv(out_rows, LANES) * LANES), 1)
        return jnp.where(token == idx.astype(jnp.int32), wgt, 0.0)

    for e in range(n_exp):
        columns = [
            pick(jnp.broadcast_to(v[e : e + 1, :], (n_main, slots)), wanted) for v in (index, weight)
        ]
        pieces.append(entry(*columns))
    for t in range(n_tail):
        at = jnp.full((n_exp, slots), n_main + t, jnp.int32) + lane0
        pieces.append(entry(pick(index, at), pick(weight, at)))
    total = n_exp * half_slots
    padded = cdiv(total, LANES) * LANES
    if padded > total:
        pieces.append(jnp.zeros((padded - total, pieces[0].shape[1]), F32))
    spread = jnp.concatenate(pieces, axis=0).T[:out_rows, :]
    high = spread.astype(BF16)
    rest = spread - high.astype(F32)
    mid = rest.astype(BF16)
    low = (rest - mid.astype(F32)).astype(BF16)
    left = jnp.concatenate([high, mid, low], axis=0)
    for e in range(n_exp):
        tail_scr[e * per_back : (e + 1) * per_back, :] = back_ref[e, n_main * all_blocks :, :].astype(F32)
        for j in range(0, all_blocks, 2):
            two = back_ref[e, j * n_main : (j + 2) * n_main, :].astype(F32)
            row_scr[e * n_main : (e + 1) * n_main, j * LANES : (j + 1) * LANES] = two[:n_main]
            row_scr[e * n_main : (e + 1) * n_main, (j + 1) * LANES : (j + 2) * LANES] = two[n_main:]
    for t in range(n_tail):
        rows = slice(main_rows + t * n_exp, main_rows + (t + 1) * n_exp)
        for j in range(all_blocks):
            row_scr[rows, j * LANES : (j + 1) * LANES] = tail_scr[
                pl.ds(t * all_blocks + j, n_exp, stride=per_back), :
            ]
    if padded > total:
        row_scr[total:, :] = jnp.zeros((padded - total, width), F32)
    chunk = 2 * LANES
    for at in range(0, width, chunk):
        cols = slice(at, at + chunk)
        got = jnp.dot(left, row_scr[:, cols].astype(BF16), preferred_element_type=F32)
        out_ref[:, cols] = (
            got[:out_rows] + (got[out_rows : 2 * out_rows] + got[2 * out_rows :])
        ).astype(BF16)


def local(tokens, norm_gain, chosen_rows, route_weights, gate_weight, up_weight, down_weight):
    tok_rows, width = tokens.shape
    n_exp, slots = chosen_rows.shape
    half_slots = slots // 2
    n_main = half_slots // SUB * SUB
    n_tail = half_slots - n_main
    hidden = gate_weight.shape[2]
    chunk_rows = slots * (width // 2) // LANES
    block = jax.ShapeDtypeStruct((n_exp, chunk_rows, LANES), BF16)
    tails = n_exp * 2 * n_tail * (width // 2 // LANES)
    outgoing = pl.pallas_call(
        dispatch_kernel,
        out_shape=block,
        in_specs=[VMEM] * 3,
        out_specs=VMEM,
        scratch_shapes=[pltpu.VMEM((tok_rows, width // 2), BF16), pltpu.VMEM((tails, LANES), F32)],
        name="dispatch",
    )(tokens, norm_gain.reshape(1, width), chosen_rows)
    swap = [(0, 1), (1, 0)]
    mine = lax.all_to_all(outgoing, "ep", split_axis=0, concat_axis=0, tiled=True)
    other = lax.ppermute(mine, "tp", swap)
    rows = n_exp * slots
    send, keep = pl.pallas_call(
        functools.partial(expert_kernel, n_main=n_main, n_tail=n_tail),
        out_shape=[block, block],
        in_specs=[VMEM] * 5,
        out_specs=[VMEM, VMEM],
        scratch_shapes=[
            pltpu.VMEM((rows, width), BF16),
            pltpu.VMEM((rows, hidden), BF16),
            pltpu.VMEM((tails, LANES), F32),
            pltpu.VMEM((2, tails, LANES), F32),
        ],
        name="expert",
    )(mine, other, gate_weight, up_weight, down_weight)
    came = lax.ppermute(send, "tp", swap)
    summed = (keep.astype(F32) + came.astype(F32)).astype(BF16)
    back = lax.all_to_all(summed, "ep", split_axis=0, concat_axis=0, tiled=True)
    padded = cdiv(n_exp * half_slots, LANES) * LANES
    return pl.pallas_call(
        combine_kernel,
        out_shape=jax.ShapeDtypeStruct((tok_rows // 2, width), BF16),
        in_specs=[VMEM] * 3,
        out_specs=VMEM,
        scratch_shapes=[pltpu.VMEM((padded, width), F32), pltpu.VMEM((tails, LANES), F32)],
        name="combine",
    )(back, chosen_rows, route_weights)


def solution(mesh):
    return jax.shard_map(
        local,
        mesh=mesh,
        in_specs=(
            P(("grp", "ep"), None),
            P(),
            P("grp", "ep"),
            P("grp", "ep"),
            P("ep", None, "tp"),
            P("ep", None, "tp"),
            P("ep", "tp", None),
        ),
        out_specs=P(("grp", "ep", "tp"), None),
        check_vma=False,
    )
```

time: 94.5 us -> 49.5 us (0.52)
  waiting for transfers between devices: 22 us -> 3.22 us
  between operations: 13.4 us -> 0.01 us
  Pallas kernels: 0 us -> 11.1 us
  local copies, waits for them, and re-layouts: 11.2 us -> 2 us
  other arithmetic: 9.62 us -> 1.05 us
  matrix products: 7.79 us -> 0 us
  blocking collectives: 24.1 us -> 31.7 us
  starting transfers between devices: 5.73 us -> 0.16 us
    all_to_all x1 -> x0, waiting for transfers between devices: 14.8 us -> none  [local(): lax.all_to_all(expert_out, 'ep', split_axis=0, concat_axis=0, tiled=True)]
    all_to_all x0 -> x1, blocking collectives: none -> 14 us  [local(): back = lax.all_to_all(summed, 'ep', split_axis=0, concat_axis=0, tiled=True)]
    pallas_call x0 -> x3, Pallas kernels: none -> 11.1 us  [the longest x1 6.53 us: local(): pl.pallas_call(functools.partial(expert_kernel, n_main=n_main, n_tail=n_t...]
    dot_general x2 -> x0, matrix products: 7.79 us -> none  [the longest x1 4.3 us: local(): jnp.dot(hidden, down_weight[0], preferred_element_type=jnp.float32)]
    reduce_scatter x1 -> x0, waiting for transfers between devices: 7.16 us -> none  [local(): lax.psum_scatter(jnp.dot(hidden, down_weight[0], preferred_element_type=j...]
    all_to_all x1 -> x0, starting transfers between devices: 5.72 us -> none  [local(): lax.all_to_all(expert_out, 'ep', split_axis=0, concat_axis=0, tiled=True)]
    all_to_all x1, blocking collectives: 21.8 us -> 17.6 us  [local(): lax.all_to_all(outgoing, 'ep', split_axis=0, concat_axis=0, tiled=True)]
    convert_element_type x3 -> x1, other arithmetic: 4.57 us -> 1.05 us  [local(): summed = (keep.astype(F32) + came.astype(F32)).astype(BF16)]
where the time goes in v1:
time: 49.5 us; the launch traced here: 49.2 us
  blocking collectives  31.7 us (64%)
  Pallas kernels  11.1 us (22%)
  waiting for transfers between devices  3.22 us (7%)
  local copies, waits for them, and re-layouts  2 us (4%)
  other arithmetic  1.05 us (2%)
    all_to_all x1, blocking collectives, local(): lax.all_to_all(outgoing, 'ep', split_axis=0, concat_axis=0, tiled=True)  17.6 us
    all_to_all x1, blocking collectives, local(): back = lax.all_to_all(summed, 'ep', split_axis=0, concat_axis=0, tiled=True)  14 us
    pallas_call x1, Pallas kernels, local(): pl.pallas_call(functools.partial(expert_kernel, n_main=n_main, n_tail=n_t...  6.53 us
    pallas_call x1, Pallas kernels, local(): pl.pallas_call(dispatch_kernel, out_shape=block, in_specs=[VMEM] * 3, out...  2.34 us
    pallas_call x1, Pallas kernels, local(): pl.pallas_call(combine_kernel, out_shape=jax.ShapeDtypeStruct((tok_rows /...  2.22 us
    ppermute x1, waiting for transfers between devices, local(): came = lax.ppermute(send, 'tp', swap)  1.64 us
    ppermute x1, waiting for transfers between devices, local(): other = lax.ppermute(mine, 'tp', swap)  1.58 us
    reshape x1, local copies, waits for them, and re-layouts, local(): norm_gain.reshape(1, width)  1.29 us
  transfers between devices with their start and end apart: 2, of which 2 were waited for; matrix products, arithmetic and copies ran while one was open for 0% of the time, Pallas kernels for 0%

profile of v1, /device:TPU:0, one launch (start us, length us, event | category | flops | bytes accessed | tf_op | source)
XLA Modules:
  0.0 49.2 jit_solution(1935404836050462186)
XLA Ops:
  0.0 1.3 %reshape.3.gain_ref = bf16[1,2048]{1,0:T(2,128)(2,1)} reshape(bf16[2048]{0:T(1024)(128)(2,1)} %param.8) | data formatting | bytes 8192 | tf_op jit(solution)/shard_map/reshape | solution.py:230
  1.3 2.3 %dispatch.1 = bf16[8,144,128]{2,1,0:T(8,128)(2,1)} custom-call(bf16[144,2048]{1,0:T(8,128)(2,1)} %tok_ref.1, bf16[1,2048]{1,0:T(2,128)(2,1)} %reshape.3.gain_ref, s32[8,18]{1,0:T(8,128)} %rows_ref.3), custom_call_target="tpu_custom_call" | custom-call | tf_op jit(solution)/shard_map/dispatch/pallas_call | solution.py:223
  3.6 17.6 %all_to_all.10.mine_ref = bf16[8,144,128]{2,1,0:T(8,128)(2,1)S(1)} all-to-all(bf16[8,144,128]{2,1,0:T(8,128)(2,1)} %dispatch.1), channel_id=1, replica_groups=mesh['grp'=2,'ep'=8,'tp'=2] {'ep'}, dimensions={0} | all-to-all | bytes 589824 | tf_op jit(solution)/shard_map/all_to_all | solution.py:232
  21.3 0.0 copy-start
  21.3 0.0 collective-permute-start
  21.3 1.6 %collective-permute-done.other_ref = bf16[8,144,128]{2,1,0:T(8,128)(2,1)S(1)} collective-permute-done((bf16[8,144,128]{2,1,0:T(8,128)(2,1)S(1)}, bf16[8,144,128]{2,1,0:T(8,128)(2,1)S(1)}, u32[]{:S(2)}, u32[]{:S(2)}) %collective-permute-start) | collective-permute-done | bytes 294944 | tf_op jit(solution)/shard_map/ppermute | solution.py:233
  22.9 0.0 copy-done
  22.9 0.0 copy-start.1
  22.9 0.7 %copy-done.1 = bf16[8,144,128]{2,1,0:T(8,128)(2,1)} copy-done((bf16[8,144,128]{2,1,0:T(8,128)(2,1)}, bf16[8,144,128]{2,1,0:T(8,128)(2,1)S(1)}, u32[]{:S(2)}) %copy-start.1) | copy-done | bytes 294936
  23.6 6.5 %expert.1 = (bf16[8,144,128]{2,1,0:T(8,128)(2,1)}, bf16[8,144,128]{2,1,0:T(8,128)(2,1)}) custom-call(bf16[8,144,128]{2,1,0:T(8,128)(2,1)} %copy-done, bf16[8,144,128]{2,1,0:T(8,128)(2,1)} %copy-done.1, bf16[1,2048,768]{2,1,0:T(8,128)(2,1)} %gate_ref.1, bf16[1,2048,768]{2,1,0:T(8,128)(2,1)} %up_ref.1, bf16[1,768,2048]{2,1,0:T(8,128)(2,1)} %down_ref.1), custom_call_target="tpu_custom_call" | custom-call | tf_op jit(solution)/shard_map/expert/pallas_call | solution.py:235
  30.1 0.2 collective-permute-start.1
  30.3 1.6 %collective-permute-done.1 = bf16[8,144,128]{2,1,0:T(8,128)(2,1)S(1)} collective-permute-done((bf16[8,144,128]{2,1,0:T(8,128)(2,1)}, bf16[8,144,128]{2,1,0:T(8,128)(2,1)S(1)}, u32[]{:S(2)}, u32[]{:S(2)}) %collective-permute-start.1) | collective-permute-done | bytes 294944 | tf_op jit(solution)/shard_map/ppermute | solution.py:248
  31.9 1.1 %add_convert_fusion = bf16[8,144,128]{2,1,0:T(8,128)(2,1)S(1)} fusion(bf16[8,144,128]{2,1,0:T(8,128)(2,1)S(1)} %collective-permute-done.1, bf16[8,144,128]{2,1,0:T(8,128)(2,1)} %get-tuple-element.7), kind=kLoop, calls=%fused_computation | loop fusion | flops 589824 | bytes 884736 | tf_op jit(solution)/shard_map/convert_element_type | solution.py:249
  32.9 14.0 %all_to_all.11.back_ref = bf16[8,144,128]{2,1,0:T(8,128)(2,1)} all-to-all(bf16[8,144,128]{2,1,0:T(8,128)(2,1)S(1)} %add_convert_fusion), channel_id=1, replica_groups=mesh['grp'=2,'ep'=8,'tp'=2] {'ep'}, dimensions={0} | all-to-all | bytes 589824 | tf_op jit(solution)/shard_map/all_to_all | solution.py:250
  47.0 2.2 %combine.1 = bf16[72,2048]{1,0:T(8,128)(2,1)} custom-call(bf16[8,144,128]{2,1,0:T(8,128)(2,1)} %all_to_all.11.back_ref, s32[8,18]{1,0:T(8,128)} %rows_ref.3, f32[8,18]{1,0:T(8,128)} %weight_ref.1), custom_call_target="tpu_custom_call" | custom-call | tf_op jit(solution)/shard_map/combine/pallas_call | solution.py:252
Async XLA Ops:
  21.3 1.6 %copy-start = (bf16[8,144,128]{2,1,0:T(8,128)(2,1)}, bf16[8,144,128]{2,1,0:T(8,128)(2,1)S(1)}, u32[]{:S(2)}) copy-start(bf16[8,144,128]{2,1,0:T(8,128)(2,1)S(1)} %all_to_all.10.mine_ref) | copy-start | bytes 884740
  21.3 1.6 %collective-permute-start = (bf16[8,144,128]{2,1,0:T(8,128)(2,1)S(1)}, bf16[8,144,128]{2,1,0:T(8,128)(2,1)S(1)}, u32[]{:S(2)}, u32[]{:S(2)}) collective-permute-start(bf16[8,144,128]{2,1,0:T(8,128)(2,1)S(1)} %all_to_all.10.mine_ref), channel_id=1, source_target_pairs={{0,1},{1,0},{2,3},{3,2},{4,5},{5,4},{6,7},{7,6},{8,9},{9,8},{10,11... | collective-permute-start | bytes 884744 | tf_op jit(solution)/shard_map/ppermute | solution.py:233
  22.9 0.7 %copy-start.1 = (bf16[8,144,128]{2,1,0:T(8,128)(2,1)}, bf16[8,144,128]{2,1,0:T(8,128)(2,1)S(1)}, u32[]{:S(2)}) copy-start(bf16[8,144,128]{2,1,0:T(8,128)(2,1)S(1)} %collective-permute-done.other_ref) | copy-start | bytes 884740
  30.1 1.8 %collective-permute-start.1 = (bf16[8,144,128]{2,1,0:T(8,128)(2,1)}, bf16[8,144,128]{2,1,0:T(8,128)(2,1)S(1)}, u32[]{:S(2)}, u32[]{:S(2)}) collective-permute-start(bf16[8,144,128]{2,1,0:T(8,128)(2,1)} %get-tuple-element.8), channel_id=1, source_target_pairs={{0,1},{1,0},{2,3},{3,2},{4,5},{5,4},{6,7},{7,6},{8,9},{9,8},{10,11... | collective-permute-start | bytes 884744 | tf_op jit(solution)/shard_map/ppermute | solution.py:248

commit v2 on v1

--- a/solution.py
+++ b/solution.py
@@ -9,9 +9,13 @@
 
 LANES = 128
 SUB = 8
+COPIES = 3
+COVER_FLOPS = 4_000_000_000
+VMEM_LIMIT = 32 * 1024 * 1024
 F32 = jnp.float32
 BF16 = jnp.bfloat16
 VMEM = pl.BlockSpec(memory_space=pltpu.VMEM)
+HBM = pl.BlockSpec(memory_space=pltpu.HBM)
 
 
 def cdiv(a, b):
@@ -28,8 +32,26 @@
     return jnp.where(sub < n_main, sub, sub - n_main + half_slots)
 
 
-def dispatch_kernel(tok_ref, gain_ref, rows_ref, out_ref, norm_scr, tail_scr):
+def dispatch_kernel(
+    tok_hbm, gain_hbm, rows_hbm, weight_hbm, out_ref, rows_ref, weight_ref,
+    tok_ref, gain_ref, norm_scr, tail_scr, sems,
+):
     tok_rows, width = tok_ref.shape
+    step = 16
+    cuts = [tok_rows * k // COPIES // step * step for k in range(COPIES)] + [tok_rows]
+    copies = [
+        pltpu.make_async_copy(gain_hbm, gain_ref, sems.at[COPIES]),
+        pltpu.make_async_copy(rows_hbm, rows_ref, sems.at[COPIES + 1]),
+        pltpu.make_async_copy(weight_hbm, weight_ref, sems.at[COPIES + 2]),
+    ]
+    parts = [
+        pltpu.make_async_copy(tok_hbm.at[low:high], tok_ref.at[low:high], sems.at[k])
+        for k, (low, high) in enumerate(zip(cuts, cuts[1:]))
+    ]
+    for copy in copies + parts:
+        copy.start()
+    for copy in copies:
+        copy.wait()
     n_dest, slots = rows_ref.shape
     half_slots = slots // 2
     n_main = half_slots // SUB * SUB
@@ -38,9 +60,13 @@
     blocks = half_width // LANES
     core = lax.axis_index("tp")
     base = pl.multiple_of(core * half_width, half_width)
-    gain = gain_ref[:, pl.ds(base, half_width)].astype(F32)
-    step = 16
+    half_blocks = half_width // LANES
+    gains = gain_ref[...].astype(F32)
+    gains = jnp.where(core == 0, gains[:half_blocks], gains[half_blocks:])
+    gain = jnp.concatenate([gains[j : j + 1, :] for j in range(half_blocks)], axis=1)
     for at in range(0, tok_rows, step):
+        if at in cuts:
+            parts[cuts.index(at)].wait()
         rows = slice(at, at + step)
         values = tok_ref[rows, :].astype(F32)
         scale = lax.rsqrt(jnp.mean(values * values, axis=-1, keepdims=True) + 1e-06)
@@ -148,15 +174,12 @@
         keep_ref[s, n_main * all_blocks :, :] = back_scr[1, rows, :].astype(BF16)
 
 
-def combine_kernel(back_ref, rows_ref, weight_ref, out_ref, row_scr, tail_scr):
+def route_kernel(rows_ref, weight_ref, left_ref):
     n_exp, slots = rows_ref.shape
     half_slots = slots // 2
     n_main = half_slots // SUB * SUB
     n_tail = half_slots - n_main
-    out_rows, width = out_ref.shape
-    all_blocks = width // LANES
-    per_back = n_tail * all_blocks
-    main_rows = n_exp * n_main
+    out_rows = left_ref.shape[0] // 3
     core = lax.axis_index("tp")
     start = lax.axis_index("ep") * (2 * out_rows) + core * out_rows
     index = (rows_ref[...] - start).astype(F32)
@@ -186,7 +209,18 @@
     rest = spread - high.astype(F32)
     mid = rest.astype(BF16)
     low = (rest - mid.astype(F32)).astype(BF16)
-    left = jnp.concatenate([high, mid, low], axis=0)
+    left_ref[...] = jnp.concatenate([high, mid, low], axis=0)
+
+
+def combine_kernel(back_ref, left_ref, out_ref, row_scr, tail_scr, *, n_main, n_tail):
+    n_exp = back_ref.shape[0]
+    out_rows, width = out_ref.shape
+    all_blocks = width // LANES
+    per_back = n_tail * all_blocks
+    main_rows = n_exp * n_main
+    total = n_exp * (n_main + n_tail)
+    padded = row_scr.shape[0]
+    left = left_ref[...]
     for e in range(n_exp):
         tail_scr[e * per_back : (e + 1) * per_back, :] = back_ref[e, n_main * all_blocks :, :].astype(F32)
         for j in range(0, all_blocks, 2):
@@ -220,14 +254,36 @@
     chunk_rows = slots * (width // 2) // LANES
     block = jax.ShapeDtypeStruct((n_exp, chunk_rows, LANES), BF16)
     tails = n_exp * 2 * n_tail * (width // 2 // LANES)
-    outgoing = pl.pallas_call(
+    args = (tokens, norm_gain.reshape(width // LANES, LANES), chosen_rows, route_weights)
+    outgoing, own_rows, own_weights = pl.pallas_call(
         dispatch_kernel,
-        out_shape=block,
-        in_specs=[VMEM] * 3,
+        out_shape=[block] + [jax.ShapeDtypeStruct(x.shape, x.dtype) for x in (chosen_rows, route_weights)],
+        in_specs=[HBM] * 4,
+        out_specs=[VMEM] * 3,
+        scratch_shapes=[
+            pltpu.VMEM((tok_rows, width), BF16),
+            pltpu.VMEM((width // LANES, LANES), BF16),
+            pltpu.VMEM((tok_rows, width // 2), BF16),
+            pltpu.VMEM((tails, LANES), F32),
+            pltpu.SemaphoreType.DMA((COPIES + 3,)),
+        ],
+        compiler_params=pltpu.CompilerParams(vmem_limit_bytes=VMEM_LIMIT),
+        name="dispatch",
+    )(*(pltpu.with_memory_space_constraint(x, pltpu.HBM) for x in args))
+    left_shape = (3 * (tok_rows // 2), cdiv(n_exp * half_slots, LANES) * LANES)
+    weight_bytes = 3 * 2 * width * hidden
+    left = pl.pallas_call(
+        route_kernel,
+        out_shape=jax.ShapeDtypeStruct(left_shape, BF16),
+        in_specs=[VMEM] * 2,
         out_specs=VMEM,
-        scratch_shapes=[pltpu.VMEM((tok_rows, width // 2), BF16), pltpu.VMEM((tails, LANES), F32)],
-        name="dispatch",
-    )(tokens, norm_gain.reshape(1, width), chosen_rows)
+        compiler_params=pltpu.CompilerParams(vmem_limit_bytes=VMEM_LIMIT),
+        cost_estimate=pl.CostEstimate(
+            flops=COVER_FLOPS, bytes_accessed=weight_bytes, transcendentals=0
+        ),
+        name="route",
+    )(own_rows, own_weights)
+    outgoing, left = lax.optimization_barrier((outgoing, left))
     swap = [(0, 1), (1, 0)]
     mine = lax.all_to_all(outgoing, "ep", split_axis=0, concat_axis=0, tiled=True)
     other = lax.ppermute(mine, "tp", swap)
@@ -243,20 +299,21 @@
             pltpu.VMEM((tails, LANES), F32),
             pltpu.VMEM((2, tails, LANES), F32),
         ],
+        compiler_params=pltpu.CompilerParams(vmem_limit_bytes=VMEM_LIMIT),
         name="expert",
     )(mine, other, gate_weight, up_weight, down_weight)
     came = lax.ppermute(send, "tp", swap)
     summed = (keep.astype(F32) + came.astype(F32)).astype(BF16)
     back = lax.all_to_all(summed, "ep", split_axis=0, concat_axis=0, tiled=True)
-    padded = cdiv(n_exp * half_slots, LANES) * LANES
     return pl.pallas_call(
-        combine_kernel,
+        functools.partial(combine_kernel, n_main=n_main, n_tail=n_tail),
         out_shape=jax.ShapeDtypeStruct((tok_rows // 2, width), BF16),
-        in_specs=[VMEM] * 3,
+        in_specs=[VMEM] * 2,
         out_specs=VMEM,
-        scratch_shapes=[pltpu.VMEM((padded, width), F32), pltpu.VMEM((tails, LANES), F32)],
+        scratch_shapes=[pltpu.VMEM((left_shape[1], width), F32), pltpu.VMEM((tails, LANES), F32)],
+        compiler_params=pltpu.CompilerParams(vmem_limit_bytes=VMEM_LIMIT),
         name="combine",
-    )(back, chosen_rows, route_weights)
+    )(back, left)
 
 
 def solution(mesh):

time: 49.5 us -> 39.5 us (0.80)
  Pallas kernels: 11.1 us -> 4.8 us
  local copies, waits for them, and re-layouts: 2 us -> 0.02 us
  other arithmetic: 1.05 us -> 0.08 us
  blocking collectives: 31.7 us -> 31 us
    pallas_call x1, Pallas kernels: 6.53 us -> 1.76 us  [local(): pl.pallas_call(functools.partial(expert_kernel, n_main=n_main, n_tail=n_t...]
    pallas_call x2 -> x3, Pallas kernels: 4.56 us -> 3.04 us  [the longest x1 1.74 us: local(): pl.pallas_call(dispatch_kernel, out_shape=[block] + [jax.ShapeDtypeStruct...]
    reshape x1 -> x0, local copies, waits for them, and re-layouts: 1.29 us -> none  [local(): norm_gain.reshape(1, width)]
    convert_element_type x1, other arithmetic: 1.05 us -> 0.08 us  [local(): summed = (keep.astype(F32) + came.astype(F32)).astype(BF16)]
    unnamed x4 -> x6, local copies, waits for them, and re-layouts: 0.71 us -> 0.02 us
    all_to_all x1, blocking collectives: 14 us -> 13.3 us  [local(): back = lax.all_to_all(summed, 'ep', split_axis=0, concat_axis=0, tiled=True)]
where the time goes in v2:
time: 39.5 us; the launch traced here: 39.2 us
  blocking collectives  31 us (78%)
  Pallas kernels  4.8 us (12%)
  waiting for transfers between devices  2.99 us (8%)
    all_to_all x1, blocking collectives, local(): lax.all_to_all(outgoing, 'ep', split_axis=0, concat_axis=0, tiled=True)  17.7 us
    all_to_all x1, blocking collectives, local(): back = lax.all_to_all(summed, 'ep', split_axis=0, concat_axis=0, tiled=True)  13.3 us
    pallas_call x1, Pallas kernels, local(): pl.pallas_call(functools.partial(expert_kernel, n_main=n_main, n_tail=n_t...  1.76 us
    pallas_call x1, Pallas kernels, local(): pl.pallas_call(dispatch_kernel, out_shape=[block] + [jax.ShapeDtypeStruct...  1.74 us
    ppermute x1, waiting for transfers between devices, local(): other = lax.ppermute(mine, 'tp', swap)  1.58 us
    ppermute x1, waiting for transfers between devices, local(): came = lax.ppermute(send, 'tp', swap)  1.41 us
    pallas_call x1, Pallas kernels, local(): pl.pallas_call(functools.partial(combine_kernel, n_main=n_main, n_tail=n_...  1.11 us
  transfers between devices with their start and end apart: 2, of which 2 were waited for; matrix products, arithmetic and copies ran while one was open for 0% of the time, Pallas kernels for 0%

profile of v2, /device:TPU:0, one launch (start us, length us, event | category | flops | bytes accessed | tf_op | source)
XLA Modules:
  0.0 39.2 jit_solution(3277611854393433568)
XLA Ops:
  0.0 1.7 %dispatch.1 = (bf16[8,144,128]{2,1,0:T(8,128)(2,1)S(1)}, s32[8,18]{1,0:T(8,128)S(1)}, f32[8,18]{1,0:T(8,128)S(1)}) custom-call(bf16[144,2048]{1,0:T(8,128)(2,1)} %tok_hbm.1, bf16[16,128]{1,0:T(8,128)(2,1)} %bitcast.1, s32[8,18]{1,0:T(8,128)} %rows_hbm.1, f32[8,18]{1,0:T(8,128)} %weight_hbm.1), custom_call_target="tpu_custom_call" | custom-call | tf_op jit(solution)/shard_map/dispatch/pallas_call | solution.py:258
  1.7 0.0 copy-start
  1.8 0.0 copy-start.1
  1.8 0.0 copy-start.2
  1.8 0.2 route.1.left_ref
  2.0 17.7 %all_to_all.10.mine_ref = bf16[8,144,128]{2,1,0:T(8,128)(2,1)S(1)} all-to-all(bf16[8,144,128]{2,1,0:T(8,128)(2,1)S(1)} %get-tuple-element.15), channel_id=1, replica_groups=mesh['grp'=2,'ep'=8,'tp'=2] {'ep'}, dimensions={0} | all-to-all | bytes 589824 | tf_op jit(solution)/shard_map/all_to_all | solution.py:288
  19.7 0.0 collective-permute-start
  19.7 1.6 %collective-permute-done.other_ref = bf16[8,144,128]{2,1,0:T(8,128)(2,1)S(1)} collective-permute-done((bf16[8,144,128]{2,1,0:T(8,128)(2,1)S(1)}, bf16[8,144,128]{2,1,0:T(8,128)(2,1)S(1)}, u32[]{:S(2)}, u32[]{:S(2)}) %collective-permute-start) | collective-permute-done | bytes 294944 | tf_op jit(solution)/shard_map/ppermute | solution.py:289
  21.3 0.0 copy-done
  21.3 0.0 copy-done.1
  21.3 0.0 copy-done.2
  21.3 1.8 %expert.1 = (bf16[8,144,128]{2,1,0:T(8,128)(2,1)S(1)}, bf16[8,144,128]{2,1,0:T(8,128)(2,1)S(1)}) custom-call(bf16[8,144,128]{2,1,0:T(8,128)(2,1)S(1)} %all_to_all.10.mine_ref, bf16[8,144,128]{2,1,0:T(8,128)(2,1)S(1)} %collective-permute-done.other_ref, bf16[1,2048,768]{2,1,0:T(8,128)(2,1)S(1)} %copy-done, bf16[1,2048,768]{2,1,0:T(8,128)(2,1)S(1)} %copy-done.1, ...), custom_call_target="tpu_custom_call" | custom-call | tf_op jit(solution)/shard_map/expert/pallas_call | solution.py:291
  23.0 0.2 collective-permute-start.1
  23.3 1.4 %collective-permute-done.1 = bf16[8,144,128]{2,1,0:T(8,128)(2,1)S(1)} collective-permute-done((bf16[8,144,128]{2,1,0:T(8,128)(2,1)S(1)}, bf16[8,144,128]{2,1,0:T(8,128)(2,1)S(1)}, u32[]{:S(2)}, u32[]{:S(2)}) %collective-permute-start.1) | collective-permute-done | bytes 294944 | tf_op jit(solution)/shard_map/ppermute | solution.py:305
  24.7 0.1 add_convert_fusion
  24.8 13.3 %all_to_all.11.back_ref = bf16[8,144,128]{2,1,0:T(8,128)(2,1)S(1)} all-to-all(bf16[8,144,128]{2,1,0:T(8,128)(2,1)S(1)} %add_convert_fusion), channel_id=1, replica_groups=mesh['grp'=2,'ep'=8,'tp'=2] {'ep'}, dimensions={0} | all-to-all | bytes 589824 | tf_op jit(solution)/shard_map/all_to_all | solution.py:307
  38.1 1.1 %combine.1 = bf16[72,2048]{1,0:T(8,128)(2,1)} custom-call(bf16[8,144,128]{2,1,0:T(8,128)(2,1)S(1)} %all_to_all.11.back_ref, bf16[216,128]{1,0:T(8,128)(2,1)S(1)} %route.1.left_ref), custom_call_target="tpu_custom_call" | custom-call | tf_op jit(solution)/shard_map/combine/pallas_call | solution.py:308
Async XLA Ops:
  1.7 19.5 %copy-start = (bf16[1,2048,768]{2,1,0:T(8,128)(2,1)S(1)}, bf16[1,2048,768]{2,1,0:T(8,128)(2,1)}, u32[]{:S(2)}) copy-start(bf16[1,2048,768]{2,1,0:T(8,128)(2,1)} %gate_ref.1) | copy-start | bytes 9437188
  1.8 19.5 %copy-start.1 = (bf16[1,2048,768]{2,1,0:T(8,128)(2,1)S(1)}, bf16[1,2048,768]{2,1,0:T(8,128)(2,1)}, u32[]{:S(2)}) copy-start(bf16[1,2048,768]{2,1,0:T(8,128)(2,1)} %up_ref.1) | copy-start | bytes 9437188
  1.8 19.5 %copy-start.2 = (bf16[1,768,2048]{2,1,0:T(8,128)(2,1)S(1)}, bf16[1,768,2048]{2,1,0:T(8,128)(2,1)}, u32[]{:S(2)}) copy-start(bf16[1,768,2048]{2,1,0:T(8,128)(2,1)} %down_ref.1) | copy-start | bytes 9437188
  19.7 1.6 %collective-permute-start = (bf16[8,144,128]{2,1,0:T(8,128)(2,1)S(1)}, bf16[8,144,128]{2,1,0:T(8,128)(2,1)S(1)}, u32[]{:S(2)}, u32[]{:S(2)}) collective-permute-start(bf16[8,144,128]{2,1,0:T(8,128)(2,1)S(1)} %all_to_all.10.mine_ref), channel_id=1, source_target_pairs={{0,1},{1,0},{2,3},{3,2},{4,5},{5,4},{6,7},{7,6},{8,9},{9,8},{10,11... | collective-permute-start | bytes 884744 | tf_op jit(solution)/shard_map/ppermute | solution.py:289
  23.0 1.6 %collective-permute-start.1 = (bf16[8,144,128]{2,1,0:T(8,128)(2,1)S(1)}, bf16[8,144,128]{2,1,0:T(8,128)(2,1)S(1)}, u32[]{:S(2)}, u32[]{:S(2)}) collective-permute-start(bf16[8,144,128]{2,1,0:T(8,128)(2,1)S(1)} %get-tuple-element.17), channel_id=1, source_target_pairs={{0,1},{1,0},{2,3},{3,2},{4,5},{5,4},{6,7},{7,6},{8,9},{9,8},{10,11... | collective-permute-start | bytes 884744 | tf_op jit(solution)/shard_map/ppermute | solution.py:305

commit v3 on v2

v3 whole, which is shorter than its diff:
```python
import functools

import jax
import jax.numpy as jnp
from jax import lax
from jax.experimental import pallas as pl
from jax.experimental.pallas import tpu as pltpu
from jax.sharding import PartitionSpec as P

LANES = 128
SUB = 8
COPIES = 3
COVER_FLOPS = 4_000_000_000
VMEM_LIMIT = 32 * 1024 * 1024
F32 = jnp.float32
BF16 = jnp.bfloat16
SWAP = [(0, 1), (1, 0)]
VMEM = pl.BlockSpec(memory_space=pltpu.VMEM)
HBM = pl.BlockSpec(memory_space=pltpu.HBM)


def cdiv(a, b):
    return (a + b - 1) // b


def partner(core, m, count):
    return lax.axis_index("ep") ^ (2 * (count - 1 - m) + core)


def pick(values, wanted):
    lane = lax.broadcasted_iota(jnp.int32, values.shape, 1)
    return jnp.sum(jnp.where(lane == wanted, values, 0.0), axis=1, keepdims=True)


def split_slots(slots):
    half_slots = slots // 2
    n_main = half_slots // SUB * SUB
    return half_slots, n_main, half_slots - n_main


def dispatch_kernel(*refs, count):
    tok_hbm, gain_hbm, rows_hbm, weight_hbm = refs[:4]
    outs = refs[4 : 4 + count]
    rows_ref, weight_ref, tok_ref, gain_ref, norm_scr, tail_scr, index_scr, sems = refs[4 + count :]
    tok_rows, width = tok_ref.shape
    slots = rows_ref.shape[1]
    step = 16
    cuts = [tok_rows * k // COPIES // step * step for k in range(COPIES)] + [tok_rows]
    copies = [
        pltpu.make_async_copy(gain_hbm, gain_ref, sems.at[COPIES]),
        pltpu.make_async_copy(rows_hbm, rows_ref, sems.at[COPIES + 1]),
        pltpu.make_async_copy(weight_hbm, weight_ref, sems.at[COPIES + 2]),
    ]
    parts = [
        pltpu.make_async_copy(tok_hbm.at[low:high], tok_ref.at[low:high], sems.at[k])
        for k, (low, high) in enumerate(zip(cuts, cuts[1:]))
    ]
    for copy in copies + parts:
        copy.start()
    for copy in copies:
        copy.wait()
    half_slots, n_main, n_tail = split_slots(slots)
    group = 2 * n_main
    blocks = width // LANES
    core = lax.axis_index("tp")
    index_scr[...] = jnp.zeros_like(index_scr)
    for m in range(count):
        index_scr[m : m + 1, :] = rows_ref[pl.ds(partner(core, m, count), 1), :]
    index = (index_scr[...] - lax.axis_index("ep") * tok_rows).astype(F32)
    sub = lax.broadcasted_iota(jnp.int32, (group, slots), 0)
    wanted = jnp.where(sub < n_main, sub, sub - n_main + half_slots)

    def one_hot(column):
        token = lax.broadcasted_iota(jnp.int32, (column.shape[0], tok_rows), 1)
        return jnp.where(token == column.astype(jnp.int32), 1.0, 0.0).astype(BF16)

    mains = [
        one_hot(pick(jnp.broadcast_to(index[m : m + 1, :], (group, slots)), wanted))
        for m in range(count)
    ]
    tails = [
        one_hot(pick(index, jnp.full(index.shape, h * half_slots + n_main + t, jnp.int32)))
        for h in range(2)
        for t in range(n_tail)
    ]
    gains = gain_ref[...].astype(F32)
    gain = jnp.concatenate([gains[j : j + 1, :] for j in range(blocks)], axis=1)
    for at in range(0, tok_rows, step):
        if at in cuts:
            parts[cuts.index(at)].wait()
        rows = slice(at, at + step)
        values = tok_ref[rows, :].astype(F32)
        scale = lax.rsqrt(jnp.mean(values * values, axis=-1, keepdims=True) + 1e-06)
        norm_scr[rows, :] = (values * scale * gain).astype(BF16)
    normed = norm_scr[...]
    together = 8
    for first in range(0, count, together):
        members = range(first, min(first + together, count))
        got = jnp.dot(
            jnp.concatenate([mains[m] for m in members], axis=0), normed, preferred_element_type=F32
        )
        for m in members:
            at = (m - first) * group
            for j in range(blocks):
                outs[m][j * group : (j + 1) * group, :] = got[
                    at : at + group, j * LANES : (j + 1) * LANES
                ].astype(BF16)
    got = jnp.dot(jnp.concatenate(tails, axis=0), normed, preferred_element_type=F32)
    padded = index.shape[0]
    per_block = 2 * n_tail * blocks
    for k in range(2 * n_tail):
        for j in range(blocks):
            tail_scr[pl.ds(k * blocks + j, padded, stride=per_block), :] = got[
                k * padded : (k + 1) * padded, j * LANES : (j + 1) * LANES
            ]
    for m in range(count):
        outs[m][group * blocks :, :] = tail_scr[m * per_block : (m + 1) * per_block, :].astype(BF16)


def expert_kernel(*refs, count, slots):
    mine, other = refs[:count], refs[count : 2 * count]
    gate_ref, up_ref, down_ref = refs[2 * count : 2 * count + 3]
    send, keep = refs[2 * count + 3 : 3 * count + 3], refs[3 * count + 3 : 4 * count + 3]
    x_scr, hidden_scr, tail_scr, back_scr = refs[4 * count + 3 :]
    _, width, hidden = gate_ref.shape
    n_main, n_tail = split_slots(slots)[1:]
    group = 2 * n_main
    blocks = width // LANES
    n_src = 2 * count
    main_rows = n_src * group
    per_block = 2 * n_tail * blocks
    core = lax.axis_index("tp")
    for side, base in ((mine, core * count), (other, (1 - core) * count)):
        for m in range(count):
            rows = pl.ds(pl.multiple_of((base + m) * group, group), group)
            for j in range(blocks):
                x_scr[rows, j * LANES : (j + 1) * LANES] = side[m][j * group : (j + 1) * group, :]
            rows = pl.ds(pl.multiple_of((base + m) * per_block, per_block), per_block)
            tail_scr[rows, :] = side[m][group * blocks :, :].astype(F32)
    for j in range(blocks):
        rest = [
            tail_scr[pl.ds(k * blocks + j, n_src, stride=per_block), :] for k in range(2 * n_tail)
        ]
        x_scr[main_rows:, j * LANES : (j + 1) * LANES] = jnp.concatenate(rest, axis=0).astype(BF16)
    chunk = 2 * LANES
    x = x_scr[...]
    for at in range(0, hidden, chunk):
        cols = slice(at, at + chunk)
        gate = jnp.dot(x, gate_ref[0, :, cols], preferred_element_type=F32)
        up = jnp.dot(x, up_ref[0, :, cols], preferred_element_type=F32)
        hidden_scr[:, cols] = (gate / (1.0 + jnp.exp(-gate)) * up).astype(BF16)
    act = hidden_scr[...]
    first = core == 0
    for at in range(0, width, chunk):
        part = jnp.dot(act, down_ref[0, :, at : at + chunk], preferred_element_type=F32)
        for b in range(chunk // LANES):
            lanes = slice(b * LANES, (b + 1) * LANES)
            j = at // LANES + b
            place = slice(j * group, (j + 1) * group)
            for m in range(count):
                low, high = (part[(s + m) * group : (s + m + 1) * group, lanes] for s in (0, count))
                send[m][place, :] = jnp.where(first, high, low).astype(BF16)
                keep[m][place, :] = jnp.where(first, low, high).astype(BF16)
            for k in range(2 * n_tail):
                row = main_rows + k * n_src
                back_scr[pl.ds(k * blocks + j, n_src, stride=per_block), :] = part[row : row + n_src, lanes]
    for m in range(count):
        low, high = (back_scr[(s + m) * per_block : (s + m + 1) * per_block, :] for s in (0, count))
        send[m][group * blocks :, :] = jnp.where(first, high, low).astype(BF16)
        keep[m][group * blocks :, :] = jnp.where(first, low, high).astype(BF16)


def route_kernel(rows_ref, weight_ref, left_ref, index_scr, weight_scr):
    n_exp, slots = rows_ref.shape
    half_slots, n_main, n_tail = split_slots(slots)
    count = n_exp // 2
    out_rows = left_ref.shape[0] // 3
    core = lax.axis_index("tp")
    for side in range(2):
        for m in range(count):
            b = side * count + m
            row = pl.ds(partner(side, m, count), 1)
            index_scr[b : b + 1, :] = rows_ref[row, :]
            weight_scr[b : b + 1, :] = weight_ref[row, :]
    start = lax.axis_index("ep") * (2 * out_rows) + core * out_rows
    index = (index_scr[...] - start).astype(F32)
    weight = weight_scr[...]
    lane0 = core * half_slots
    wanted = lax.broadcasted_iota(jnp.int32, (n_main, slots), 0) + lane0
    pieces = []

    def entry(idx, wgt):
        token = lax.broadcasted_iota(jnp.int32, (idx.shape[0], cdiv(out_rows, LANES) * LANES), 1)
        return jnp.where(token == idx.astype(jnp.int32), wgt, 0.0)

    for e in range(n_exp):
        columns = [
            pick(jnp.broadcast_to(v[e : e + 1, :], (n_main, slots)), wanted) for v in (index, weight)
        ]
        pieces.append(entry(*columns))
    for t in range(n_tail):
        at = jnp.full((n_exp, slots), n_main + t, jnp.int32) + lane0
        pieces.append(entry(pick(index, at), pick(weight, at)))
    total = n_exp * half_slots
    padded = left_ref.shape[1]
    if padded > total:
        pieces.append(jnp.zeros((padded - total, pieces[0].shape[1]), F32))
    spread = jnp.concatenate(pieces, axis=0).T[:out_rows, :]
    high = spread.astype(BF16)
    rest = spread - high.astype(F32)
    mid = rest.astype(BF16)
    low = (rest - mid.astype(F32)).astype(BF16)
    left_ref[...] = jnp.concatenate([high, mid, low], axis=0)


def combine_kernel(*refs, count, slots):
    mine, other = refs[:count], refs[count : 2 * count]
    left_ref, out_ref, row_scr, tail_scr = refs[2 * count :]
    n_exp = 2 * count
    out_rows, width = out_ref.shape
    half_slots, n_main, n_tail = split_slots(slots)
    group = 2 * n_main
    blocks = width // LANES
    per_half = n_tail * blocks
    main_rows = n_exp * n_main
    total = n_exp * half_slots
    padded = row_scr.shape[0]
    core = lax.axis_index("tp")
    first = core == 0
    for side, base in ((mine, core * count), (other, (1 - core) * count)):
        for m in range(count):
            rows = pl.ds(pl.multiple_of((base + m) * n_main, n_main), n_main)
            for j in range(blocks):
                two = side[m][j * group : (j + 1) * group, :].astype(F32)
                row_scr[rows, j * LANES : (j + 1) * LANES] = jnp.where(first, two[:n_main], two[n_main:])
            two = side[m][group * blocks :, :].astype(F32)
            rows = pl.ds(pl.multiple_of((base + m) * per_half, per_half), per_half)
            tail_scr[rows, :] = jnp.where(first, two[:per_half], two[per_half:])
    for t in range(n_tail):
        rows = slice(main_rows + t * n_exp, main_rows + (t + 1) * n_exp)
        for j in range(blocks):
            row_scr[rows, j * LANES : (j + 1) * LANES] = tail_scr[
                pl.ds(t * blocks + j, n_exp, stride=per_half), :
            ]
    if padded > total:
        row_scr[total:, :] = jnp.zeros((padded - total, width), F32)
    left = left_ref[...]
    chunk = 2 * LANES
    for at in range(0, width, chunk):
        cols = slice(at, at + chunk)
        got = jnp.dot(left, row_scr[:, cols].astype(BF16), preferred_element_type=F32)
        out_ref[:, cols] = (
            got[:out_rows] + (got[out_rows : 2 * out_rows] + got[2 * out_rows :])
        ).astype(BF16)


def exchange(blocks, n_exp):
    count = len(blocks)
    came = []
    for m, block in enumerate(blocks):
        far = 2 * (count - 1 - m)
        pairs = [(2 * e + c, 2 * (e ^ (far + c)) + c) for e in range(n_exp) for c in range(2)]
        came.append(lax.ppermute(block, ("ep", "tp"), pairs))
    return came + [lax.ppermute(block, "tp", SWAP) for block in came]


def local(tokens, norm_gain, chosen_rows, route_weights, gate_weight, up_weight, down_weight):
    tok_rows, width = tokens.shape
    n_exp, slots = chosen_rows.shape
    half_slots, n_main, n_tail = split_slots(slots)
    count = n_exp // 2
    hidden = gate_weight.shape[2]
    blocks = width // LANES
    block = jax.ShapeDtypeStruct((slots * blocks, LANES), BF16)
    padded = cdiv(count, SUB) * SUB
    args = (tokens, norm_gain.reshape(blocks, LANES), chosen_rows, route_weights)
    params = pltpu.CompilerParams(vmem_limit_bytes=VMEM_LIMIT)
    *outgoing, own_rows, own_weights = pl.pallas_call(
        functools.partial(dispatch_kernel, count=count),
        out_shape=[block] * count
        + [jax.ShapeDtypeStruct(x.shape, x.dtype) for x in (chosen_rows, route_weights)],
        in_specs=[HBM] * 4,
        out_specs=[VMEM] * (count + 2),
        scratch_shapes=[
            pltpu.VMEM((tok_rows, width), BF16),
            pltpu.VMEM((blocks, LANES), BF16),
            pltpu.VMEM((tok_rows, width), BF16),
            pltpu.VMEM((padded * 2 * n_tail * blocks, LANES), F32),
            pltpu.VMEM((padded, slots), jnp.int32),
            pltpu.SemaphoreType.DMA((COPIES + 3,)),
        ],
        compiler_params=params,
        name="dispatch",
    )(*(pltpu.with_memory_space_constraint(x, pltpu.HBM) for x in args))
    left_shape = (3 * (tok_rows // 2), cdiv(n_exp * half_slots, LANES) * LANES)
    weight_bytes = 3 * 2 * width * hidden
    left = pl.pallas_call(
        route_kernel,
        out_shape=jax.ShapeDtypeStruct(left_shape, BF16),
        in_specs=[VMEM] * 2,
        out_specs=VMEM,
        scratch_shapes=[pltpu.VMEM((n_exp, slots), jnp.int32), pltpu.VMEM((n_exp, slots), F32)],
        compiler_params=params,
        cost_estimate=pl.CostEstimate(
            flops=COVER_FLOPS, bytes_accessed=weight_bytes, transcendentals=0
        ),
        name="route",
    )(own_rows, own_weights)
    *outgoing, left = lax.optimization_barrier((*outgoing, left))
    arrived = exchange(outgoing, n_exp)
    tails = n_exp * 2 * n_tail * blocks
    results = pl.pallas_call(
        functools.partial(expert_kernel, count=count, slots=slots),
        out_shape=[block] * (2 * count),
        in_specs=[VMEM] * (2 * count + 3),
        out_specs=[VMEM] * (2 * count),
        scratch_shapes=[
            pltpu.VMEM((n_exp * slots, width), BF16),
            pltpu.VMEM((n_exp * slots, hidden), BF16),
            pltpu.VMEM((tails, LANES), F32),
            pltpu.VMEM((tails, LANES), F32),
        ],
        compiler_params=params,
        name="expert",
    )(*arrived, gate_weight, up_weight, down_weight)
    came = [lax.ppermute(part, "tp", SWAP) for part in results[:count]]
    summed = [(a.astype(F32) + b.astype(F32)).astype(BF16) for a, b in zip(results[count:], came)]
    back = exchange(summed, n_exp)
    return pl.pallas_call(
        functools.partial(combine_kernel, count=count, slots=slots),
        out_shape=jax.ShapeDtypeStruct((tok_rows // 2, width), BF16),
        in_specs=[VMEM] * (2 * count + 1),
        out_specs=VMEM,
        scratch_shapes=[
            pltpu.VMEM((left_shape[1], width), F32),
            pltpu.VMEM((n_exp * n_tail * blocks, LANES), F32),
        ],
        compiler_params=params,
        name="combine",
    )(*back, left)


def solution(mesh):
    return jax.shard_map(
        local,
        mesh=mesh,
        in_specs=(
            P(("grp", "ep"), None),
            P(),
            P("grp", "ep"),
            P("grp", "ep"),
            P("ep", None, "tp"),
            P("ep", None, "tp"),
            P("ep", "tp", None),
        ),
        out_specs=P(("grp", "ep", "tp"), None),
        check_vma=False,
    )
```

time: 39.5 us -> 32.2 us (0.82)
  blocking collectives: 31 us -> 0 us
  starting transfers between devices: 0.24 us -> 16.1 us
  waiting for transfers between devices: 2.99 us -> 10.7 us
    all_to_all x2 -> x0, blocking collectives: 31 us -> none  [the longest x1 17.7 us: local(): lax.all_to_all(outgoing, 'ep', split_axis=0, concat_axis=0, tiled=True)]
    ppermute x2 -> x20, starting transfers between devices: 0.24 us -> 16.1 us  [the longest x8 11.7 us: exchange(): came.append(lax.ppermute(block, ('ep', 'tp'), pairs))]
    ppermute x2 -> x20, waiting for transfers between devices: 2.99 us -> 10.7 us  [the longest x8 8.35 us: exchange(): came.append(lax.ppermute(block, ('ep', 'tp'), pairs))]
  transfers between devices with their start and end apart: 2 -> 20, of which waited for: 2 -> 11; matrix products, arithmetic and copies ran while one was open for 0% -> 0% of each run, Pallas kernels for 0% -> 0%
where the time goes in v3:
time: 32.2 us; the launch traced here: 32 us
  starting transfers between devices  16.1 us (50%)
  waiting for transfers between devices  10.7 us (33%)
  Pallas kernels  4.94 us (15%)
    ppermute x8, starting transfers between devices, exchange(): came.append(lax.ppermute(block, ('ep', 'tp'), pairs))  11.7 us
    ppermute x8, waiting for transfers between devices, exchange(): came.append(lax.ppermute(block, ('ep', 'tp'), pairs))  8.35 us
    ppermute x8, starting transfers between devices, exchange(): return came + [lax.ppermute(block, 'tp', SWAP) for block in came]  3.37 us
    ppermute x8, waiting for transfers between devices, exchange(): return came + [lax.ppermute(block, 'tp', SWAP) for block in came]  2.11 us
    pallas_call x1, Pallas kernels, local(): pl.pallas_call(functools.partial(expert_kernel, count=count, slots=slots)...  1.83 us
    pallas_call x1, Pallas kernels, local(): pl.pallas_call(functools.partial(dispatch_kernel, count=count), out_shape...  1.74 us
    pallas_call x1, Pallas kernels, local(): pl.pallas_call(functools.partial(combine_kernel, count=count, slots=slots...  1.17 us
    ppermute x4, starting transfers between devices, local(): came = [lax.ppermute(part, 'tp', SWAP) for part in results[:count]]  1.09 us
  transfers between devices with their start and end apart: 20, of which 11 were waited for; matrix products, arithmetic and copies ran while one was open for 0% of the time, Pallas kernels for 0%

profile of v3, /device:TPU:0, one launch (start us, length us, event | category | flops | bytes accessed | tf_op | source)
XLA Modules:
  0.0 32.0 jit_solution(14457124612674534827)
XLA Ops:
  0.0 1.7 %dispatch.1 = (bf16[288,128]{1,0:T(8,128)(2,1)S(1)}, bf16[288,128]{1,0:T(8,128)(2,1)S(1)}, bf16[288,128]{1,0:T(8,128)(2,1)S(1)}, bf16[288,128]{1,0:T(8,128)(2,1)...) custom-call(bf16[144,2048]{1,0:T(8,128)(2,1)} %refs_0_.1, bf16[16,128]{1,0:T(8,128)(2,1)} %bitcast.1, s32[8,18]{1,0:T(8,128)} %refs_2_.1, ...), custom_call_target="tpu_custom_call" | custom-call | tf_op jit(solution)/shard_map/dispatch/pallas_call | solution.py:278
  1.8 0.0 copy-start
  1.8 0.0 copy-start.1
  1.8 0.0 copy-start.2
  1.8 0.2 route.1.refs_8_
  2.0 5.1 %collective-permute-start = (bf16[288,128]{1,0:T(8,128)(2,1)S(1)}, bf16[288,128]{1,0:T(8,128)(2,1)S(1)}, u32[]{:S(2)}, u32[]{:S(2)}) collective-permute-start(bf16[288,128]{1,0:T(8,128)(2,1)S(1)} %get-tuple-element.30), channel_id=1, source_target_pairs={{0,12},{1,15},{2,14},{3,13},{4,8},{5,11},{6,10},{7,9},{8,4},{9,7},... | collective-permute-start | bytes 221192 | tf_op jit(solution)/shard_map/ppermute | solution.py:263
  7.1 0.0 collective-permute-start.1
  7.1 0.6 %collective-permute-start.2 = (bf16[288,128]{1,0:T(8,128)(2,1)S(1)}, bf16[288,128]{1,0:T(8,128)(2,1)S(1)}, u32[]{:S(2)}, u32[]{:S(2)}) collective-permute-start(bf16[288,128]{1,0:T(8,128)(2,1)S(1)} %get-tuple-element.32), channel_id=1, source_target_pairs={{0,4},{1,7},{2,6},{3,5},{4,0},{5,3},{6,2},{7,1},{8,12},{9,15},{10,... | collective-permute-start | bytes 221192 | tf_op jit(solution)/shard_map/ppermute | solution.py:263
  7.8 0.7 %collective-permute-start.3 = (bf16[288,128]{1,0:T(8,128)(2,1)S(1)}, bf16[288,128]{1,0:T(8,128)(2,1)S(1)}, u32[]{:S(2)}, u32[]{:S(2)}) collective-permute-start(bf16[288,128]{1,0:T(8,128)(2,1)S(1)} %get-tuple-element.33), channel_id=1, source_target_pairs={{0,0},{1,3},{2,2},{3,1},{4,4},{5,7},{6,6},{7,5},{8,8},{9,11},{10,1... | collective-permute-start | bytes 221192 | tf_op jit(solution)/shard_map/ppermute | solution.py:263
  8.4 1.9 %collective-permute-done.refs_0_ = bf16[288,128]{1,0:T(8,128)(2,1)S(1)} collective-permute-done((bf16[288,128]{1,0:T(8,128)(2,1)S(1)}, bf16[288,128]{1,0:T(8,128)(2,1)S(1)}, u32[]{:S(2)}, u32[]{:S(2)}) %collective-permute-start) | collective-permute-done | bytes 73760 | tf_op jit(solution)/shard_map/ppermute | solution.py:263
  10.3 0.9 %collective-permute-start.4 = (bf16[288,128]{1,0:T(8,128)(2,1)S(1)}, bf16[288,128]{1,0:T(8,128)(2,1)S(1)}, u32[]{:S(2)}, u32[]{:S(2)}) collective-permute-start(bf16[288,128]{1,0:T(8,128)(2,1)S(1)} %collective-permute-done.refs_0_), channel_id=1, source_target_pairs={{0,1},{1,0},{2,3},{3,2},{4,5},{5,4},{6,7},{7,6},{8,9},{9,8},{10,11... | collective-permute-start | bytes 221192 | tf_op jit(solution)/shard_map/ppermute | solution.py:264
  11.2 3.1 %collective-permute-done.1.refs_1_ = bf16[288,128]{1,0:T(8,128)(2,1)S(1)} collective-permute-done((bf16[288,128]{1,0:T(8,128)(2,1)S(1)}, bf16[288,128]{1,0:T(8,128)(2,1)S(1)}, u32[]{:S(2)}, u32[]{:S(2)}) %collective-permute-start.1) | collective-permute-done | bytes 73760 | tf_op jit(solution)/shard_map/ppermute | solution.py:263
  14.3 0.0 collective-permute-start.5
  14.3 0.0 collective-permute-done.2.refs_2_
  14.3 0.5 %collective-permute-start.6 = (bf16[288,128]{1,0:T(8,128)(2,1)S(1)}, bf16[288,128]{1,0:T(8,128)(2,1)S(1)}, u32[]{:S(2)}, u32[]{:S(2)}) collective-permute-start(bf16[288,128]{1,0:T(8,128)(2,1)S(1)} %collective-permute-done.2.refs_2_), channel_id=1, source_target_pairs={{0,1},{1,0},{2,3},{3,2},{4,5},{5,4},{6,7},{7,6},{8,9},{9,8},{10,11... | collective-permute-start | bytes 221192 | tf_op jit(solution)/shard_map/ppermute | solution.py:264
  14.8 0.0 collective-permute-done.3.refs_3_
  14.8 0.1 collective-permute-start.7
  14.8 0.0 collective-permute-done.4.refs_4_
  14.8 0.7 %collective-permute-done.5.refs_5_ = bf16[288,128]{1,0:T(8,128)(2,1)S(1)} collective-permute-done((bf16[288,128]{1,0:T(8,128)(2,1)S(1)}, bf16[288,128]{1,0:T(8,128)(2,1)S(1)}, u32[]{:S(2)}, u32[]{:S(2)}) %collective-permute-start.5) | collective-permute-done | bytes 73760 | tf_op jit(solution)/shard_map/ppermute | solution.py:264
  15.5 0.2 collective-permute-done.6.refs_6_
  15.7 0.4 %collective-permute-done.7.refs_7_ = bf16[288,128]{1,0:T(8,128)(2,1)S(1)} collective-permute-done((bf16[288,128]{1,0:T(8,128)(2,1)S(1)}, bf16[288,128]{1,0:T(8,128)(2,1)S(1)}, u32[]{:S(2)}, u32[]{:S(2)}) %collective-permute-start.7) | collective-permute-done | bytes 73760 | tf_op jit(solution)/shard_map/ppermute | solution.py:264
  16.0 0.0 copy-done
  16.0 0.0 copy-done.1
  16.0 0.0 copy-done.2
  16.0 1.8 %expert.1 = (bf16[288,128]{1,0:T(8,128)(2,1)S(1)}, bf16[288,128]{1,0:T(8,128)(2,1)S(1)}, bf16[288,128]{1,0:T(8,128)(2,1)S(1)}, bf16[288,128]{1,0:T(8,128)(2,1)S(...) custom-call(bf16[288,128]{1,0:T(8,128)(2,1)S(1)} %collective-permute, ...), custom_call_target="tpu_custom_call" | custom-call | tf_op jit(solution)/shard_map/expert/pallas_call | solution.py:312
  17.9 0.2 collective-permute-start.8
  18.1 0.4 %collective-permute-start.10 = (bf16[288,128]{1,0:T(8,128)(2,1)S(1)}, bf16[288,128]{1,0:T(8,128)(2,1)S(1)}, u32[]{:S(2)}, u32[]{:S(2)}) collective-permute-start(bf16[288,128]{1,0:T(8,128)(2,1)S(1)} %get-tuple-element.37), channel_id=1, source_target_pairs={{0,1},{1,0},{2,3},{3,2},{4,5},{5,4},{6,7},{7,6},{8,9},{9,8},{10,11... | collective-permute-start | bytes 221192 | tf_op jit(solution)/shard_map/ppermute | solution.py:326
  18.5 0.1 collective-permute-start.12
  18.6 0.4 %collective-permute-start.14 = (bf16[288,128]{1,0:T(8,128)(2,1)S(1)}, bf16[288,128]{1,0:T(8,128)(2,1)S(1)}, u32[]{:S(2)}, u32[]{:S(2)}) collective-permute-start(bf16[288,128]{1,0:T(8,128)(2,1)S(1)} %get-tuple-element.41), channel_id=1, source_target_pairs={{0,1},{1,0},{2,3},{3,2},{4,5},{5,4},{6,7},{7,6},{8,9},{9,8},{10,11... | collective-permute-start | bytes 221192 | tf_op jit(solution)/shard_map/ppermute | solution.py:326
  19.0 0.2 collective-permute-done.8
  19.2 2.5 %collective-permute-start.9 = (bf16[288,128]{1,0:T(8,128)(2,1)S(1)}, bf16[288,128]{1,0:T(8,128)(2,1)S(1)}, u32[]{:S(2)}, u32[]{:S(2)}) collective-permute-start(bf16[288,128]{1,0:T(8,128)(2,1)S(1)} %add_convert_fusion.3), channel_id=1, source_target_pairs={{0,12},{1,15},{2,14},{3,13},{4,8},{5,11},{6,10},{7,9},{8,4},{9,7},... | collective-permute-start | bytes 221192 | tf_op jit(solution)/shard_map/ppermute | solution.py:263
  21.8 0.0 collective-permute-done.10
  21.8 0.1 collective-permute-start.11
  21.9 0.0 collective-permute-done.12
  21.9 2.0 %collective-permute-start.13 = (bf16[288,128]{1,0:T(8,128)(2,1)S(1)}, bf16[288,128]{1,0:T(8,128)(2,1)S(1)}, u32[]{:S(2)}, u32[]{:S(2)}) collective-permute-start(bf16[288,128]{1,0:T(8,128)(2,1)S(1)} %add_convert_fusion.1), channel_id=1, source_target_pairs={{0,4},{1,7},{2,6},{3,5},{4,0},{5,3},{6,2},{7,1},{8,12},{9,15},{10,... | collective-permute-start | bytes 221192 | tf_op jit(solution)/shard_map/ppermute | solution.py:263
  23.9 0.0 collective-permute-done.14
  23.9 0.7 %collective-permute-start.15 = (bf16[288,128]{1,0:T(8,128)(2,1)S(1)}, bf16[288,128]{1,0:T(8,128)(2,1)S(1)}, u32[]{:S(2)}, u32[]{:S(2)}) collective-permute-start(bf16[288,128]{1,0:T(8,128)(2,1)S(1)} %add_convert_fusion), channel_id=1, source_target_pairs={{0,0},{1,3},{2,2},{3,1},{4,4},{5,7},{6,6},{7,5},{8,8},{9,11},{10,1... | collective-permute-start | bytes 221192 | tf_op jit(solution)/shard_map/ppermute | solution.py:263
  24.6 1.7 %collective-permute-done.9.refs_0_ = bf16[288,128]{1,0:T(8,128)(2,1)S(1)} collective-permute-done((bf16[288,128]{1,0:T(8,128)(2,1)S(1)}, bf16[288,128]{1,0:T(8,128)(2,1)S(1)}, u32[]{:S(2)}, u32[]{:S(2)}) %collective-permute-start.9) | collective-permute-done | bytes 73760 | tf_op jit(solution)/shard_map/ppermute | solution.py:263
  26.2 1.1 %collective-permute-start.16 = (bf16[288,128]{1,0:T(8,128)(2,1)S(1)}, bf16[288,128]{1,0:T(8,128)(2,1)S(1)}, u32[]{:S(2)}, u32[]{:S(2)}) collective-permute-start(bf16[288,128]{1,0:T(8,128)(2,1)S(1)} %collective-permute-done.9.refs_0_), channel_id=1, source_target_pairs={{0,1},{1,0},{2,3},{3,2},{4,5},{5,4},{6,7},{7,6},{8,9},{9,8},{10,11... | collective-permute-start | bytes 221192 | tf_op jit(solution)/shard_map/ppermute | solution.py:264
  27.3 1.7 %collective-permute-done.11.refs_1_ = bf16[288,128]{1,0:T(8,128)(2,1)S(1)} collective-permute-done((bf16[288,128]{1,0:T(8,128)(2,1)S(1)}, bf16[288,128]{1,0:T(8,128)(2,1)S(1)}, u32[]{:S(2)}, u32[]{:S(2)}) %collective-permute-start.11) | collective-permute-done | bytes 73760 | tf_op jit(solution)/shard_map/ppermute | solution.py:263
  29.0 0.4 %collective-permute-start.17 = (bf16[288,128]{1,0:T(8,128)(2,1)S(1)}, bf16[288,128]{1,0:T(8,128)(2,1)S(1)}, u32[]{:S(2)}, u32[]{:S(2)}) collective-permute-start(bf16[288,128]{1,0:T(8,128)(2,1)S(1)} %collective-permute-done.11.refs_1_), channel_id=1, source_target_pairs={{0,1},{1,0},{2,3},{3,2},{4,5},{5,4},{6,7},{7,6},{8,9},{9,8},{10,11... | collective-permute-start | bytes 221192 | tf_op jit(solution)/shard_map/ppermute | solution.py:264
  29.4 0.0 collective-permute-done.13.refs_2_
  29.4 0.1 collective-permute-start.18
  29.6 0.0 collective-permute-done.15.refs_3_
  29.6 0.4 %collective-permute-start.19 = (bf16[288,128]{1,0:T(8,128)(2,1)S(1)}, bf16[288,128]{1,0:T(8,128)(2,1)S(1)}, u32[]{:S(2)}, u32[]{:S(2)}) collective-permute-start(bf16[288,128]{1,0:T(8,128)(2,1)S(1)} %collective-permute-done.15.refs_3_), channel_id=1, source_target_pairs={{0,1},{1,0},{2,3},{3,2},{4,5},{5,4},{6,7},{7,6},{8,9},{9,8},{10,11... | collective-permute-start | bytes 221192 | tf_op jit(solution)/shard_map/ppermute | solution.py:264
  29.9 0.0 collective-permute-done.16.refs_4_
  29.9 0.4 %collective-permute-done.17.refs_5_ = bf16[288,128]{1,0:T(8,128)(2,1)S(1)} collective-permute-done((bf16[288,128]{1,0:T(8,128)(2,1)S(1)}, bf16[288,128]{1,0:T(8,128)(2,1)S(1)}, u32[]{:S(2)}, u32[]{:S(2)}) %collective-permute-start.17) | collective-permute-done | bytes 73760 | tf_op jit(solution)/shard_map/ppermute | solution.py:264
  30.3 0.4 %collective-permute-done.18.refs_6_ = bf16[288,128]{1,0:T(8,128)(2,1)S(1)} collective-permute-done((bf16[288,128]{1,0:T(8,128)(2,1)S(1)}, bf16[288,128]{1,0:T(8,128)(2,1)S(1)}, u32[]{:S(2)}, u32[]{:S(2)}) %collective-permute-start.18) | collective-permute-done | bytes 73760 | tf_op jit(solution)/shard_map/ppermute | solution.py:264
  30.7 0.2 collective-permute-done.19.refs_7_
  30.8 1.2 %combine.1 = bf16[72,2048]{1,0:T(8,128)(2,1)} custom-call(bf16[288,128]{1,0:T(8,128)(2,1)S(1)} %collective-permute-done.9.refs_0_, bf16[288,128]{1,0:T(8,128)(2,1)S(1)} %collective-permute-done.11.refs_1_, bf16[288,128]{1,0:T(8,128)(2,1)S(1)} %collective-permute-done.13.refs_2_, bf16[288,128]{1,0:T(8,128)(2,1)S(1)} %collective-permute-done.15.refs_3_, ...), custom_call_target="tpu_custom_call" | custom-call | tf_op jit(solution)/shard_map/combine/pallas_call | solution.py:329
  (4 shorter events, 0.1 us)
Async XLA Ops:
  1.8 14.3 %copy-start = (bf16[1,2048,768]{2,1,0:T(8,128)(2,1)S(1)}, bf16[1,2048,768]{2,1,0:T(8,128)(2,1)}, u32[]{:S(2)}) copy-start(bf16[1,2048,768]{2,1,0:T(8,128)(2,1)} %refs_8_.1) | copy-start | bytes 9437188
  1.8 14.3 %copy-start.1 = (bf16[1,2048,768]{2,1,0:T(8,128)(2,1)S(1)}, bf16[1,2048,768]{2,1,0:T(8,128)(2,1)}, u32[]{:S(2)}) copy-start(bf16[1,2048,768]{2,1,0:T(8,128)(2,1)} %refs_9_.1) | copy-start | bytes 9437188
  1.8 14.3 %copy-start.2 = (bf16[1,768,2048]{2,1,0:T(8,128)(2,1)S(1)}, bf16[1,768,2048]{2,1,0:T(8,128)(2,1)}, u32[]{:S(2)}) copy-start(bf16[1,768,2048]{2,1,0:T(8,128)(2,1)} %refs_10_.1) | copy-start | bytes 9437188
  2.0 8.3 %collective-permute-start = (bf16[288,128]{1,0:T(8,128)(2,1)S(1)}, bf16[288,128]{1,0:T(8,128)(2,1)S(1)}, u32[]{:S(2)}, u32[]{:S(2)}) collective-permute-start(bf16[288,128]{1,0:T(8,128)(2,1)S(1)} %get-tuple-element.30), channel_id=1, source_target_pairs={{0,12},{1,15},{2,14},{3,13},{4,8},{5,11},{6,10},{7,9},{8,4},{9,7},... | collective-permute-start | bytes 221192 | tf_op jit(solution)/shard_map/ppermute | solution.py:263
  7.1 7.1 %collective-permute-start.1 = (bf16[288,128]{1,0:T(8,128)(2,1)S(1)}, bf16[288,128]{1,0:T(8,128)(2,1)S(1)}, u32[]{:S(2)}, u32[]{:S(2)}) collective-permute-start(bf16[288,128]{1,0:T(8,128)(2,1)S(1)} %get-tuple-element.31), channel_id=1, source_target_pairs={{0,8},{1,11},{2,10},{3,9},{4,12},{5,15},{6,14},{7,13},{8,0},{9,3},... | collective-permute-start | bytes 221192 | tf_op jit(solution)/shard_map/ppermute | solution.py:263
  7.1 7.1 %collective-permute-start.2 = (bf16[288,128]{1,0:T(8,128)(2,1)S(1)}, bf16[288,128]{1,0:T(8,128)(2,1)S(1)}, u32[]{:S(2)}, u32[]{:S(2)}) collective-permute-start(bf16[288,128]{1,0:T(8,128)(2,1)S(1)} %get-tuple-element.32), channel_id=1, source_target_pairs={{0,4},{1,7},{2,6},{3,5},{4,0},{5,3},{6,2},{7,1},{8,12},{9,15},{10,... | collective-permute-start | bytes 221192 | tf_op jit(solution)/shard_map/ppermute | solution.py:263
  7.8 7.0 %collective-permute-start.3 = (bf16[288,128]{1,0:T(8,128)(2,1)S(1)}, bf16[288,128]{1,0:T(8,128)(2,1)S(1)}, u32[]{:S(2)}, u32[]{:S(2)}) collective-permute-start(bf16[288,128]{1,0:T(8,128)(2,1)S(1)} %get-tuple-element.33), channel_id=1, source_target_pairs={{0,0},{1,3},{2,2},{3,1},{4,4},{5,7},{6,6},{7,5},{8,8},{9,11},{10,1... | collective-permute-start | bytes 221192 | tf_op jit(solution)/shard_map/ppermute | solution.py:263
  10.3 4.5 %collective-permute-start.4 = (bf16[288,128]{1,0:T(8,128)(2,1)S(1)}, bf16[288,128]{1,0:T(8,128)(2,1)S(1)}, u32[]{:S(2)}, u32[]{:S(2)}) collective-permute-start(bf16[288,128]{1,0:T(8,128)(2,1)S(1)} %collective-permute-done.refs_0_), channel_id=1, source_target_pairs={{0,1},{1,0},{2,3},{3,2},{4,5},{5,4},{6,7},{7,6},{8,9},{9,8},{10,11... | collective-permute-start | bytes 221192 | tf_op jit(solution)/shard_map/ppermute | solution.py:264
  14.3 1.3 %collective-permute-start.5 = (bf16[288,128]{1,0:T(8,128)(2,1)S(1)}, bf16[288,128]{1,0:T(8,128)(2,1)S(1)}, u32[]{:S(2)}, u32[]{:S(2)}) collective-permute-start(bf16[288,128]{1,0:T(8,128)(2,1)S(1)} %collective-permute-done.1.refs_1_), channel_id=1, source_target_pairs={{0,1},{1,0},{2,3},{3,2},{4,5},{5,4},{6,7},{7,6},{8,9},{9,8},{10,11... | collective-permute-start | bytes 221192 | tf_op jit(solution)/shard_map/ppermute | solution.py:264
  14.3 1.4 %collective-permute-start.6 = (bf16[288,128]{1,0:T(8,128)(2,1)S(1)}, bf16[288,128]{1,0:T(8,128)(2,1)S(1)}, u32[]{:S(2)}, u32[]{:S(2)}) collective-permute-start(bf16[288,128]{1,0:T(8,128)(2,1)S(1)} %collective-permute-done.2.refs_2_), channel_id=1, source_target_pairs={{0,1},{1,0},{2,3},{3,2},{4,5},{5,4},{6,7},{7,6},{8,9},{9,8},{10,11... | collective-permute-start | bytes 221192 | tf_op jit(solution)/shard_map/ppermute | solution.py:264
  14.8 1.3 %collective-permute-start.7 = (bf16[288,128]{1,0:T(8,128)(2,1)S(1)}, bf16[288,128]{1,0:T(8,128)(2,1)S(1)}, u32[]{:S(2)}, u32[]{:S(2)}) collective-permute-start(bf16[288,128]{1,0:T(8,128)(2,1)S(1)} %collective-permute-done.3.refs_3_), channel_id=1, source_target_pairs={{0,1},{1,0},{2,3},{3,2},{4,5},{5,4},{6,7},{7,6},{8,9},{9,8},{10,11... | collective-permute-start | bytes 221192 | tf_op jit(solution)/shard_map/ppermute | solution.py:264
  17.9 1.3 %collective-permute-start.8 = (bf16[288,128]{1,0:T(8,128)(2,1)S(1)}, bf16[288,128]{1,0:T(8,128)(2,1)S(1)}, u32[]{:S(2)}, u32[]{:S(2)}) collective-permute-start(bf16[288,128]{1,0:T(8,128)(2,1)S(1)} %get-tuple-element.35), channel_id=1, source_target_pairs={{0,1},{1,0},{2,3},{3,2},{4,5},{5,4},{6,7},{7,6},{8,9},{9,8},{10,11... | collective-permute-start | bytes 221192 | tf_op jit(solution)/shard_map/ppermute | solution.py:326
  18.1 3.7 %collective-permute-start.10 = (bf16[288,128]{1,0:T(8,128)(2,1)S(1)}, bf16[288,128]{1,0:T(8,128)(2,1)S(1)}, u32[]{:S(2)}, u32[]{:S(2)}) collective-permute-start(bf16[288,128]{1,0:T(8,128)(2,1)S(1)} %get-tuple-element.37), channel_id=1, source_target_pairs={{0,1},{1,0},{2,3},{3,2},{4,5},{5,4},{6,7},{7,6},{8,9},{9,8},{10,11... | collective-permute-start | bytes 221192 | tf_op jit(solution)/shard_map/ppermute | solution.py:326
  18.5 3.4 %collective-permute-start.12 = (bf16[288,128]{1,0:T(8,128)(2,1)S(1)}, bf16[288,128]{1,0:T(8,128)(2,1)S(1)}, u32[]{:S(2)}, u32[]{:S(2)}) collective-permute-start(bf16[288,128]{1,0:T(8,128)(2,1)S(1)} %get-tuple-element.39), channel_id=1, source_target_pairs={{0,1},{1,0},{2,3},{3,2},{4,5},{5,4},{6,7},{7,6},{8,9},{9,8},{10,11... | collective-permute-start | bytes 221192 | tf_op jit(solution)/shard_map/ppermute | solution.py:326
  18.6 5.3 %collective-permute-start.14 = (bf16[288,128]{1,0:T(8,128)(2,1)S(1)}, bf16[288,128]{1,0:T(8,128)(2,1)S(1)}, u32[]{:S(2)}, u32[]{:S(2)}) collective-permute-start(bf16[288,128]{1,0:T(8,128)(2,1)S(1)} %get-tuple-element.41), channel_id=1, source_target_pairs={{0,1},{1,0},{2,3},{3,2},{4,5},{5,4},{6,7},{7,6},{8,9},{9,8},{10,11... | collective-permute-start | bytes 221192 | tf_op jit(solution)/shard_map/ppermute | solution.py:326
  19.2 7.0 %collective-permute-start.9 = (bf16[288,128]{1,0:T(8,128)(2,1)S(1)}, bf16[288,128]{1,0:T(8,128)(2,1)S(1)}, u32[]{:S(2)}, u32[]{:S(2)}) collective-permute-start(bf16[288,128]{1,0:T(8,128)(2,1)S(1)} %add_convert_fusion.3), channel_id=1, source_target_pairs={{0,12},{1,15},{2,14},{3,13},{4,8},{5,11},{6,10},{7,9},{8,4},{9,7},... | collective-permute-start | bytes 221192 | tf_op jit(solution)/shard_map/ppermute | solution.py:263
  21.8 7.2 %collective-permute-start.11 = (bf16[288,128]{1,0:T(8,128)(2,1)S(1)}, bf16[288,128]{1,0:T(8,128)(2,1)S(1)}, u32[]{:S(2)}, u32[]{:S(2)}) collective-permute-start(bf16[288,128]{1,0:T(8,128)(2,1)S(1)} %add_convert_fusion.2), channel_id=1, source_target_pairs={{0,8},{1,11},{2,10},{3,9},{4,12},{5,15},{6,14},{7,13},{8,0},{9,3},... | collective-permute-start | bytes 221192 | tf_op jit(solution)/shard_map/ppermute | solution.py:263
  21.9 7.5 %collective-permute-start.13 = (bf16[288,128]{1,0:T(8,128)(2,1)S(1)}, bf16[288,128]{1,0:T(8,128)(2,1)S(1)}, u32[]{:S(2)}, u32[]{:S(2)}) collective-permute-start(bf16[288,128]{1,0:T(8,128)(2,1)S(1)} %add_convert_fusion.1), channel_id=1, source_target_pairs={{0,4},{1,7},{2,6},{3,5},{4,0},{5,3},{6,2},{7,1},{8,12},{9,15},{10,... | collective-permute-start | bytes 221192 | tf_op jit(solution)/shard_map/ppermute | solution.py:263
  23.9 5.6 %collective-permute-start.15 = (bf16[288,128]{1,0:T(8,128)(2,1)S(1)}, bf16[288,128]{1,0:T(8,128)(2,1)S(1)}, u32[]{:S(2)}, u32[]{:S(2)}) collective-permute-start(bf16[288,128]{1,0:T(8,128)(2,1)S(1)} %add_convert_fusion), channel_id=1, source_target_pairs={{0,0},{1,3},{2,2},{3,1},{4,4},{5,7},{6,6},{7,5},{8,8},{9,11},{10,1... | collective-permute-start | bytes 221192 | tf_op jit(solution)/shard_map/ppermute | solution.py:263
  26.2 3.7 %collective-permute-start.16 = (bf16[288,128]{1,0:T(8,128)(2,1)S(1)}, bf16[288,128]{1,0:T(8,128)(2,1)S(1)}, u32[]{:S(2)}, u32[]{:S(2)}) collective-permute-start(bf16[288,128]{1,0:T(8,128)(2,1)S(1)} %collective-permute-done.9.refs_0_), channel_id=1, source_target_pairs={{0,1},{1,0},{2,3},{3,2},{4,5},{5,4},{6,7},{7,6},{8,9},{9,8},{10,11... | collective-permute-start | bytes 221192 | tf_op jit(solution)/shard_map/ppermute | solution.py:264
  29.0 1.3 %collective-permute-start.17 = (bf16[288,128]{1,0:T(8,128)(2,1)S(1)}, bf16[288,128]{1,0:T(8,128)(2,1)S(1)}, u32[]{:S(2)}, u32[]{:S(2)}) collective-permute-start(bf16[288,128]{1,0:T(8,128)(2,1)S(1)} %collective-permute-done.11.refs_1_), channel_id=1, source_target_pairs={{0,1},{1,0},{2,3},{3,2},{4,5},{5,4},{6,7},{7,6},{8,9},{9,8},{10,11... | collective-permute-start | bytes 221192 | tf_op jit(solution)/shard_map/ppermute | solution.py:264
  29.4 1.3 %collective-permute-start.18 = (bf16[288,128]{1,0:T(8,128)(2,1)S(1)}, bf16[288,128]{1,0:T(8,128)(2,1)S(1)}, u32[]{:S(2)}, u32[]{:S(2)}) collective-permute-start(bf16[288,128]{1,0:T(8,128)(2,1)S(1)} %collective-permute-done.13.refs_2_), channel_id=1, source_target_pairs={{0,1},{1,0},{2,3},{3,2},{4,5},{5,4},{6,7},{7,6},{8,9},{9,8},{10,11... | collective-permute-start | bytes 221192 | tf_op jit(solution)/shard_map/ppermute | solution.py:264
  29.6 1.3 %collective-permute-start.19 = (bf16[288,128]{1,0:T(8,128)(2,1)S(1)}, bf16[288,128]{1,0:T(8,128)(2,1)S(1)}, u32[]{:S(2)}, u32[]{:S(2)}) collective-permute-start(bf16[288,128]{1,0:T(8,128)(2,1)S(1)} %collective-permute-done.15.refs_3_), channel_id=1, source_target_pairs={{0,1},{1,0},{2,3},{3,2},{4,5},{5,4},{6,7},{7,6},{8,9},{9,8},{10,11... | collective-permute-start | bytes 221192 | tf_op jit(solution)/shard_map/ppermute | solution.py:264

commit v4 on v3

--- a/solution.py
+++ b/solution.py
@@ -7,9 +7,11 @@
 from jax.experimental.pallas import tpu as pltpu
 from jax.sharding import PartitionSpec as P
 
+
 LANES = 128
 SUB = 8
 COPIES = 3
+TOGETHER = 1
 COVER_FLOPS = 4_000_000_000
 VMEM_LIMIT = 32 * 1024 * 1024
 F32 = jnp.float32
@@ -23,8 +25,12 @@
     return (a + b - 1) // b
 
 
+def turn(core, m):
+    return 1 - core if m == 0 else core
+
+
 def partner(core, m, count):
-    return lax.axis_index("ep") ^ (2 * (count - 1 - m) + core)
+    return lax.axis_index("ep") ^ (2 * (count - 1 - m) + turn(core, m))
 
 
 def pick(values, wanted):
@@ -120,8 +126,12 @@
 def expert_kernel(*refs, count, slots):
     mine, other = refs[:count], refs[count : 2 * count]
     gate_ref, up_ref, down_ref = refs[2 * count : 2 * count + 3]
-    send, keep = refs[2 * count + 3 : 3 * count + 3], refs[3 * count + 3 : 4 * count + 3]
-    x_scr, hidden_scr, tail_scr, back_scr = refs[4 * count + 3 :]
+    sends = count // TOGETHER
+    rest = refs[2 * count + 3 :]
+    rows = slots * gate_ref.shape[1] // LANES
+    send = [rest[m // TOGETHER].at[pl.ds(m % TOGETHER * rows, rows)] for m in range(count)]
+    keep = rest[sends : sends + count]
+    x_scr, hidden_scr, tail_scr, back_scr = rest[sends + count :]
     _, width, hidden = gate_ref.shape
     n_main, n_tail = split_slots(slots)[1:]
     group = 2 * n_main
@@ -256,22 +266,25 @@
 
 def exchange(blocks, n_exp):
     count = len(blocks)
-    came = []
+    came, passed = [], []
     for m, block in enumerate(blocks):
         far = 2 * (count - 1 - m)
-        pairs = [(2 * e + c, 2 * (e ^ (far + c)) + c) for e in range(n_exp) for c in range(2)]
+        pairs = [(2 * e + c, 2 * (e ^ (far + turn(c, m))) + c) for e in range(n_exp) for c in range(2)]
         came.append(lax.ppermute(block, ("ep", "tp"), pairs))
-    return came + [lax.ppermute(block, "tp", SWAP) for block in came]
+    for block in came:
+        passed.append(lax.ppermute(block, "tp", SWAP))
+    return came + passed
 
 
 def local(tokens, norm_gain, chosen_rows, route_weights, gate_weight, up_weight, down_weight):
     tok_rows, width = tokens.shape
     n_exp, slots = chosen_rows.shape
-    half_slots, n_main, n_tail = split_slots(slots)
+    half_slots, _, n_tail = split_slots(slots)
     count = n_exp // 2
     hidden = gate_weight.shape[2]
     blocks = width // LANES
     block = jax.ShapeDtypeStruct((slots * blocks, LANES), BF16)
+    several = jax.ShapeDtypeStruct((TOGETHER * slots * blocks, LANES), BF16)
     padded = cdiv(count, SUB) * SUB
     args = (tokens, norm_gain.reshape(blocks, LANES), chosen_rows, route_weights)
     params = pltpu.CompilerParams(vmem_limit_bytes=VMEM_LIMIT)
@@ -306,14 +319,13 @@
         ),
         name="route",
     )(own_rows, own_weights)
-    *outgoing, left = lax.optimization_barrier((*outgoing, left))
     arrived = exchange(outgoing, n_exp)
     tails = n_exp * 2 * n_tail * blocks
     results = pl.pallas_call(
         functools.partial(expert_kernel, count=count, slots=slots),
-        out_shape=[block] * (2 * count),
+        out_shape=[several] * (count // TOGETHER) + [block] * count,
         in_specs=[VMEM] * (2 * count + 3),
-        out_specs=[VMEM] * (2 * count),
+        out_specs=[VMEM] * (count // TOGETHER + count),
         scratch_shapes=[
             pltpu.VMEM((n_exp * slots, width), BF16),
             pltpu.VMEM((n_exp * slots, hidden), BF16),
@@ -323,8 +335,11 @@
         compiler_params=params,
         name="expert",
     )(*arrived, gate_weight, up_weight, down_weight)
-    came = [lax.ppermute(part, "tp", SWAP) for part in results[:count]]
-    summed = [(a.astype(F32) + b.astype(F32)).astype(BF16) for a, b in zip(results[count:], came)]
+    came = []
+    for part in results[:-count]:
+        both = lax.ppermute(part, "tp", SWAP)
+        came += [both[k * block.shape[0] : (k + 1) * block.shape[0]] for k in range(TOGETHER)]
+    summed = [(a.astype(F32) + b.astype(F32)).astype(BF16) for a, b in zip(results[-count:], came)]
     back = exchange(summed, n_exp)
     return pl.pallas_call(
         functools.partial(combine_kernel, count=count, slots=slots),

time: 32.2 us -> 38.7 us (1.20)
  local copies, waits for them, and re-layouts: 0.02 us -> 5.67 us
  starting transfers between devices: 16.1 us -> 19.3 us
  waiting for transfers between devices: 10.7 us -> 8.35 us
    unnamed x6, local copies, waits for them, and re-layouts: 0.02 us -> 5.67 us
    ppermute x8, waiting for transfers between devices: 8.35 us -> 5.87 us  [exchange(): came.append(lax.ppermute(block, ('ep', 'tp'), pairs))]
    ppermute x12, starting transfers between devices: 4.46 us -> 6.08 us  [the longest x8 5 us: exchange(): passed.append(lax.ppermute(block, 'tp', SWAP))]
    ppermute x8, starting transfers between devices: 11.7 us -> 13.2 us  [exchange(): came.append(lax.ppermute(block, ('ep', 'tp'), pairs))]
  transfers between devices with their start and end apart: 20 -> 20, of which waited for: 11 -> 8; matrix products, arithmetic and copies ran while one was open for 0% -> 0% of each run, Pallas kernels for 0% -> 0%
where the time goes in v4:
time: 38.7 us; the launch traced here: 38.4 us
  starting transfers between devices  19.3 us (50%)
  waiting for transfers between devices  8.35 us (22%)
  local copies, waits for them, and re-layouts  5.67 us (15%)
  Pallas kernels  4.92 us (13%)
    ppermute x8, starting transfers between devices, exchange(): came.append(lax.ppermute(block, ('ep', 'tp'), pairs))  13.2 us
    ppermute x8, waiting for transfers between devices, exchange(): came.append(lax.ppermute(block, ('ep', 'tp'), pairs))  5.87 us
    unnamed x6, local copies, waits for them, and re-layouts  5.67 us
    ppermute x8, starting transfers between devices, exchange(): passed.append(lax.ppermute(block, 'tp', SWAP))  5 us
    ppermute x8, waiting for transfers between devices, exchange(): passed.append(lax.ppermute(block, 'tp', SWAP))  2.23 us
    pallas_call x1, Pallas kernels, local(): pl.pallas_call(functools.partial(expert_kernel, count=count, slots=slots)...  1.81 us
    pallas_call x1, Pallas kernels, local(): pl.pallas_call(functools.partial(dispatch_kernel, count=count), out_shape...  1.74 us
    pallas_call x1, Pallas kernels, local(): pl.pallas_call(functools.partial(combine_kernel, count=count, slots=slots...  1.18 us
  transfers between devices with their start and end apart: 20, of which 8 were waited for; matrix products, arithmetic and copies ran while one was open for 0% of the time, Pallas kernels for 0%

profile of v4, /device:TPU:0, one launch (start us, length us, event | category | flops | bytes accessed | tf_op | source)
XLA Modules:
  0.0 38.4 jit_solution(6259116530419020877)
XLA Ops:
  0.0 1.7 %dispatch.1 = (bf16[288,128]{1,0:T(8,128)(2,1)S(1)}, bf16[288,128]{1,0:T(8,128)(2,1)S(1)}, bf16[288,128]{1,0:T(8,128)(2,1)S(1)}, bf16[288,128]{1,0:T(8,128)(2,1)...) custom-call(bf16[144,2048]{1,0:T(8,128)(2,1)} %refs_0_.1, bf16[16,128]{1,0:T(8,128)(2,1)} %bitcast.1, s32[8,18]{1,0:T(8,128)} %refs_2_.1, ...), custom_call_target="tpu_custom_call" | custom-call | tf_op jit(solution)/shard_map/dispatch/pallas_call | solution.py:291
  1.8 6.1 %collective-permute-start = (bf16[288,128]{1,0:T(8,128)(2,1)S(1)}, bf16[288,128]{1,0:T(8,128)(2,1)S(1)}, u32[]{:S(2)}, u32[]{:S(2)}) collective-permute-start(bf16[288,128]{1,0:T(8,128)(2,1)S(1)} %get-tuple-element.19), channel_id=1, source_target_pairs={{0,14},{1,13},{2,12},{3,15},{4,10},{5,9},{6,8},{7,11},{8,6},{9,5},... | collective-permute-start | bytes 221192 | tf_op jit(solution)/shard_map/ppermute | solution.py:273
  7.8 0.0 collective-permute-start.1
  7.9 0.8 %collective-permute-start.2 = (bf16[288,128]{1,0:T(8,128)(2,1)S(1)}, bf16[288,128]{1,0:T(8,128)(2,1)S(1)}, u32[]{:S(2)}, u32[]{:S(2)}) collective-permute-start(bf16[288,128]{1,0:T(8,128)(2,1)S(1)} %get-tuple-element.21), channel_id=1, source_target_pairs={{0,4},{1,7},{2,6},{3,5},{4,0},{5,3},{6,2},{7,1},{8,12},{9,15},{10,... | collective-permute-start | bytes 221192 | tf_op jit(solution)/shard_map/ppermute | solution.py:273
  8.6 0.7 %collective-permute-start.3 = (bf16[288,128]{1,0:T(8,128)(2,1)S(1)}, bf16[288,128]{1,0:T(8,128)(2,1)S(1)}, u32[]{:S(2)}, u32[]{:S(2)}) collective-permute-start(bf16[288,128]{1,0:T(8,128)(2,1)S(1)} %get-tuple-element.22), channel_id=1, source_target_pairs={{0,0},{1,3},{2,2},{3,1},{4,4},{5,7},{6,6},{7,5},{8,8},{9,11},{10,1... | collective-permute-start | bytes 221192 | tf_op jit(solution)/shard_map/ppermute | solution.py:273
  9.3 1.3 %collective-permute-done.refs_0_ = bf16[288,128]{1,0:T(8,128)(2,1)S(1)} collective-permute-done((bf16[288,128]{1,0:T(8,128)(2,1)S(1)}, bf16[288,128]{1,0:T(8,128)(2,1)S(1)}, u32[]{:S(2)}, u32[]{:S(2)}) %collective-permute-start) | collective-permute-done | bytes 73760 | tf_op jit(solution)/shard_map/ppermute | solution.py:273
  10.6 0.4 collective-permute-start.4
  10.9 2.7 %collective-permute-done.1.refs_1_ = bf16[288,128]{1,0:T(8,128)(2,1)S(1)} collective-permute-done((bf16[288,128]{1,0:T(8,128)(2,1)S(1)}, bf16[288,128]{1,0:T(8,128)(2,1)S(1)}, u32[]{:S(2)}, u32[]{:S(2)}) %collective-permute-start.1) | collective-permute-done | bytes 73760 | tf_op jit(solution)/shard_map/ppermute | solution.py:273
  13.7 0.0 collective-permute-start.5
  13.7 0.0 collective-permute-done.2.refs_2_
  13.7 0.5 %collective-permute-start.6 = (bf16[288,128]{1,0:T(8,128)(2,1)S(1)}, bf16[288,128]{1,0:T(8,128)(2,1)S(1)}, u32[]{:S(2)}, u32[]{:S(2)}) collective-permute-start(bf16[288,128]{1,0:T(8,128)(2,1)S(1)} %collective-permute-done.2.refs_2_), channel_id=1, source_target_pairs={{0,1},{1,0},{2,3},{3,2},{4,5},{5,4},{6,7},{7,6},{8,9},{9,8},{10,11... | collective-permute-start | bytes 221192 | tf_op jit(solution)/shard_map/ppermute | solution.py:275
  14.2 0.0 collective-permute-done.3.refs_3_
  14.2 0.1 collective-permute-start.7
  14.3 0.0 collective-permute-done.4.refs_4_
  14.3 0.7 %collective-permute-done.5.refs_5_ = bf16[288,128]{1,0:T(8,128)(2,1)S(1)} collective-permute-done((bf16[288,128]{1,0:T(8,128)(2,1)S(1)}, bf16[288,128]{1,0:T(8,128)(2,1)S(1)}, u32[]{:S(2)}, u32[]{:S(2)}) %collective-permute-start.5) | collective-permute-done | bytes 73760 | tf_op jit(solution)/shard_map/ppermute | solution.py:275
  14.9 0.2 collective-permute-done.6.refs_6_
  15.1 0.4 collective-permute-done.7.refs_7_
  15.5 0.0 copy-start
  15.5 1.9 %copy-done = bf16[1,2048,768]{2,1,0:T(8,128)(2,1)S(1)} copy-done((bf16[1,2048,768]{2,1,0:T(8,128)(2,1)S(1)}, bf16[1,2048,768]{2,1,0:T(8,128)(2,1)}, u32[]{:S(2)}) %copy-start) | copy-done | bytes 3145752
  17.3 0.0 copy-start.1
  17.3 1.9 %copy-done.1 = bf16[1,2048,768]{2,1,0:T(8,128)(2,1)S(1)} copy-done((bf16[1,2048,768]{2,1,0:T(8,128)(2,1)S(1)}, bf16[1,2048,768]{2,1,0:T(8,128)(2,1)}, u32[]{:S(2)}) %copy-start.1) | copy-done | bytes 3145752
  19.2 0.0 copy-start.2
  19.2 1.9 %copy-done.2 = bf16[1,768,2048]{2,1,0:T(8,128)(2,1)S(1)} copy-done((bf16[1,768,2048]{2,1,0:T(8,128)(2,1)S(1)}, bf16[1,768,2048]{2,1,0:T(8,128)(2,1)}, u32[]{:S(2)}) %copy-start.2) | copy-done | bytes 3145752
  21.1 1.8 %expert.1 = (bf16[288,128]{1,0:T(8,128)(2,1)S(1)}, bf16[288,128]{1,0:T(8,128)(2,1)S(1)}, bf16[288,128]{1,0:T(8,128)(2,1)S(1)}, bf16[288,128]{1,0:T(8,128)(2,1)S(...) custom-call(bf16[288,128]{1,0:T(8,128)(2,1)S(1)} %collective-permute, ...), custom_call_target="tpu_custom_call" | custom-call | tf_op jit(solution)/shard_map/expert/pallas_call | solution.py:324
  22.9 0.2 collective-permute-start.14
  23.2 0.4 collective-permute-start.12
  23.5 0.1 collective-permute-start.10
  23.7 0.4 collective-permute-start.8
  24.0 0.2 collective-permute-done.14
  24.3 0.7 %collective-permute-start.15 = (bf16[288,128]{1,0:T(8,128)(2,1)S(1)}, bf16[288,128]{1,0:T(8,128)(2,1)S(1)}, u32[]{:S(2)}, u32[]{:S(2)}) collective-permute-start(bf16[288,128]{1,0:T(8,128)(2,1)S(1)} %add_convert_fusion), channel_id=1, source_target_pairs={{0,0},{1,3},{2,2},{3,1},{4,4},{5,7},{6,6},{7,5},{8,8},{9,11},{10,1... | collective-permute-start | bytes 221192 | tf_op jit(solution)/shard_map/ppermute | solution.py:273
  25.0 0.0 collective-permute-done.12
  25.0 0.3 collective-permute-start.13
  25.3 0.0 collective-permute-done.10
  25.4 3.4 %collective-permute-start.11 = (bf16[288,128]{1,0:T(8,128)(2,1)S(1)}, bf16[288,128]{1,0:T(8,128)(2,1)S(1)}, u32[]{:S(2)}, u32[]{:S(2)}) collective-permute-start(bf16[288,128]{1,0:T(8,128)(2,1)S(1)} %add_convert_fusion.2), channel_id=1, source_target_pairs={{0,8},{1,11},{2,10},{3,9},{4,12},{5,15},{6,14},{7,13},{8,0},{9,3},... | collective-permute-start | bytes 221192 | tf_op jit(solution)/shard_map/ppermute | solution.py:273
  28.7 0.0 collective-permute-done.8
  28.8 1.3 %collective-permute-start.9 = (bf16[288,128]{1,0:T(8,128)(2,1)S(1)}, bf16[288,128]{1,0:T(8,128)(2,1)S(1)}, u32[]{:S(2)}, u32[]{:S(2)}) collective-permute-start(bf16[288,128]{1,0:T(8,128)(2,1)S(1)} %add_convert_fusion.3), channel_id=1, source_target_pairs={{0,14},{1,13},{2,12},{3,15},{4,10},{5,9},{6,8},{7,11},{8,6},{9,5},... | collective-permute-start | bytes 221192 | tf_op jit(solution)/shard_map/ppermute | solution.py:273
  30.1 0.0 collective-permute-done.15.refs_3_
  30.1 1.7 %collective-permute-start.19 = (bf16[288,128]{1,0:T(8,128)(2,1)S(1)}, bf16[288,128]{1,0:T(8,128)(2,1)S(1)}, u32[]{:S(2)}, u32[]{:S(2)}) collective-permute-start(bf16[288,128]{1,0:T(8,128)(2,1)S(1)} %collective-permute-done.15.refs_3_), channel_id=1, source_target_pairs={{0,1},{1,0},{2,3},{3,2},{4,5},{5,4},{6,7},{7,6},{8,9},{9,8},{10,11... | collective-permute-start | bytes 221192 | tf_op jit(solution)/shard_map/ppermute | solution.py:275
  31.8 0.0 collective-permute-done.13.refs_2_
  31.8 0.2 collective-permute-start.18
  32.1 0.0 collective-permute-done.11.refs_1_
  32.1 2.1 %collective-permute-start.17 = (bf16[288,128]{1,0:T(8,128)(2,1)S(1)}, bf16[288,128]{1,0:T(8,128)(2,1)S(1)}, u32[]{:S(2)}, u32[]{:S(2)}) collective-permute-start(bf16[288,128]{1,0:T(8,128)(2,1)S(1)} %collective-permute-done.11.refs_1_), channel_id=1, source_target_pairs={{0,1},{1,0},{2,3},{3,2},{4,5},{5,4},{6,7},{7,6},{8,9},{9,8},{10,11... | collective-permute-start | bytes 221192 | tf_op jit(solution)/shard_map/ppermute | solution.py:275
  34.1 1.8 %collective-permute-done.9.refs_0_ = bf16[288,128]{1,0:T(8,128)(2,1)S(1)} collective-permute-done((bf16[288,128]{1,0:T(8,128)(2,1)S(1)}, bf16[288,128]{1,0:T(8,128)(2,1)S(1)}, u32[]{:S(2)}, u32[]{:S(2)}) %collective-permute-start.9) | collective-permute-done | bytes 73760 | tf_op jit(solution)/shard_map/ppermute | solution.py:273
  36.0 0.0 collective-permute-start.16
  36.0 0.2 route.1.refs_8_
  36.2 0.0 collective-permute-done.19.refs_7_
  36.2 0.0 collective-permute-done.18.refs_6_
  36.2 0.0 collective-permute-done.17.refs_5_
  36.2 1.0 %collective-permute-done.16.refs_4_ = bf16[288,128]{1,0:T(8,128)(2,1)S(1)} collective-permute-done((bf16[288,128]{1,0:T(8,128)(2,1)S(1)}, bf16[288,128]{1,0:T(8,128)(2,1)S(1)}, u32[]{:S(2)}, u32[]{:S(2)}) %collective-permute-start.16) | collective-permute-done | bytes 73760 | tf_op jit(solution)/shard_map/ppermute | solution.py:275
  37.2 1.2 %combine.1 = bf16[72,2048]{1,0:T(8,128)(2,1)} custom-call(bf16[288,128]{1,0:T(8,128)(2,1)S(1)} %collective-permute-done.9.refs_0_, bf16[288,128]{1,0:T(8,128)(2,1)S(1)} %collective-permute-done.11.refs_1_, bf16[288,128]{1,0:T(8,128)(2,1)S(1)} %collective-permute-done.13.refs_2_, bf16[288,128]{1,0:T(8,128)(2,1)S(1)} %collective-permute-done.15.refs_3_, ...), custom_call_target="tpu_custom_call" | custom-call | tf_op jit(solution)/shard_map/combine/pallas_call | solution.py:344
  (4 shorter events, 0.1 us)
Async XLA Ops:
  1.8 8.8 %collective-permute-start = (bf16[288,128]{1,0:T(8,128)(2,1)S(1)}, bf16[288,128]{1,0:T(8,128)(2,1)S(1)}, u32[]{:S(2)}, u32[]{:S(2)}) collective-permute-start(bf16[288,128]{1,0:T(8,128)(2,1)S(1)} %get-tuple-element.19), channel_id=1, source_target_pairs={{0,14},{1,13},{2,12},{3,15},{4,10},{5,9},{6,8},{7,11},{8,6},{9,5},... | collective-permute-start | bytes 221192 | tf_op jit(solution)/shard_map/ppermute | solution.py:273
  7.8 5.8 %collective-permute-start.1 = (bf16[288,128]{1,0:T(8,128)(2,1)S(1)}, bf16[288,128]{1,0:T(8,128)(2,1)S(1)}, u32[]{:S(2)}, u32[]{:S(2)}) collective-permute-start(bf16[288,128]{1,0:T(8,128)(2,1)S(1)} %get-tuple-element.20), channel_id=1, source_target_pairs={{0,8},{1,11},{2,10},{3,9},{4,12},{5,15},{6,14},{7,13},{8,0},{9,3},... | collective-permute-start | bytes 221192 | tf_op jit(solution)/shard_map/ppermute | solution.py:273
  7.9 5.8 %collective-permute-start.2 = (bf16[288,128]{1,0:T(8,128)(2,1)S(1)}, bf16[288,128]{1,0:T(8,128)(2,1)S(1)}, u32[]{:S(2)}, u32[]{:S(2)}) collective-permute-start(bf16[288,128]{1,0:T(8,128)(2,1)S(1)} %get-tuple-element.21), channel_id=1, source_target_pairs={{0,4},{1,7},{2,6},{3,5},{4,0},{5,3},{6,2},{7,1},{8,12},{9,15},{10,... | collective-permute-start | bytes 221192 | tf_op jit(solution)/shard_map/ppermute | solution.py:273
  8.6 5.5 %collective-permute-start.3 = (bf16[288,128]{1,0:T(8,128)(2,1)S(1)}, bf16[288,128]{1,0:T(8,128)(2,1)S(1)}, u32[]{:S(2)}, u32[]{:S(2)}) collective-permute-start(bf16[288,128]{1,0:T(8,128)(2,1)S(1)} %get-tuple-element.22), channel_id=1, source_target_pairs={{0,0},{1,3},{2,2},{3,1},{4,4},{5,7},{6,6},{7,5},{8,8},{9,11},{10,1... | collective-permute-start | bytes 221192 | tf_op jit(solution)/shard_map/ppermute | solution.py:273
  10.6 3.7 %collective-permute-start.4 = (bf16[288,128]{1,0:T(8,128)(2,1)S(1)}, bf16[288,128]{1,0:T(8,128)(2,1)S(1)}, u32[]{:S(2)}, u32[]{:S(2)}) collective-permute-start(bf16[288,128]{1,0:T(8,128)(2,1)S(1)} %collective-permute-done.refs_0_), channel_id=1, source_target_pairs={{0,1},{1,0},{2,3},{3,2},{4,5},{5,4},{6,7},{7,6},{8,9},{9,8},{10,11... | collective-permute-start | bytes 221192 | tf_op jit(solution)/shard_map/ppermute | solution.py:275
  13.7 1.3 %collective-permute-start.5 = (bf16[288,128]{1,0:T(8,128)(2,1)S(1)}, bf16[288,128]{1,0:T(8,128)(2,1)S(1)}, u32[]{:S(2)}, u32[]{:S(2)}) collective-permute-start(bf16[288,128]{1,0:T(8,128)(2,1)S(1)} %collective-permute-done.1.refs_1_), channel_id=1, source_target_pairs={{0,1},{1,0},{2,3},{3,2},{4,5},{5,4},{6,7},{7,6},{8,9},{9,8},{10,11... | collective-permute-start | bytes 221192 | tf_op jit(solution)/shard_map/ppermute | solution.py:275
  13.7 1.4 %collective-permute-start.6 = (bf16[288,128]{1,0:T(8,128)(2,1)S(1)}, bf16[288,128]{1,0:T(8,128)(2,1)S(1)}, u32[]{:S(2)}, u32[]{:S(2)}) collective-permute-start(bf16[288,128]{1,0:T(8,128)(2,1)S(1)} %collective-permute-done.2.refs_2_), channel_id=1, source_target_pairs={{0,1},{1,0},{2,3},{3,2},{4,5},{5,4},{6,7},{7,6},{8,9},{9,8},{10,11... | collective-permute-start | bytes 221192 | tf_op jit(solution)/shard_map/ppermute | solution.py:275
  14.2 1.3 %collective-permute-start.7 = (bf16[288,128]{1,0:T(8,128)(2,1)S(1)}, bf16[288,128]{1,0:T(8,128)(2,1)S(1)}, u32[]{:S(2)}, u32[]{:S(2)}) collective-permute-start(bf16[288,128]{1,0:T(8,128)(2,1)S(1)} %collective-permute-done.3.refs_3_), channel_id=1, source_target_pairs={{0,1},{1,0},{2,3},{3,2},{4,5},{5,4},{6,7},{7,6},{8,9},{9,8},{10,11... | collective-permute-start | bytes 221192 | tf_op jit(solution)/shard_map/ppermute | solution.py:275
  15.5 1.9 %copy-start = (bf16[1,2048,768]{2,1,0:T(8,128)(2,1)S(1)}, bf16[1,2048,768]{2,1,0:T(8,128)(2,1)}, u32[]{:S(2)}) copy-start(bf16[1,2048,768]{2,1,0:T(8,128)(2,1)} %refs_8_.1) | copy-start | bytes 9437188
  17.3 1.9 %copy-start.1 = (bf16[1,2048,768]{2,1,0:T(8,128)(2,1)S(1)}, bf16[1,2048,768]{2,1,0:T(8,128)(2,1)}, u32[]{:S(2)}) copy-start(bf16[1,2048,768]{2,1,0:T(8,128)(2,1)} %refs_9_.1) | copy-start | bytes 9437188
  19.2 1.9 %copy-start.2 = (bf16[1,768,2048]{2,1,0:T(8,128)(2,1)S(1)}, bf16[1,768,2048]{2,1,0:T(8,128)(2,1)}, u32[]{:S(2)}) copy-start(bf16[1,768,2048]{2,1,0:T(8,128)(2,1)} %refs_10_.1) | copy-start | bytes 9437188
  22.9 1.3 %collective-permute-start.14 = (bf16[288,128]{1,0:T(8,128)(2,1)S(1)}, bf16[288,128]{1,0:T(8,128)(2,1)S(1)}, u32[]{:S(2)}, u32[]{:S(2)}) collective-permute-start(bf16[288,128]{1,0:T(8,128)(2,1)S(1)} %get-tuple-element.30), channel_id=1, source_target_pairs={{0,1},{1,0},{2,3},{3,2},{4,5},{5,4},{6,7},{7,6},{8,9},{9,8},{10,11... | collective-permute-start | bytes 221192 | tf_op jit(solution)/shard_map/ppermute | solution.py:340
  23.2 1.8 %collective-permute-start.12 = (bf16[288,128]{1,0:T(8,128)(2,1)S(1)}, bf16[288,128]{1,0:T(8,128)(2,1)S(1)}, u32[]{:S(2)}, u32[]{:S(2)}) collective-permute-start(bf16[288,128]{1,0:T(8,128)(2,1)S(1)} %get-tuple-element.28), channel_id=1, source_target_pairs={{0,1},{1,0},{2,3},{3,2},{4,5},{5,4},{6,7},{7,6},{8,9},{9,8},{10,11... | collective-permute-start | bytes 221192 | tf_op jit(solution)/shard_map/ppermute | solution.py:340
  23.5 1.8 %collective-permute-start.10 = (bf16[288,128]{1,0:T(8,128)(2,1)S(1)}, bf16[288,128]{1,0:T(8,128)(2,1)S(1)}, u32[]{:S(2)}, u32[]{:S(2)}) collective-permute-start(bf16[288,128]{1,0:T(8,128)(2,1)S(1)} %get-tuple-element.26), channel_id=1, source_target_pairs={{0,1},{1,0},{2,3},{3,2},{4,5},{5,4},{6,7},{7,6},{8,9},{9,8},{10,11... | collective-permute-start | bytes 221192 | tf_op jit(solution)/shard_map/ppermute | solution.py:340
  23.7 5.1 %collective-permute-start.8 = (bf16[288,128]{1,0:T(8,128)(2,1)S(1)}, bf16[288,128]{1,0:T(8,128)(2,1)S(1)}, u32[]{:S(2)}, u32[]{:S(2)}) collective-permute-start(bf16[288,128]{1,0:T(8,128)(2,1)S(1)} %get-tuple-element.24), channel_id=1, source_target_pairs={{0,1},{1,0},{2,3},{3,2},{4,5},{5,4},{6,7},{7,6},{8,9},{9,8},{10,11... | collective-permute-start | bytes 221192 | tf_op jit(solution)/shard_map/ppermute | solution.py:340
  24.3 5.8 %collective-permute-start.15 = (bf16[288,128]{1,0:T(8,128)(2,1)S(1)}, bf16[288,128]{1,0:T(8,128)(2,1)S(1)}, u32[]{:S(2)}, u32[]{:S(2)}) collective-permute-start(bf16[288,128]{1,0:T(8,128)(2,1)S(1)} %add_convert_fusion), channel_id=1, source_target_pairs={{0,0},{1,3},{2,2},{3,1},{4,4},{5,7},{6,6},{7,5},{8,8},{9,11},{10,1... | collective-permute-start | bytes 221192 | tf_op jit(solution)/shard_map/ppermute | solution.py:273
  25.0 6.8 %collective-permute-start.13 = (bf16[288,128]{1,0:T(8,128)(2,1)S(1)}, bf16[288,128]{1,0:T(8,128)(2,1)S(1)}, u32[]{:S(2)}, u32[]{:S(2)}) collective-permute-start(bf16[288,128]{1,0:T(8,128)(2,1)S(1)} %add_convert_fusion.1), channel_id=1, source_target_pairs={{0,4},{1,7},{2,6},{3,5},{4,0},{5,3},{6,2},{7,1},{8,12},{9,15},{10,... | collective-permute-start | bytes 221192 | tf_op jit(solution)/shard_map/ppermute | solution.py:273
  25.4 6.7 %collective-permute-start.11 = (bf16[288,128]{1,0:T(8,128)(2,1)S(1)}, bf16[288,128]{1,0:T(8,128)(2,1)S(1)}, u32[]{:S(2)}, u32[]{:S(2)}) collective-permute-start(bf16[288,128]{1,0:T(8,128)(2,1)S(1)} %add_convert_fusion.2), channel_id=1, source_target_pairs={{0,8},{1,11},{2,10},{3,9},{4,12},{5,15},{6,14},{7,13},{8,0},{9,3},... | collective-permute-start | bytes 221192 | tf_op jit(solution)/shard_map/ppermute | solution.py:273
  28.8 7.2 %collective-permute-start.9 = (bf16[288,128]{1,0:T(8,128)(2,1)S(1)}, bf16[288,128]{1,0:T(8,128)(2,1)S(1)}, u32[]{:S(2)}, u32[]{:S(2)}) collective-permute-start(bf16[288,128]{1,0:T(8,128)(2,1)S(1)} %add_convert_fusion.3), channel_id=1, source_target_pairs={{0,14},{1,13},{2,12},{3,15},{4,10},{5,9},{6,8},{7,11},{8,6},{9,5},... | collective-permute-start | bytes 221192 | tf_op jit(solution)/shard_map/ppermute | solution.py:273
  30.1 6.1 %collective-permute-start.19 = (bf16[288,128]{1,0:T(8,128)(2,1)S(1)}, bf16[288,128]{1,0:T(8,128)(2,1)S(1)}, u32[]{:S(2)}, u32[]{:S(2)}) collective-permute-start(bf16[288,128]{1,0:T(8,128)(2,1)S(1)} %collective-permute-done.15.refs_3_), channel_id=1, source_target_pairs={{0,1},{1,0},{2,3},{3,2},{4,5},{5,4},{6,7},{7,6},{8,9},{9,8},{10,11... | collective-permute-start | bytes 221192 | tf_op jit(solution)/shard_map/ppermute | solution.py:275
  31.8 4.4 %collective-permute-start.18 = (bf16[288,128]{1,0:T(8,128)(2,1)S(1)}, bf16[288,128]{1,0:T(8,128)(2,1)S(1)}, u32[]{:S(2)}, u32[]{:S(2)}) collective-permute-start(bf16[288,128]{1,0:T(8,128)(2,1)S(1)} %collective-permute-done.13.refs_2_), channel_id=1, source_target_pairs={{0,1},{1,0},{2,3},{3,2},{4,5},{5,4},{6,7},{7,6},{8,9},{9,8},{10,11... | collective-permute-start | bytes 221192 | tf_op jit(solution)/shard_map/ppermute | solution.py:275
  32.1 4.1 %collective-permute-start.17 = (bf16[288,128]{1,0:T(8,128)(2,1)S(1)}, bf16[288,128]{1,0:T(8,128)(2,1)S(1)}, u32[]{:S(2)}, u32[]{:S(2)}) collective-permute-start(bf16[288,128]{1,0:T(8,128)(2,1)S(1)} %collective-permute-done.11.refs_1_), channel_id=1, source_target_pairs={{0,1},{1,0},{2,3},{3,2},{4,5},{5,4},{6,7},{7,6},{8,9},{9,8},{10,11... | collective-permute-start | bytes 221192 | tf_op jit(solution)/shard_map/ppermute | solution.py:275
  36.0 1.3 %collective-permute-start.16 = (bf16[288,128]{1,0:T(8,128)(2,1)S(1)}, bf16[288,128]{1,0:T(8,128)(2,1)S(1)}, u32[]{:S(2)}, u32[]{:S(2)}) collective-permute-start(bf16[288,128]{1,0:T(8,128)(2,1)S(1)} %collective-permute-done.9.refs_0_), channel_id=1, source_target_pairs={{0,1},{1,0},{2,3},{3,2},{4,5},{5,4},{6,7},{7,6},{8,9},{9,8},{10,11... | collective-permute-start | bytes 221192 | tf_op jit(solution)/shard_map/ppermute | solution.py:275

commit v5 on v3

v5 whole, which is shorter than its diff:
```python
import functools

import jax
import jax.numpy as jnp
from jax import lax
from jax.experimental import pallas as pl
from jax.experimental.pallas import tpu as pltpu
from jax.sharding import PartitionSpec as P


LANES = 128
SUB = 8
COPIES = 3
COVER_FLOPS = 4_000_000_000
VMEM_LIMIT = 32 * 1024 * 1024
F32 = jnp.float32
BF16 = jnp.bfloat16
SWAP = [(0, 1), (1, 0)]
VMEM = pl.BlockSpec(memory_space=pltpu.VMEM)
HBM = pl.BlockSpec(memory_space=pltpu.HBM)


def cdiv(a, b):
    return (a + b - 1) // b


def turn(core, m):
    return 1 - core if m == 0 else core


def partner(core, m, far):
    if m < far:
        return lax.axis_index("ep") ^ (2 * (far - m) + turn(core, m))
    return lax.axis_index("ep") ^ (far + 1 - m)


def pick(values, wanted):
    lane = lax.broadcasted_iota(jnp.int32, values.shape, 1)
    return jnp.sum(jnp.where(lane == wanted, values, 0.0), axis=1, keepdims=True)


def split_slots(slots):
    half_slots = slots // 2
    n_main = half_slots // SUB * SUB
    return half_slots, n_main, half_slots - n_main


def dispatch_kernel(*refs, far):
    count = far + 2
    tok_hbm, gain_hbm, rows_hbm, weight_hbm = refs[:4]
    outs = refs[4 : 4 + count]
    rows_ref, weight_ref, tok_ref, gain_ref, norm_scr, tail_scr, index_scr, sems = refs[4 + count :]
    tok_rows, width = tok_ref.shape
    slots = rows_ref.shape[1]
    step = 16
    cuts = [tok_rows * k // COPIES // step * step for k in range(COPIES)] + [tok_rows]
    copies = [
        pltpu.make_async_copy(gain_hbm, gain_ref, sems.at[COPIES]),
        pltpu.make_async_copy(rows_hbm, rows_ref, sems.at[COPIES + 1]),
        pltpu.make_async_copy(weight_hbm, weight_ref, sems.at[COPIES + 2]),
    ]
    parts = [
        pltpu.make_async_copy(tok_hbm.at[low:high], tok_ref.at[low:high], sems.at[k])
        for k, (low, high) in enumerate(zip(cuts, cuts[1:]))
    ]
    for copy in copies + parts:
        copy.start()
    for copy in copies:
        copy.wait()
    half_slots, n_main, n_tail = split_slots(slots)
    group = 2 * n_main
    blocks = width // LANES
    core = lax.axis_index("tp")
    index_scr[...] = jnp.zeros_like(index_scr)
    for m in range(count):
        index_scr[m : m + 1, :] = rows_ref[pl.ds(partner(core, m, far), 1), :]
    index = (index_scr[...] - lax.axis_index("ep") * tok_rows).astype(F32)
    sub = lax.broadcasted_iota(jnp.int32, (group, slots), 0)
    wanted = jnp.where(sub < n_main, sub, sub - n_main + half_slots)

    def one_hot(column):
        token = lax.broadcasted_iota(jnp.int32, (column.shape[0], tok_rows), 1)
        return jnp.where(token == column.astype(jnp.int32), 1.0, 0.0).astype(BF16)

    mains = [
        one_hot(pick(jnp.broadcast_to(index[m : m + 1, :], (group, slots)), wanted))
        for m in range(count)
    ]
    tails = [
        one_hot(pick(index, jnp.full(index.shape, h * half_slots + n_main + t, jnp.int32)))
        for h in range(2)
        for t in range(n_tail)
    ]
    gains = gain_ref[...].astype(F32)
    gain = jnp.concatenate([gains[j : j + 1, :] for j in range(blocks)], axis=1)
    for at in range(0, tok_rows, step):
        if at in cuts:
            parts[cuts.index(at)].wait()
        rows = slice(at, at + step)
        values = tok_ref[rows, :].astype(F32)
        scale = lax.rsqrt(jnp.mean(values * values, axis=-1, keepdims=True) + 1e-06)
        norm_scr[rows, :] = (values * scale * gain).astype(BF16)
    normed = norm_scr[...]
    together = 8
    for first in range(0, count, together):
        members = range(first, min(first + together, count))
        got = jnp.dot(
            jnp.concatenate([mains[m] for m in members], axis=0), normed, preferred_element_type=F32
        )
        for m in members:
            at = (m - first) * group
            for j in range(blocks):
                outs[m][j * group : (j + 1) * group, :] = got[
                    at : at + group, j * LANES : (j + 1) * LANES
                ].astype(BF16)
    got = jnp.dot(jnp.concatenate(tails, axis=0), normed, preferred_element_type=F32)
    padded = index.shape[0]
    per_block = 2 * n_tail * blocks
    for k in range(2 * n_tail):
        for j in range(blocks):
            tail_scr[pl.ds(k * blocks + j, padded, stride=per_block), :] = got[
                k * padded : (k + 1) * padded, j * LANES : (j + 1) * LANES
            ]
    for m in range(count):
        outs[m][group * blocks :, :] = tail_scr[m * per_block : (m + 1) * per_block, :].astype(BF16)


def expert_kernel(*refs, far, slots):
    mine, other, near = refs[:far], refs[far : 2 * far], refs[2 * far : 2 * far + 2]
    gate_ref, up_ref, down_ref = refs[2 * far + 2 : 2 * far + 5]
    rest = refs[2 * far + 5 :]
    send, keep = rest[: far + 1], rest[far + 1 : 2 * far + 2]
    x_scr, hidden_scr, tail_scr, back_scr = rest[2 * far + 2 :]
    _, width, hidden = gate_ref.shape
    n_main, n_tail = split_slots(slots)[1:]
    group = 2 * n_main
    blocks = width // LANES
    n_src = 2 * far + 2
    main_rows = n_src * group
    per_half = n_tail * blocks
    per_block = 2 * per_half
    core = lax.axis_index("tp")
    first = core == 0
    for side, base in ((mine, core * far), (other, (1 - core) * far), (near, 2 * far)):
        for m, ref in enumerate(side):
            rows = pl.ds(pl.multiple_of((base + m) * group, group), group)
            for j in range(blocks):
                x_scr[rows, j * LANES : (j + 1) * LANES] = ref[j * group : (j + 1) * group, :]
            rows = pl.ds(pl.multiple_of((base + m) * per_block, per_block), per_block)
            tail_scr[rows, :] = ref[group * blocks :, :].astype(F32)
    for j in range(blocks):
        last = [
            tail_scr[pl.ds(k * blocks + j, n_src, stride=per_block), :] for k in range(2 * n_tail)
        ]
        x_scr[main_rows:, j * LANES : (j + 1) * LANES] = jnp.concatenate(last, axis=0).astype(BF16)
    chunk = 2 * LANES
    x = x_scr[...]
    for at in range(0, hidden, chunk):
        cols = slice(at, at + chunk)
        gate = jnp.dot(x, gate_ref[0, :, cols], preferred_element_type=F32)
        up = jnp.dot(x, up_ref[0, :, cols], preferred_element_type=F32)
        hidden_scr[:, cols] = (gate / (1.0 + jnp.exp(-gate)) * up).astype(BF16)
    act = hidden_scr[...]

    def give(m, place, low, high):
        send[m][place, :] = jnp.where(first, high, low).astype(BF16)
        keep[m][place, :] = jnp.where(first, low, high).astype(BF16)

    half_rows = slots // 2 * blocks
    for at in range(0, width, chunk):
        part = jnp.dot(act, down_ref[0, :, at : at + chunk], preferred_element_type=F32)
        j = at // LANES
        for b in range(2):
            lanes = slice(b * LANES, (b + 1) * LANES)
            for m in range(far):
                low, high = (part[(s + m) * group : (s + m + 1) * group, lanes] for s in (0, far))
                give(m, slice((j + b) * group, (j + b + 1) * group), low, high)
            for k in range(2 * n_tail):
                row = main_rows + k * n_src
                back_scr[pl.ds(k * blocks + j + b, n_src, stride=per_block), :] = part[
                    row : row + n_src, lanes
                ]
        for q in range(2):
            row = (2 * far + q) * group
            low, high = (
                jnp.concatenate([part[r : r + n_main, :LANES], part[r : r + n_main, LANES:]], axis=0)
                for r in (row, row + n_main)
            )
            start = q * half_rows + j * n_main
            give(far, slice(start, start + group), low, high)
    for m in range(far):
        low, high = (back_scr[(s + m) * per_block : (s + m + 1) * per_block, :] for s in (0, far))
        give(m, slice(group * blocks, group * blocks + per_block), low, high)
    for q in range(2):
        row = (2 * far + q) * per_block
        low, high = (back_scr[r : r + per_half, :] for r in (row, row + per_half))
        start = q * half_rows + n_main * blocks
        give(far, slice(start, start + per_half), low, high)


def groups(far):
    last = (1, min(1, far - 1))
    blocks = [(side, m) for side in range(2) for m in range(far)] + [(0, far), (0, far + 1)]
    return [b for b in blocks if b != last], [last]


def depth(n_blocks, slots):
    _, n_main, n_tail = split_slots(slots)
    return n_blocks * n_main + n_tail * cdiv(n_blocks, SUB) * SUB


def route_kernel(rows_ref, weight_ref, *refs, far):
    slots = rows_ref.shape[1]
    half_slots, n_main, n_tail = split_slots(slots)
    lefts, (index_scr, weight_scr) = refs[:2], refs[2:]
    out_rows = lefts[0].shape[0] // 3
    core = lax.axis_index("tp")
    start = lax.axis_index("ep") * (2 * out_rows) + core * out_rows
    lane0 = core * half_slots
    wanted = lax.broadcasted_iota(jnp.int32, (n_main, slots), 0) + lane0

    def entry(idx, wgt):
        token = lax.broadcasted_iota(jnp.int32, (idx.shape[0], cdiv(out_rows, LANES) * LANES), 1)
        return jnp.where(token == idx.astype(jnp.int32), wgt, 0.0)

    for members, left_ref in zip(groups(far), lefts):
        padded = cdiv(len(members), SUB) * SUB
        index_scr[...] = jnp.zeros_like(index_scr)
        weight_scr[...] = jnp.zeros_like(weight_scr)
        for b, (side, m) in enumerate(members):
            row = pl.ds(partner(1 - core if side else core, m, far), 1)
            index_scr[b : b + 1, :] = rows_ref[row, :]
            weight_scr[b : b + 1, :] = weight_ref[row, :]
        index = (index_scr[:padded, :] - start).astype(F32)
        weight = weight_scr[:padded, :]
        pieces = []
        for b in range(len(members)):
            columns = [
                pick(jnp.broadcast_to(v[b : b + 1, :], (n_main, slots)), wanted)
                for v in (index, weight)
            ]
            pieces.append(entry(*columns))
        for t in range(n_tail):
            at = jnp.full((padded, slots), n_main + t, jnp.int32) + lane0
            pieces.append(entry(pick(index, at), pick(weight, at)))
        total = depth(len(members), slots)
        pieces.append(jnp.zeros((cdiv(total, LANES) * LANES - total, pieces[0].shape[1]), F32))
        pieces = [piece for piece in pieces if piece.shape[0]]
        spread = jnp.concatenate(pieces, axis=0).T[:out_rows, :]
        high = spread.astype(BF16)
        rest = spread - high.astype(F32)
        mid = rest.astype(BF16)
        low = (rest - mid.astype(F32)).astype(BF16)
        left_ref[...] = jnp.concatenate([high, mid, low], axis=0)[:, :total]


def combine_kernel(*refs, members, slots, width):
    count = len(members)
    full = slots * (width // LANES)
    sides, left_ref = refs[:count], refs[count]
    before, out_ref, row_scr, tail_scr = (None, *refs[count + 1 :])[-4:]
    out_rows = out_ref.shape[0]
    n_main, n_tail = split_slots(slots)[1:]
    blocks = width // LANES
    per_half = n_tail * blocks
    padded = cdiv(count, SUB) * SUB
    first = lax.axis_index("tp") == 0
    if padded > count:
        tail_scr[...] = jnp.zeros_like(tail_scr)
    for b, ref in enumerate(sides):
        rows = slice(b * n_main, (b + 1) * n_main)
        whole = ref.shape[0] == full
        for j in range(0, blocks, 2):
            if whole:
                pair = [
                    ref[k * 2 * n_main : (k + 1) * 2 * n_main, :].astype(F32) for k in (j, j + 1)
                ]
                pair = [jnp.where(first, two[:n_main], two[n_main:]) for two in pair]
            else:
                two = ref[j * n_main : (j + 2) * n_main, :].astype(F32)
                pair = [two[:n_main], two[n_main:]]
            for k in range(2):
                row_scr[rows, (j + k) * LANES : (j + k + 1) * LANES] = pair[k]
        if whole:
            two = ref[2 * n_main * blocks :, :].astype(F32)
            two = jnp.where(first, two[:per_half], two[per_half:])
        else:
            two = ref[n_main * blocks :, :].astype(F32)
        tail_scr[b * per_half : (b + 1) * per_half, :] = two
    for t in range(n_tail):
        rows = slice(count * n_main + t * padded, count * n_main + (t + 1) * padded)
        for j in range(blocks):
            row_scr[rows, j * LANES : (j + 1) * LANES] = tail_scr[
                pl.ds(t * blocks + j, padded, stride=per_half), :
            ]
    left = left_ref[...]
    chunk = 2 * LANES
    for at in range(0, width, chunk):
        cols = slice(at, at + chunk)
        got = jnp.dot(left, row_scr[:, cols].astype(BF16), preferred_element_type=F32)
        got = got[:out_rows] + (got[out_rows : 2 * out_rows] + got[2 * out_rows :])
        if before is not None:
            got = before[:, cols] + got
        out_ref[:, cols] = got.astype(out_ref.dtype)


def exchange(blocks, n_exp):
    far = len(blocks) - 1
    came, passed = [], []
    for m, block in enumerate(blocks):
        gap = [2 * (far - m) + turn(c, m) if m < far else 1 for c in range(2)]
        pairs = [(2 * e + c, 2 * (e ^ gap[c]) + c) for e in range(n_exp) for c in range(2)]
        came.append(lax.ppermute(block, ("ep", "tp"), pairs))
    for block in came[:far]:
        passed.append(lax.ppermute(block, "tp", SWAP))
    return came[:far], passed, came[far]


def local(tokens, norm_gain, chosen_rows, route_weights, gate_weight, up_weight, down_weight):
    tok_rows, width = tokens.shape
    n_exp, slots = chosen_rows.shape
    _, n_tail = split_slots(slots)[1:]
    far = n_exp // 2 - 1
    hidden = gate_weight.shape[2]
    blocks = width // LANES
    block = jax.ShapeDtypeStruct((slots * blocks, LANES), BF16)
    padded = cdiv(far + 2, SUB) * SUB
    args = (tokens, norm_gain.reshape(blocks, LANES), chosen_rows, route_weights)
    params = pltpu.CompilerParams(vmem_limit_bytes=VMEM_LIMIT)
    *outgoing, own, own_rows, own_weights = pl.pallas_call(
        functools.partial(dispatch_kernel, far=far),
        out_shape=[block] * (far + 2)
        + [jax.ShapeDtypeStruct(x.shape, x.dtype) for x in (chosen_rows, route_weights)],
        in_specs=[HBM] * 4,
        out_specs=[VMEM] * (far + 4),
        scratch_shapes=[
            pltpu.VMEM((tok_rows, width), BF16),
            pltpu.VMEM((blocks, LANES), BF16),
            pltpu.VMEM((tok_rows, width), BF16),
            pltpu.VMEM((padded * 2 * n_tail * blocks, LANES), F32),
            pltpu.VMEM((padded, slots), jnp.int32),
            pltpu.SemaphoreType.DMA((COPIES + 3,)),
        ],
        compiler_params=params,
        name="dispatch",
    )(*(pltpu.with_memory_space_constraint(x, pltpu.HBM) for x in args))
    out_rows = tok_rows // 2
    members = groups(far)
    depths = [depth(len(m), slots) for m in members]
    weight_bytes = 3 * 2 * width * hidden
    most = cdiv(len(members[0]), SUB) * SUB
    lefts = pl.pallas_call(
        functools.partial(route_kernel, far=far),
        out_shape=[jax.ShapeDtypeStruct((3 * out_rows, d), BF16) for d in depths],
        in_specs=[VMEM] * 2,
        out_specs=[VMEM] * 2,
        scratch_shapes=[pltpu.VMEM((most, slots), jnp.int32), pltpu.VMEM((most, slots), F32)],
        compiler_params=params,
        cost_estimate=pl.CostEstimate(
            flops=COVER_FLOPS, bytes_accessed=weight_bytes, transcendentals=0
        ),
        name="route",
    )(own_rows, own_weights)
    mine, other, near = exchange(outgoing, n_exp)
    tails = n_exp * 2 * n_tail * blocks
    results = pl.pallas_call(
        functools.partial(expert_kernel, far=far, slots=slots),
        out_shape=[block] * (2 * far + 2),
        in_specs=[VMEM] * (2 * far + 5),
        out_specs=[VMEM] * (2 * far + 2),
        scratch_shapes=[
            pltpu.VMEM((n_exp * slots, width), BF16),
            pltpu.VMEM((n_exp * slots, hidden), BF16),
            pltpu.VMEM((tails, LANES), F32),
            pltpu.VMEM((tails, LANES), F32),
        ],
        compiler_params=params,
        name="expert",
    )(*mine, *other, near, own, gate_weight, up_weight, down_weight)
    came = []
    for part in results[: far + 1]:
        came.append(lax.ppermute(part, "tp", SWAP))

    def add(a, b):
        return (a.astype(F32) + b.astype(F32)).astype(BF16)

    summed = [add(a, b) for a, b in zip(results[far + 1 : -1], came)]
    half = slots // 2 * blocks
    neighbour, own = (add(results[-1][rows], came[-1][rows]) for rows in (slice(0, half), slice(half, None)))
    mine, other, near = exchange(summed + [neighbour], n_exp)
    sides = ([*mine, near, own], other)
    total = None
    for k, (blocks_in, left) in enumerate(zip(members, lefts)):
        final = k == len(members) - 1
        ins = [sides[side][m] for side, m in blocks_in] + [left] + ([] if total is None else [total])
        total = pl.pallas_call(
            functools.partial(combine_kernel, members=blocks_in, slots=slots, width=width),
            out_shape=jax.ShapeDtypeStruct((out_rows, width), BF16 if final else F32),
            in_specs=[VMEM] * len(ins),
            out_specs=VMEM,
            scratch_shapes=[
                pltpu.VMEM((depths[k], width), F32),
                pltpu.VMEM((cdiv(len(blocks_in), SUB) * SUB * n_tail * blocks, LANES), F32),
            ],
            compiler_params=params,
        )(*ins)
    return total


def solution(mesh):
    return jax.shard_map(
        local,
        mesh=mesh,
        in_specs=(
            P(("grp", "ep"), None),
            P(),
            P("grp", "ep"),
            P("grp", "ep"),
            P("ep", None, "tp"),
            P("ep", None, "tp"),
            P("ep", "tp", None),
        ),
        out_specs=P(("grp", "ep", "tp"), None),
        check_vma=False,
    )
```

time: 32.2 us -> 37.7 us (1.17)
  local copies, waits for them, and re-layouts: 0.02 us -> 5.67 us
  starting transfers between devices: 16.1 us -> 14.2 us
  waiting for transfers between devices: 10.7 us -> 12.1 us
    unnamed x6, local copies, waits for them, and re-layouts: 0.02 us -> 5.67 us
    ppermute x12 -> x10, starting transfers between devices: 4.46 us -> 1.68 us  [the longest x4 1.09 us: local(): came.append(lax.ppermute(part, 'tp', SWAP))]
    ppermute x8, waiting for transfers between devices: 8.35 us -> 10.4 us  [exchange(): came.append(lax.ppermute(block, ('ep', 'tp'), pairs))]
    ppermute x8, starting transfers between devices: 11.7 us -> 12.5 us  [exchange(): came.append(lax.ppermute(block, ('ep', 'tp'), pairs))]
    ppermute x12 -> x10, waiting for transfers between devices: 2.36 us -> 1.69 us  [the longest x6 1.44 us: exchange(): passed.append(lax.ppermute(block, 'tp', SWAP))]
    pallas_call x4 -> x5, Pallas kernels: 4.94 us -> 5.26 us  [the longest x1 1.79 us: local(): pl.pallas_call(functools.partial(expert_kernel, far=far, slots=slots), ou...]
  transfers between devices with their start and end apart: 20 -> 18, of which waited for: 11 -> 8; matrix products, arithmetic and copies ran while one was open for 0% -> 0% of each run, Pallas kernels for 0% -> 2%
where the time goes in v5:
time: 37.7 us; the launch traced here: 37.4 us
  starting transfers between devices  14.2 us (38%)
  waiting for transfers between devices  12.1 us (32%)
  local copies, waits for them, and re-layouts  5.67 us (15%)
  Pallas kernels  5.26 us (14%)
    ppermute x8, starting transfers between devices, exchange(): came.append(lax.ppermute(block, ('ep', 'tp'), pairs))  12.5 us
    ppermute x8, waiting for transfers between devices, exchange(): came.append(lax.ppermute(block, ('ep', 'tp'), pairs))  10.4 us
    unnamed x6, local copies, waits for them, and re-layouts  5.67 us
    pallas_call x1, Pallas kernels, local(): pl.pallas_call(functools.partial(expert_kernel, far=far, slots=slots), ou...  1.79 us
    pallas_call x1, Pallas kernels, local(): pl.pallas_call(functools.partial(dispatch_kernel, far=far), out_shape=[bl...  1.76 us
    pallas_call x2, Pallas kernels, local(): pl.pallas_call(functools.partial(combine_kernel, members=blocks_in, slots...  1.51 us
    ppermute x6, waiting for transfers between devices, exchange(): passed.append(lax.ppermute(block, 'tp', SWAP))  1.44 us
    ppermute x4, starting transfers between devices, local(): came.append(lax.ppermute(part, 'tp', SWAP))  1.09 us
  transfers between devices with their start and end apart: 18, of which 8 were waited for; matrix products, arithmetic and copies ran while one was open for 0% of the time, Pallas kernels for 2%

profile of v5, /device:TPU:0, one launch (start us, length us, event | category | flops | bytes accessed | tf_op | source)
XLA Modules:
  0.0 37.4 jit_solution(6049587090535089651)
XLA Ops:
  0.0 1.8 %dispatch.1 = (bf16[288,128]{1,0:T(8,128)(2,1)S(1)}, bf16[288,128]{1,0:T(8,128)(2,1)S(1)}, bf16[288,128]{1,0:T(8,128)(2,1)S(1)}, bf16[288,128]{1,0:T(8,128)(2,1)...) custom-call(bf16[144,2048]{1,0:T(8,128)(2,1)} %refs_0_.1, bf16[16,128]{1,0:T(8,128)(2,1)} %bitcast.1, ...), custom_call_target="tpu_custom_call" | custom-call | tf_op jit(solution)/shard_map/dispatch/pallas_call | solution.py:330
  1.8 6.1 %collective-permute-start = (bf16[288,128]{1,0:T(8,128)(2,1)S(1)}, bf16[288,128]{1,0:T(8,128)(2,1)S(1)}, u32[]{:S(2)}, u32[]{:S(2)}) collective-permute-start(bf16[288,128]{1,0:T(8,128)(2,1)S(1)} %get-tuple-element.22), channel_id=1, source_target_pairs={{0,14},{1,13},{2,12},{3,15},{4,10},{5,9},{6,8},{7,11},{8,6},{9,5},... | collective-permute-start | bytes 221192 | tf_op jit(solution)/shard_map/ppermute | solution.py:313
  7.9 0.0 collective-permute-start.1
  7.9 0.8 %collective-permute-start.2 = (bf16[288,128]{1,0:T(8,128)(2,1)S(1)}, bf16[288,128]{1,0:T(8,128)(2,1)S(1)}, u32[]{:S(2)}, u32[]{:S(2)}) collective-permute-start(bf16[288,128]{1,0:T(8,128)(2,1)S(1)} %get-tuple-element.24), channel_id=1, source_target_pairs={{0,4},{1,7},{2,6},{3,5},{4,0},{5,3},{6,2},{7,1},{8,12},{9,15},{10,... | collective-permute-start | bytes 221192 | tf_op jit(solution)/shard_map/ppermute | solution.py:313
  8.7 0.4 %collective-permute-start.6 = (bf16[288,128]{1,0:T(8,128)(2,1)S(1)}, bf16[288,128]{1,0:T(8,128)(2,1)S(1)}, u32[]{:S(2)}, u32[]{:S(2)}) collective-permute-start(bf16[288,128]{1,0:T(8,128)(2,1)S(1)} %get-tuple-element.25), channel_id=1, source_target_pairs={{0,2},{1,3},{2,0},{3,1},{4,6},{5,7},{6,4},{7,5},{8,10},{9,11},{10,... | collective-permute-start | bytes 221192 | tf_op jit(solution)/shard_map/ppermute | solution.py:313
  9.1 1.5 %collective-permute-done.refs_0_ = bf16[288,128]{1,0:T(8,128)(2,1)S(1)} collective-permute-done((bf16[288,128]{1,0:T(8,128)(2,1)S(1)}, bf16[288,128]{1,0:T(8,128)(2,1)S(1)}, u32[]{:S(2)}, u32[]{:S(2)}) %collective-permute-start) | collective-permute-done | bytes 73760 | tf_op jit(solution)/shard_map/ppermute | solution.py:313
  10.6 0.0 collective-permute-start.3
  10.6 3.1 %collective-permute-done.1.refs_1_ = bf16[288,128]{1,0:T(8,128)(2,1)S(1)} collective-permute-done((bf16[288,128]{1,0:T(8,128)(2,1)S(1)}, bf16[288,128]{1,0:T(8,128)(2,1)S(1)}, u32[]{:S(2)}, u32[]{:S(2)}) %collective-permute-start.1) | collective-permute-done | bytes 73760 | tf_op jit(solution)/shard_map/ppermute | solution.py:313
  13.7 0.0 collective-permute-start.4
  13.7 0.0 collective-permute-done.2.refs_2_
  13.7 0.5 %collective-permute-start.5 = (bf16[288,128]{1,0:T(8,128)(2,1)S(1)}, bf16[288,128]{1,0:T(8,128)(2,1)S(1)}, u32[]{:S(2)}, u32[]{:S(2)}) collective-permute-start(bf16[288,128]{1,0:T(8,128)(2,1)S(1)} %collective-permute-done.2.refs_2_), channel_id=1, source_target_pairs={{0,1},{1,0},{2,3},{3,2},{4,5},{5,4},{6,7},{7,6},{8,9},{9,8},{10,11... | collective-permute-start | bytes 221192 | tf_op jit(solution)/shard_map/ppermute | solution.py:315
  14.2 0.0 collective-permute-done.6.refs_6_
  14.2 0.0 collective-permute-done.3.refs_3_
  14.2 0.7 %collective-permute-done.4.refs_4_ = bf16[288,128]{1,0:T(8,128)(2,1)S(1)} collective-permute-done((bf16[288,128]{1,0:T(8,128)(2,1)S(1)}, bf16[288,128]{1,0:T(8,128)(2,1)S(1)}, u32[]{:S(2)}, u32[]{:S(2)}) %collective-permute-start.4) | collective-permute-done | bytes 73760 | tf_op jit(solution)/shard_map/ppermute | solution.py:315
  14.9 0.2 collective-permute-done.5.refs_5_
  15.1 0.0 copy-start
  15.1 1.9 %copy-done = bf16[1,2048,768]{2,1,0:T(8,128)(2,1)S(1)} copy-done((bf16[1,2048,768]{2,1,0:T(8,128)(2,1)S(1)}, bf16[1,2048,768]{2,1,0:T(8,128)(2,1)}, u32[]{:S(2)}) %copy-start) | copy-done | bytes 3145752
  17.0 0.0 copy-start.1
  17.0 1.9 %copy-done.1 = bf16[1,2048,768]{2,1,0:T(8,128)(2,1)S(1)} copy-done((bf16[1,2048,768]{2,1,0:T(8,128)(2,1)S(1)}, bf16[1,2048,768]{2,1,0:T(8,128)(2,1)}, u32[]{:S(2)}) %copy-start.1) | copy-done | bytes 3145752
  18.9 0.0 copy-start.2
  18.9 1.9 %copy-done.2 = bf16[1,768,2048]{2,1,0:T(8,128)(2,1)S(1)} copy-done((bf16[1,768,2048]{2,1,0:T(8,128)(2,1)S(1)}, bf16[1,768,2048]{2,1,0:T(8,128)(2,1)}, u32[]{:S(2)}) %copy-start.2) | copy-done | bytes 3145752
  20.8 1.8 %expert.1 = (bf16[288,128]{1,0:T(8,128)(2,1)S(1)}, bf16[288,128]{1,0:T(8,128)(2,1)S(1)}, bf16[288,128]{1,0:T(8,128)(2,1)S(1)}, bf16[288,128]{1,0:T(8,128)(2,1)S(...) custom-call(bf16[288,128]{1,0:T(8,128)(2,1)S(1)} %collective-permute, ...), custom_call_target="tpu_custom_call" | custom-call | tf_op jit(solution)/shard_map/expert/pallas_call | solution.py:366
  22.6 0.4 %collective-permute-start.12 = (bf16[288,128]{1,0:T(8,128)(2,1)S(1)}, bf16[288,128]{1,0:T(8,128)(2,1)S(1)}, u32[]{:S(2)}, u32[]{:S(2)}) collective-permute-start(bf16[288,128]{1,0:T(8,128)(2,1)S(1)} %get-tuple-element.35), channel_id=1, source_target_pairs={{0,1},{1,0},{2,3},{3,2},{4,5},{5,4},{6,7},{7,6},{8,9},{9,8},{10,11... | collective-permute-start | bytes 221192 | tf_op jit(solution)/shard_map/ppermute | solution.py:382
  23.0 0.2 collective-permute-start.16
  23.1 0.3 collective-permute-start.10
  23.5 0.2 collective-permute-start.7
  23.7 0.2 collective-permute-done.12
  23.9 0.6 %collective-permute-start.13 = (bf16[288,128]{1,0:T(8,128)(2,1)S(1)}, bf16[288,128]{1,0:T(8,128)(2,1)S(1)}, u32[]{:S(2)}, u32[]{:S(2)}) collective-permute-start(bf16[288,128]{1,0:T(8,128)(2,1)S(1)} %add_convert_fusion), channel_id=1, source_target_pairs={{0,4},{1,7},{2,6},{3,5},{4,0},{5,3},{6,2},{7,1},{8,12},{9,15},{10,... | collective-permute-start | bytes 221192 | tf_op jit(solution)/shard_map/ppermute | solution.py:313
  24.5 0.0 collective-permute-done.10
  24.5 3.6 %collective-permute-start.11 = (bf16[288,128]{1,0:T(8,128)(2,1)S(1)}, bf16[288,128]{1,0:T(8,128)(2,1)S(1)}, u32[]{:S(2)}, u32[]{:S(2)}) collective-permute-start(bf16[288,128]{1,0:T(8,128)(2,1)S(1)} %add_convert_fusion.1), channel_id=1, source_target_pairs={{0,14},{1,13},{2,12},{3,15},{4,10},{5,9},{6,8},{7,11},{8,6},{9,5},... | collective-permute-start | bytes 221192 | tf_op jit(solution)/shard_map/ppermute | solution.py:313
  28.1 0.0 collective-permute-done.7
  28.1 0.1 collective-permute-start.8
  28.2 0.0 collective-permute-done.16
  28.2 1.0 %collective-permute-start.17 = (bf16[144,128]{1,0:T(8,128)(2,1)S(1)}, bf16[144,128]{1,0:T(8,128)(2,1)S(1)}, u32[]{:S(2)}, u32[]{:S(2)}) collective-permute-start(bf16[144,128]{1,0:T(8,128)(2,1)S(1)} %get-tuple-element.40), channel_id=1, source_target_pairs={{0,2},{1,3},{2,0},{3,1},{4,6},{5,7},{6,4},{7,5},{8,10},{9,11},{10,... | collective-permute-start | bytes 110600 | tf_op jit(solution)/shard_map/ppermute | solution.py:313
  29.2 0.0 collective-permute-done.13.refs_2_
  29.2 0.0 collective-permute-start.15
  29.2 2.9 %collective-permute-done.11.refs_0_ = bf16[288,128]{1,0:T(8,128)(2,1)S(1)} collective-permute-done((bf16[288,128]{1,0:T(8,128)(2,1)S(1)}, bf16[288,128]{1,0:T(8,128)(2,1)S(1)}, u32[]{:S(2)}, u32[]{:S(2)}) %collective-permute-start.11) | collective-permute-done | bytes 73760 | tf_op jit(solution)/shard_map/ppermute | solution.py:313
  32.1 0.0 collective-permute-start.14
  32.1 2.9 %collective-permute-done.8.refs_1_ = bf16[288,128]{1,0:T(8,128)(2,1)S(1)} collective-permute-done((bf16[288,128]{1,0:T(8,128)(2,1)S(1)}, bf16[288,128]{1,0:T(8,128)(2,1)S(1)}, u32[]{:S(2)}, u32[]{:S(2)}) %collective-permute-start.8) | collective-permute-done | bytes 73760 | tf_op jit(solution)/shard_map/ppermute | solution.py:313
  35.0 0.1 collective-permute-start.9
  35.1 0.2 route.1
  35.3 0.0 collective-permute-done.17.refs_5_
  35.3 0.0 collective-permute-done.15.refs_4_
  35.4 0.0 collective-permute-done.14.refs_3_
  35.4 0.4 %shard_map.73.refs_2_ = f32[72,2048]{1,0:T(8,128)S(1)} custom-call(bf16[288,128]{1,0:T(8,128)(2,1)S(1)} %collective-permute-done.11.refs_0_, bf16[288,128]{1,0:T(8,128)(2,1)S(1)} %collective-permute-done.8.refs_1_, bf16[288,128]{1,0:T(8,128)(2,1)S(1)} %collective-permute-done.13.refs_2_, bf16[288,128]{1,0:T(8,128)(2,1)S(1)} %collective-permute-done.14.refs_3_, ...), custom_call_target="tpu_custom_call" | custom-call | tf_op jit(solution)/shard_map/pallas_call | solution.py:396
  35.8 0.5 %collective-permute-done.9.refs_0_ = bf16[288,128]{1,0:T(8,128)(2,1)S(1)} collective-permute-done((bf16[288,128]{1,0:T(8,128)(2,1)S(1)}, bf16[288,128]{1,0:T(8,128)(2,1)S(1)}, u32[]{:S(2)}, u32[]{:S(2)}) %collective-permute-start.9) | collective-permute-done | bytes 73760 | tf_op jit(solution)/shard_map/ppermute | solution.py:315
  36.3 1.1 %shard_map.74 = bf16[72,2048]{1,0:T(8,128)(2,1)} custom-call(bf16[288,128]{1,0:T(8,128)(2,1)S(1)} %collective-permute-done.9.refs_0_, bf16[216,16]{1,0:T(8,128)(2,1)S(1)} %get-tuple-element.31.refs_1_, f32[72,2048]{1,0:T(8,128)S(1)} %shard_map.73.refs_2_), custom_call_target="tpu_custom_call" | custom-call | tf_op jit(solution)/shard_map/pallas_call | solution.py:396
  (4 shorter events, 0.1 us)
Async XLA Ops:
  1.8 8.8 %collective-permute-start = (bf16[288,128]{1,0:T(8,128)(2,1)S(1)}, bf16[288,128]{1,0:T(8,128)(2,1)S(1)}, u32[]{:S(2)}, u32[]{:S(2)}) collective-permute-start(bf16[288,128]{1,0:T(8,128)(2,1)S(1)} %get-tuple-element.22), channel_id=1, source_target_pairs={{0,14},{1,13},{2,12},{3,15},{4,10},{5,9},{6,8},{7,11},{8,6},{9,5},... | collective-permute-start | bytes 221192 | tf_op jit(solution)/shard_map/ppermute | solution.py:313
  7.9 5.8 %collective-permute-start.1 = (bf16[288,128]{1,0:T(8,128)(2,1)S(1)}, bf16[288,128]{1,0:T(8,128)(2,1)S(1)}, u32[]{:S(2)}, u32[]{:S(2)}) collective-permute-start(bf16[288,128]{1,0:T(8,128)(2,1)S(1)} %get-tuple-element.23), channel_id=1, source_target_pairs={{0,8},{1,11},{2,10},{3,9},{4,12},{5,15},{6,14},{7,13},{8,0},{9,3},... | collective-permute-start | bytes 221192 | tf_op jit(solution)/shard_map/ppermute | solution.py:313
  7.9 5.8 %collective-permute-start.2 = (bf16[288,128]{1,0:T(8,128)(2,1)S(1)}, bf16[288,128]{1,0:T(8,128)(2,1)S(1)}, u32[]{:S(2)}, u32[]{:S(2)}) collective-permute-start(bf16[288,128]{1,0:T(8,128)(2,1)S(1)} %get-tuple-element.24), channel_id=1, source_target_pairs={{0,4},{1,7},{2,6},{3,5},{4,0},{5,3},{6,2},{7,1},{8,12},{9,15},{10,... | collective-permute-start | bytes 221192 | tf_op jit(solution)/shard_map/ppermute | solution.py:313
  8.7 5.5 %collective-permute-start.6 = (bf16[288,128]{1,0:T(8,128)(2,1)S(1)}, bf16[288,128]{1,0:T(8,128)(2,1)S(1)}, u32[]{:S(2)}, u32[]{:S(2)}) collective-permute-start(bf16[288,128]{1,0:T(8,128)(2,1)S(1)} %get-tuple-element.25), channel_id=1, source_target_pairs={{0,2},{1,3},{2,0},{3,1},{4,6},{5,7},{6,4},{7,5},{8,10},{9,11},{10,... | collective-permute-start | bytes 221192 | tf_op jit(solution)/shard_map/ppermute | solution.py:313
  10.6 3.6 %collective-permute-start.3 = (bf16[288,128]{1,0:T(8,128)(2,1)S(1)}, bf16[288,128]{1,0:T(8,128)(2,1)S(1)}, u32[]{:S(2)}, u32[]{:S(2)}) collective-permute-start(bf16[288,128]{1,0:T(8,128)(2,1)S(1)} %collective-permute-done.refs_0_), channel_id=1, source_target_pairs={{0,1},{1,0},{2,3},{3,2},{4,5},{5,4},{6,7},{7,6},{8,9},{9,8},{10,11... | collective-permute-start | bytes 221192 | tf_op jit(solution)/shard_map/ppermute | solution.py:315
  13.7 1.3 %collective-permute-start.4 = (bf16[288,128]{1,0:T(8,128)(2,1)S(1)}, bf16[288,128]{1,0:T(8,128)(2,1)S(1)}, u32[]{:S(2)}, u32[]{:S(2)}) collective-permute-start(bf16[288,128]{1,0:T(8,128)(2,1)S(1)} %collective-permute-done.1.refs_1_), channel_id=1, source_target_pairs={{0,1},{1,0},{2,3},{3,2},{4,5},{5,4},{6,7},{7,6},{8,9},{9,8},{10,11... | collective-permute-start | bytes 221192 | tf_op jit(solution)/shard_map/ppermute | solution.py:315
  13.7 1.4 %collective-permute-start.5 = (bf16[288,128]{1,0:T(8,128)(2,1)S(1)}, bf16[288,128]{1,0:T(8,128)(2,1)S(1)}, u32[]{:S(2)}, u32[]{:S(2)}) collective-permute-start(bf16[288,128]{1,0:T(8,128)(2,1)S(1)} %collective-permute-done.2.refs_2_), channel_id=1, source_target_pairs={{0,1},{1,0},{2,3},{3,2},{4,5},{5,4},{6,7},{7,6},{8,9},{9,8},{10,11... | collective-permute-start | bytes 221192 | tf_op jit(solution)/shard_map/ppermute | solution.py:315
  15.1 1.9 %copy-start = (bf16[1,2048,768]{2,1,0:T(8,128)(2,1)S(1)}, bf16[1,2048,768]{2,1,0:T(8,128)(2,1)}, u32[]{:S(2)}) copy-start(bf16[1,2048,768]{2,1,0:T(8,128)(2,1)} %refs_8_.1) | copy-start | bytes 9437188
  17.0 1.9 %copy-start.1 = (bf16[1,2048,768]{2,1,0:T(8,128)(2,1)S(1)}, bf16[1,2048,768]{2,1,0:T(8,128)(2,1)}, u32[]{:S(2)}) copy-start(bf16[1,2048,768]{2,1,0:T(8,128)(2,1)} %refs_9_.1) | copy-start | bytes 9437188
  18.9 1.9 %copy-start.2 = (bf16[1,768,2048]{2,1,0:T(8,128)(2,1)S(1)}, bf16[1,768,2048]{2,1,0:T(8,128)(2,1)}, u32[]{:S(2)}) copy-start(bf16[1,768,2048]{2,1,0:T(8,128)(2,1)} %refs_10_.1) | copy-start | bytes 9437188
  22.6 1.3 %collective-permute-start.12 = (bf16[288,128]{1,0:T(8,128)(2,1)S(1)}, bf16[288,128]{1,0:T(8,128)(2,1)S(1)}, u32[]{:S(2)}, u32[]{:S(2)}) collective-permute-start(bf16[288,128]{1,0:T(8,128)(2,1)S(1)} %get-tuple-element.35), channel_id=1, source_target_pairs={{0,1},{1,0},{2,3},{3,2},{4,5},{5,4},{6,7},{7,6},{8,9},{9,8},{10,11... | collective-permute-start | bytes 221192 | tf_op jit(solution)/shard_map/ppermute | solution.py:382
  23.0 5.2 %collective-permute-start.16 = (bf16[288,128]{1,0:T(8,128)(2,1)S(1)}, bf16[288,128]{1,0:T(8,128)(2,1)S(1)}, u32[]{:S(2)}, u32[]{:S(2)}) collective-permute-start(bf16[288,128]{1,0:T(8,128)(2,1)S(1)} %get-tuple-element.37), channel_id=1, source_target_pairs={{0,1},{1,0},{2,3},{3,2},{4,5},{5,4},{6,7},{7,6},{8,9},{9,8},{10,11... | collective-permute-start | bytes 221192 | tf_op jit(solution)/shard_map/ppermute | solution.py:382
  23.1 1.4 %collective-permute-start.10 = (bf16[288,128]{1,0:T(8,128)(2,1)S(1)}, bf16[288,128]{1,0:T(8,128)(2,1)S(1)}, u32[]{:S(2)}, u32[]{:S(2)}) collective-permute-start(bf16[288,128]{1,0:T(8,128)(2,1)S(1)} %get-tuple-element.33), channel_id=1, source_target_pairs={{0,1},{1,0},{2,3},{3,2},{4,5},{5,4},{6,7},{7,6},{8,9},{9,8},{10,11... | collective-permute-start | bytes 221192 | tf_op jit(solution)/shard_map/ppermute | solution.py:382
  23.5 4.6 %collective-permute-start.7 = (bf16[288,128]{1,0:T(8,128)(2,1)S(1)}, bf16[288,128]{1,0:T(8,128)(2,1)S(1)}, u32[]{:S(2)}, u32[]{:S(2)}) collective-permute-start(bf16[288,128]{1,0:T(8,128)(2,1)S(1)} %get-tuple-element.28), channel_id=1, source_target_pairs={{0,1},{1,0},{2,3},{3,2},{4,5},{5,4},{6,7},{7,6},{8,9},{9,8},{10,11... | collective-permute-start | bytes 221192 | tf_op jit(solution)/shard_map/ppermute | solution.py:382
  23.9 5.3 %collective-permute-start.13 = (bf16[288,128]{1,0:T(8,128)(2,1)S(1)}, bf16[288,128]{1,0:T(8,128)(2,1)S(1)}, u32[]{:S(2)}, u32[]{:S(2)}) collective-permute-start(bf16[288,128]{1,0:T(8,128)(2,1)S(1)} %add_convert_fusion), channel_id=1, source_target_pairs={{0,4},{1,7},{2,6},{3,5},{4,0},{5,3},{6,2},{7,1},{8,12},{9,15},{10,... | collective-permute-start | bytes 221192 | tf_op jit(solution)/shard_map/ppermute | solution.py:313
  24.5 7.6 %collective-permute-start.11 = (bf16[288,128]{1,0:T(8,128)(2,1)S(1)}, bf16[288,128]{1,0:T(8,128)(2,1)S(1)}, u32[]{:S(2)}, u32[]{:S(2)}) collective-permute-start(bf16[288,128]{1,0:T(8,128)(2,1)S(1)} %add_convert_fusion.1), channel_id=1, source_target_pairs={{0,14},{1,13},{2,12},{3,15},{4,10},{5,9},{6,8},{7,11},{8,6},{9,5},... | collective-permute-start | bytes 221192 | tf_op jit(solution)/shard_map/ppermute | solution.py:313
  28.1 6.9 %collective-permute-start.8 = (bf16[288,128]{1,0:T(8,128)(2,1)S(1)}, bf16[288,128]{1,0:T(8,128)(2,1)S(1)}, u32[]{:S(2)}, u32[]{:S(2)}) collective-permute-start(bf16[288,128]{1,0:T(8,128)(2,1)S(1)} %add_convert_fusion.2), channel_id=1, source_target_pairs={{0,8},{1,11},{2,10},{3,9},{4,12},{5,15},{6,14},{7,13},{8,0},{9,3},... | collective-permute-start | bytes 221192 | tf_op jit(solution)/shard_map/ppermute | solution.py:313
  28.2 7.1 %collective-permute-start.17 = (bf16[144,128]{1,0:T(8,128)(2,1)S(1)}, bf16[144,128]{1,0:T(8,128)(2,1)S(1)}, u32[]{:S(2)}, u32[]{:S(2)}) collective-permute-start(bf16[144,128]{1,0:T(8,128)(2,1)S(1)} %get-tuple-element.40), channel_id=1, source_target_pairs={{0,2},{1,3},{2,0},{3,1},{4,6},{5,7},{6,4},{7,5},{8,10},{9,11},{10,... | collective-permute-start | bytes 110600 | tf_op jit(solution)/shard_map/ppermute | solution.py:313
  29.2 6.1 %collective-permute-start.15 = (bf16[288,128]{1,0:T(8,128)(2,1)S(1)}, bf16[288,128]{1,0:T(8,128)(2,1)S(1)}, u32[]{:S(2)}, u32[]{:S(2)}) collective-permute-start(bf16[288,128]{1,0:T(8,128)(2,1)S(1)} %collective-permute-done.13.refs_2_), channel_id=1, source_target_pairs={{0,1},{1,0},{2,3},{3,2},{4,5},{5,4},{6,7},{7,6},{8,9},{9,8},{10,11... | collective-permute-start | bytes 221192 | tf_op jit(solution)/shard_map/ppermute | solution.py:315
  32.1 3.2 %collective-permute-start.14 = (bf16[288,128]{1,0:T(8,128)(2,1)S(1)}, bf16[288,128]{1,0:T(8,128)(2,1)S(1)}, u32[]{:S(2)}, u32[]{:S(2)}) collective-permute-start(bf16[288,128]{1,0:T(8,128)(2,1)S(1)} %collective-permute-done.11.refs_0_), channel_id=1, source_target_pairs={{0,1},{1,0},{2,3},{3,2},{4,5},{5,4},{6,7},{7,6},{8,9},{9,8},{10,11... | collective-permute-start | bytes 221192 | tf_op jit(solution)/shard_map/ppermute | solution.py:315
  35.0 1.3 %collective-permute-start.9 = (bf16[288,128]{1,0:T(8,128)(2,1)S(1)}, bf16[288,128]{1,0:T(8,128)(2,1)S(1)}, u32[]{:S(2)}, u32[]{:S(2)}) collective-permute-start(bf16[288,128]{1,0:T(8,128)(2,1)S(1)} %collective-permute-done.8.refs_1_), channel_id=1, source_target_pairs={{0,1},{1,0},{2,3},{3,2},{4,5},{5,4},{6,7},{7,6},{8,9},{9,8},{10,11... | collective-permute-start | bytes 221192 | tf_op jit(solution)/shard_map/ppermute | solution.py:315

commit v6 on v5

--- a/solution.py
+++ b/solution.py
@@ -10,7 +10,8 @@
 
 LANES = 128
 SUB = 8
-COPIES = 3
+COPIES = 1
+OUT_COPIES = 4
 COVER_FLOPS = 4_000_000_000
 VMEM_LIMIT = 32 * 1024 * 1024
 F32 = jnp.float32
@@ -65,7 +66,7 @@
     ]
     for copy in copies + parts:
         copy.start()
-    for copy in copies:
+    for copy in copies + parts:
         copy.wait()
     half_slots, n_main, n_tail = split_slots(slots)
     group = 2 * n_main
@@ -94,33 +95,28 @@
     gains = gain_ref[...].astype(F32)
     gain = jnp.concatenate([gains[j : j + 1, :] for j in range(blocks)], axis=1)
     for at in range(0, tok_rows, step):
-        if at in cuts:
-            parts[cuts.index(at)].wait()
         rows = slice(at, at + step)
         values = tok_ref[rows, :].astype(F32)
         scale = lax.rsqrt(jnp.mean(values * values, axis=-1, keepdims=True) + 1e-06)
         norm_scr[rows, :] = (values * scale * gain).astype(BF16)
-    normed = norm_scr[...]
-    together = 8
-    for first in range(0, count, together):
-        members = range(first, min(first + together, count))
-        got = jnp.dot(
-            jnp.concatenate([mains[m] for m in members], axis=0), normed, preferred_element_type=F32
-        )
-        for m in members:
-            at = (m - first) * group
-            for j in range(blocks):
-                outs[m][j * group : (j + 1) * group, :] = got[
-                    at : at + group, j * LANES : (j + 1) * LANES
-                ].astype(BF16)
-    got = jnp.dot(jnp.concatenate(tails, axis=0), normed, preferred_element_type=F32)
+    left = jnp.concatenate(mains + tails, axis=0)
     padded = index.shape[0]
     per_block = 2 * n_tail * blocks
-    for k in range(2 * n_tail):
-        for j in range(blocks):
-            tail_scr[pl.ds(k * blocks + j, padded, stride=per_block), :] = got[
-                k * padded : (k + 1) * padded, j * LANES : (j + 1) * LANES
-            ]
+    chunk = 2 * LANES
+    for at in range(0, width, chunk):
+        got = jnp.dot(left, norm_scr[:, at : at + chunk], preferred_element_type=F32)
+        for b in range(chunk // LANES):
+            lanes = slice(b * LANES, (b + 1) * LANES)
+            j = at // LANES + b
+            for m in range(count):
+                outs[m][j * group : (j + 1) * group, :] = got[
+                    m * group : (m + 1) * group, lanes
+                ].astype(BF16)
+            for k in range(2 * n_tail):
+                row = count * group + k * padded
+                tail_scr[pl.ds(k * blocks + j, padded, stride=per_block), :] = got[
+                    row : row + padded, lanes
+                ]
     for m in range(count):
         outs[m][group * blocks :, :] = tail_scr[m * per_block : (m + 1) * per_block, :].astype(BF16)
 
@@ -254,11 +250,16 @@
         left_ref[...] = jnp.concatenate([high, mid, low], axis=0)[:, :total]
 
 
-def combine_kernel(*refs, members, slots, width):
+def combine_kernel(*refs, members, slots, width, copies):
     count = len(members)
     full = slots * (width // LANES)
     sides, left_ref = refs[:count], refs[count]
-    before, out_ref, row_scr, tail_scr = (None, *refs[count + 1 :])[-4:]
+    rest = refs[count + 1 :]
+    before = None
+    if copies:
+        before, out_hbm, row_scr, tail_scr, out_ref, sems = rest
+    else:
+        out_ref, row_scr, tail_scr = rest
     out_rows = out_ref.shape[0]
     n_main, n_tail = split_slots(slots)[1:]
     blocks = width // LANES
@@ -295,6 +296,7 @@
             ]
     left = left_ref[...]
     chunk = 2 * LANES
+    started = []
     for at in range(0, width, chunk):
         cols = slice(at, at + chunk)
         got = jnp.dot(left, row_scr[:, cols].astype(BF16), preferred_element_type=F32)
@@ -302,6 +304,16 @@
         if before is not None:
             got = before[:, cols] + got
         out_ref[:, cols] = got.astype(out_ref.dtype)
+        if copies and (at + chunk) % (width // copies) == 0:
+            cols = slice(at + chunk - width // copies, at + chunk)
+            started.append(
+                pltpu.make_async_copy(
+                    out_ref.at[:, cols], out_hbm.at[:, cols], sems.at[len(started)]
+                )
+            )
+            started[-1].start()
+    for copy in started:
+        copy.wait()
 
 
 def exchange(blocks, n_exp):
@@ -394,14 +406,21 @@
         final = k == len(members) - 1
         ins = [sides[side][m] for side, m in blocks_in] + [left] + ([] if total is None else [total])
         total = pl.pallas_call(
-            functools.partial(combine_kernel, members=blocks_in, slots=slots, width=width),
+            functools.partial(
+                combine_kernel,
+                members=blocks_in,
+                slots=slots,
+                width=width,
+                copies=OUT_COPIES if final else 0,
+            ),
             out_shape=jax.ShapeDtypeStruct((out_rows, width), BF16 if final else F32),
             in_specs=[VMEM] * len(ins),
-            out_specs=VMEM,
+            out_specs=pl.BlockSpec(memory_space=pl.ANY) if final else VMEM,
             scratch_shapes=[
                 pltpu.VMEM((depths[k], width), F32),
                 pltpu.VMEM((cdiv(len(blocks_in), SUB) * SUB * n_tail * blocks, LANES), F32),
-            ],
+            ]
+            + [pltpu.VMEM((out_rows, width), BF16), pltpu.SemaphoreType.DMA((OUT_COPIES,))] * final,
             compiler_params=params,
         )(*ins)
     return total

time: 37.7 us -> 37.5 us (level)
  no operation moved by 1% of the time
where the time goes in v6:
time: 37.5 us; the launch traced here: 37.2 us
  starting transfers between devices  14.2 us (38%)
  waiting for transfers between devices  12.1 us (32%)
  local copies, waits for them, and re-layouts  5.67 us (15%)
  Pallas kernels  5.05 us (13%)
    ppermute x8, starting transfers between devices, exchange(): came.append(lax.ppermute(block, ('ep', 'tp'), pairs))  12.5 us
    ppermute x8, waiting for transfers between devices, exchange(): came.append(lax.ppermute(block, ('ep', 'tp'), pairs))  10.4 us
    unnamed x6, local copies, waits for them, and re-layouts  5.67 us
    pallas_call x1, Pallas kernels, local(): pl.pallas_call(functools.partial(expert_kernel, far=far, slots=slots), ou...  1.77 us
    pallas_call x1, Pallas kernels, local(): pl.pallas_call(functools.partial(dispatch_kernel, far=far), out_shape=[bl...  1.61 us
    pallas_call x2, Pallas kernels, local(): pl.pallas_call(functools.partial(combine_kernel, members=blocks_in, slots...  1.47 us
    ppermute x6, waiting for transfers between devices, exchange(): passed.append(lax.ppermute(block, 'tp', SWAP))  1.44 us
    ppermute x4, starting transfers between devices, local(): came.append(lax.ppermute(part, 'tp', SWAP))  1.09 us
  transfers between devices with their start and end apart: 18, of which 8 were waited for; matrix products, arithmetic and copies ran while one was open for 0% of the time, Pallas kernels for 2%

profile of v6, /device:TPU:0, one launch (start us, length us, event | category | flops | bytes accessed | tf_op | source)
XLA Modules:
  0.0 37.2 jit_solution(5082011193642316193)
XLA Ops:
  0.0 1.6 %dispatch.1 = (bf16[288,128]{1,0:T(8,128)(2,1)S(1)}, bf16[288,128]{1,0:T(8,128)(2,1)S(1)}, bf16[288,128]{1,0:T(8,128)(2,1)S(1)}, bf16[288,128]{1,0:T(8,128)(2,1)...) custom-call(bf16[144,2048]{1,0:T(8,128)(2,1)} %refs_0_.1, bf16[16,128]{1,0:T(8,128)(2,1)} %bitcast.1, ...), custom_call_target="tpu_custom_call" | custom-call | tf_op jit(solution)/shard_map/dispatch/pallas_call | solution.py:342
  1.6 6.1 %collective-permute-start = (bf16[288,128]{1,0:T(8,128)(2,1)S(1)}, bf16[288,128]{1,0:T(8,128)(2,1)S(1)}, u32[]{:S(2)}, u32[]{:S(2)}) collective-permute-start(bf16[288,128]{1,0:T(8,128)(2,1)S(1)} %get-tuple-element.22), channel_id=1, source_target_pairs={{0,14},{1,13},{2,12},{3,15},{4,10},{5,9},{6,8},{7,11},{8,6},{9,5},... | collective-permute-start | bytes 221192 | tf_op jit(solution)/shard_map/ppermute | solution.py:325
  7.7 0.0 collective-permute-start.1
  7.7 0.8 %collective-permute-start.2 = (bf16[288,128]{1,0:T(8,128)(2,1)S(1)}, bf16[288,128]{1,0:T(8,128)(2,1)S(1)}, u32[]{:S(2)}, u32[]{:S(2)}) collective-permute-start(bf16[288,128]{1,0:T(8,128)(2,1)S(1)} %get-tuple-element.24), channel_id=1, source_target_pairs={{0,4},{1,7},{2,6},{3,5},{4,0},{5,3},{6,2},{7,1},{8,12},{9,15},{10,... | collective-permute-start | bytes 221192 | tf_op jit(solution)/shard_map/ppermute | solution.py:325
  8.5 0.4 %collective-permute-start.6 = (bf16[288,128]{1,0:T(8,128)(2,1)S(1)}, bf16[288,128]{1,0:T(8,128)(2,1)S(1)}, u32[]{:S(2)}, u32[]{:S(2)}) collective-permute-start(bf16[288,128]{1,0:T(8,128)(2,1)S(1)} %get-tuple-element.25), channel_id=1, source_target_pairs={{0,2},{1,3},{2,0},{3,1},{4,6},{5,7},{6,4},{7,5},{8,10},{9,11},{10,... | collective-permute-start | bytes 221192 | tf_op jit(solution)/shard_map/ppermute | solution.py:325
  8.9 1.5 %collective-permute-done.refs_0_ = bf16[288,128]{1,0:T(8,128)(2,1)S(1)} collective-permute-done((bf16[288,128]{1,0:T(8,128)(2,1)S(1)}, bf16[288,128]{1,0:T(8,128)(2,1)S(1)}, u32[]{:S(2)}, u32[]{:S(2)}) %collective-permute-start) | collective-permute-done | bytes 73760 | tf_op jit(solution)/shard_map/ppermute | solution.py:325
  10.5 0.0 collective-permute-start.3
  10.5 3.1 %collective-permute-done.1.refs_1_ = bf16[288,128]{1,0:T(8,128)(2,1)S(1)} collective-permute-done((bf16[288,128]{1,0:T(8,128)(2,1)S(1)}, bf16[288,128]{1,0:T(8,128)(2,1)S(1)}, u32[]{:S(2)}, u32[]{:S(2)}) %collective-permute-start.1) | collective-permute-done | bytes 73760 | tf_op jit(solution)/shard_map/ppermute | solution.py:325
  13.5 0.0 collective-permute-start.4
  13.6 0.0 collective-permute-done.2.refs_2_
  13.6 0.5 %collective-permute-start.5 = (bf16[288,128]{1,0:T(8,128)(2,1)S(1)}, bf16[288,128]{1,0:T(8,128)(2,1)S(1)}, u32[]{:S(2)}, u32[]{:S(2)}) collective-permute-start(bf16[288,128]{1,0:T(8,128)(2,1)S(1)} %collective-permute-done.2.refs_2_), channel_id=1, source_target_pairs={{0,1},{1,0},{2,3},{3,2},{4,5},{5,4},{6,7},{7,6},{8,9},{9,8},{10,11... | collective-permute-start | bytes 221192 | tf_op jit(solution)/shard_map/ppermute | solution.py:327
  14.1 0.0 collective-permute-done.6.refs_6_
  14.1 0.0 collective-permute-done.3.refs_3_
  14.1 0.7 %collective-permute-done.4.refs_4_ = bf16[288,128]{1,0:T(8,128)(2,1)S(1)} collective-permute-done((bf16[288,128]{1,0:T(8,128)(2,1)S(1)}, bf16[288,128]{1,0:T(8,128)(2,1)S(1)}, u32[]{:S(2)}, u32[]{:S(2)}) %collective-permute-start.4) | collective-permute-done | bytes 73760 | tf_op jit(solution)/shard_map/ppermute | solution.py:327
  14.8 0.2 collective-permute-done.5.refs_5_
  15.0 0.0 copy-start
  15.0 1.9 %copy-done = bf16[1,2048,768]{2,1,0:T(8,128)(2,1)S(1)} copy-done((bf16[1,2048,768]{2,1,0:T(8,128)(2,1)S(1)}, bf16[1,2048,768]{2,1,0:T(8,128)(2,1)}, u32[]{:S(2)}) %copy-start) | copy-done | bytes 3145752
  16.9 0.0 copy-start.1
  16.9 1.9 %copy-done.1 = bf16[1,2048,768]{2,1,0:T(8,128)(2,1)S(1)} copy-done((bf16[1,2048,768]{2,1,0:T(8,128)(2,1)S(1)}, bf16[1,2048,768]{2,1,0:T(8,128)(2,1)}, u32[]{:S(2)}) %copy-start.1) | copy-done | bytes 3145752
  18.8 0.0 copy-start.2
  18.8 1.9 %copy-done.2 = bf16[1,768,2048]{2,1,0:T(8,128)(2,1)S(1)} copy-done((bf16[1,768,2048]{2,1,0:T(8,128)(2,1)S(1)}, bf16[1,768,2048]{2,1,0:T(8,128)(2,1)}, u32[]{:S(2)}) %copy-start.2) | copy-done | bytes 3145752
  20.6 1.8 %expert.1 = (bf16[288,128]{1,0:T(8,128)(2,1)S(1)}, bf16[288,128]{1,0:T(8,128)(2,1)S(1)}, bf16[288,128]{1,0:T(8,128)(2,1)S(1)}, bf16[288,128]{1,0:T(8,128)(2,1)S(...) custom-call(bf16[288,128]{1,0:T(8,128)(2,1)S(1)} %collective-permute, ...), custom_call_target="tpu_custom_call" | custom-call | tf_op jit(solution)/shard_map/expert/pallas_call | solution.py:378
  22.4 0.4 %collective-permute-start.12 = (bf16[288,128]{1,0:T(8,128)(2,1)S(1)}, bf16[288,128]{1,0:T(8,128)(2,1)S(1)}, u32[]{:S(2)}, u32[]{:S(2)}) collective-permute-start(bf16[288,128]{1,0:T(8,128)(2,1)S(1)} %get-tuple-element.35), channel_id=1, source_target_pairs={{0,1},{1,0},{2,3},{3,2},{4,5},{5,4},{6,7},{7,6},{8,9},{9,8},{10,11... | collective-permute-start | bytes 221192 | tf_op jit(solution)/shard_map/ppermute | solution.py:394
  22.8 0.2 collective-permute-start.16
  23.0 0.3 collective-permute-start.10
  23.3 0.2 collective-permute-start.7
  23.5 0.2 collective-permute-done.12
  23.8 0.6 %collective-permute-start.13 = (bf16[288,128]{1,0:T(8,128)(2,1)S(1)}, bf16[288,128]{1,0:T(8,128)(2,1)S(1)}, u32[]{:S(2)}, u32[]{:S(2)}) collective-permute-start(bf16[288,128]{1,0:T(8,128)(2,1)S(1)} %add_convert_fusion), channel_id=1, source_target_pairs={{0,4},{1,7},{2,6},{3,5},{4,0},{5,3},{6,2},{7,1},{8,12},{9,15},{10,... | collective-permute-start | bytes 221192 | tf_op jit(solution)/shard_map/ppermute | solution.py:325
  24.4 0.0 collective-permute-done.10
  24.4 3.6 %collective-permute-start.11 = (bf16[288,128]{1,0:T(8,128)(2,1)S(1)}, bf16[288,128]{1,0:T(8,128)(2,1)S(1)}, u32[]{:S(2)}, u32[]{:S(2)}) collective-permute-start(bf16[288,128]{1,0:T(8,128)(2,1)S(1)} %add_convert_fusion.1), channel_id=1, source_target_pairs={{0,14},{1,13},{2,12},{3,15},{4,10},{5,9},{6,8},{7,11},{8,6},{9,5},... | collective-permute-start | bytes 221192 | tf_op jit(solution)/shard_map/ppermute | solution.py:325
  28.0 0.0 collective-permute-done.7
  28.0 0.1 collective-permute-start.8
  28.1 0.0 collective-permute-done.16
  28.1 1.0 %collective-permute-start.17 = (bf16[144,128]{1,0:T(8,128)(2,1)S(1)}, bf16[144,128]{1,0:T(8,128)(2,1)S(1)}, u32[]{:S(2)}, u32[]{:S(2)}) collective-permute-start(bf16[144,128]{1,0:T(8,128)(2,1)S(1)} %get-tuple-element.40), channel_id=1, source_target_pairs={{0,2},{1,3},{2,0},{3,1},{4,6},{5,7},{6,4},{7,5},{8,10},{9,11},{10,... | collective-permute-start | bytes 110600 | tf_op jit(solution)/shard_map/ppermute | solution.py:325
  29.1 0.0 collective-permute-done.13.refs_2_
  29.1 0.0 collective-permute-start.15
  29.1 2.9 %collective-permute-done.11.refs_0_ = bf16[288,128]{1,0:T(8,128)(2,1)S(1)} collective-permute-done((bf16[288,128]{1,0:T(8,128)(2,1)S(1)}, bf16[288,128]{1,0:T(8,128)(2,1)S(1)}, u32[]{:S(2)}, u32[]{:S(2)}) %collective-permute-start.11) | collective-permute-done | bytes 73760 | tf_op jit(solution)/shard_map/ppermute | solution.py:325
  32.0 0.0 collective-permute-start.14
  32.0 2.9 %collective-permute-done.8.refs_1_ = bf16[288,128]{1,0:T(8,128)(2,1)S(1)} collective-permute-done((bf16[288,128]{1,0:T(8,128)(2,1)S(1)}, bf16[288,128]{1,0:T(8,128)(2,1)S(1)}, u32[]{:S(2)}, u32[]{:S(2)}) %collective-permute-start.8) | collective-permute-done | bytes 73760 | tf_op jit(solution)/shard_map/ppermute | solution.py:325
  34.9 0.1 collective-permute-start.9
  35.0 0.2 route.1
  35.2 0.0 collective-permute-done.17.refs_5_
  35.2 0.0 collective-permute-done.15.refs_4_
  35.2 0.0 collective-permute-done.14.refs_3_
  35.2 0.4 %shard_map.73.refs_2_ = f32[72,2048]{1,0:T(8,128)S(1)} custom-call(bf16[288,128]{1,0:T(8,128)(2,1)S(1)} %collective-permute-done.11.refs_0_, bf16[288,128]{1,0:T(8,128)(2,1)S(1)} %collective-permute-done.8.refs_1_, bf16[288,128]{1,0:T(8,128)(2,1)S(1)} %collective-permute-done.13.refs_2_, bf16[288,128]{1,0:T(8,128)(2,1)S(1)} %collective-permute-done.14.refs_3_, ...), custom_call_target="tpu_custom_call" | custom-call | tf_op jit(solution)/shard_map/pallas_call | solution.py:408
  35.6 0.5 %collective-permute-done.9.refs_0_ = bf16[288,128]{1,0:T(8,128)(2,1)S(1)} collective-permute-done((bf16[288,128]{1,0:T(8,128)(2,1)S(1)}, bf16[288,128]{1,0:T(8,128)(2,1)S(1)}, u32[]{:S(2)}, u32[]{:S(2)}) %collective-permute-start.9) | collective-permute-done | bytes 73760 | tf_op jit(solution)/shard_map/ppermute | solution.py:327
  36.2 1.1 %shard_map.74 = bf16[72,2048]{1,0:T(8,128)(2,1)} custom-call(bf16[288,128]{1,0:T(8,128)(2,1)S(1)} %collective-permute-done.9.refs_0_, bf16[216,16]{1,0:T(8,128)(2,1)S(1)} %get-tuple-element.31.refs_1_, f32[72,2048]{1,0:T(8,128)S(1)} %shard_map.73.refs_2_), custom_call_target="tpu_custom_call" | custom-call | tf_op jit(solution)/shard_map/pallas_call | solution.py:408
  (4 shorter events, 0.1 us)
Async XLA Ops:
  1.6 8.8 %collective-permute-start = (bf16[288,128]{1,0:T(8,128)(2,1)S(1)}, bf16[288,128]{1,0:T(8,128)(2,1)S(1)}, u32[]{:S(2)}, u32[]{:S(2)}) collective-permute-start(bf16[288,128]{1,0:T(8,128)(2,1)S(1)} %get-tuple-element.22), channel_id=1, source_target_pairs={{0,14},{1,13},{2,12},{3,15},{4,10},{5,9},{6,8},{7,11},{8,6},{9,5},... | collective-permute-start | bytes 221192 | tf_op jit(solution)/shard_map/ppermute | solution.py:325
  7.7 5.8 %collective-permute-start.1 = (bf16[288,128]{1,0:T(8,128)(2,1)S(1)}, bf16[288,128]{1,0:T(8,128)(2,1)S(1)}, u32[]{:S(2)}, u32[]{:S(2)}) collective-permute-start(bf16[288,128]{1,0:T(8,128)(2,1)S(1)} %get-tuple-element.23), channel_id=1, source_target_pairs={{0,8},{1,11},{2,10},{3,9},{4,12},{5,15},{6,14},{7,13},{8,0},{9,3},... | collective-permute-start | bytes 221192 | tf_op jit(solution)/shard_map/ppermute | solution.py:325
  7.7 5.8 %collective-permute-start.2 = (bf16[288,128]{1,0:T(8,128)(2,1)S(1)}, bf16[288,128]{1,0:T(8,128)(2,1)S(1)}, u32[]{:S(2)}, u32[]{:S(2)}) collective-permute-start(bf16[288,128]{1,0:T(8,128)(2,1)S(1)} %get-tuple-element.24), channel_id=1, source_target_pairs={{0,4},{1,7},{2,6},{3,5},{4,0},{5,3},{6,2},{7,1},{8,12},{9,15},{10,... | collective-permute-start | bytes 221192 | tf_op jit(solution)/shard_map/ppermute | solution.py:325
  8.5 5.5 %collective-permute-start.6 = (bf16[288,128]{1,0:T(8,128)(2,1)S(1)}, bf16[288,128]{1,0:T(8,128)(2,1)S(1)}, u32[]{:S(2)}, u32[]{:S(2)}) collective-permute-start(bf16[288,128]{1,0:T(8,128)(2,1)S(1)} %get-tuple-element.25), channel_id=1, source_target_pairs={{0,2},{1,3},{2,0},{3,1},{4,6},{5,7},{6,4},{7,5},{8,10},{9,11},{10,... | collective-permute-start | bytes 221192 | tf_op jit(solution)/shard_map/ppermute | solution.py:325
  10.5 3.6 %collective-permute-start.3 = (bf16[288,128]{1,0:T(8,128)(2,1)S(1)}, bf16[288,128]{1,0:T(8,128)(2,1)S(1)}, u32[]{:S(2)}, u32[]{:S(2)}) collective-permute-start(bf16[288,128]{1,0:T(8,128)(2,1)S(1)} %collective-permute-done.refs_0_), channel_id=1, source_target_pairs={{0,1},{1,0},{2,3},{3,2},{4,5},{5,4},{6,7},{7,6},{8,9},{9,8},{10,11... | collective-permute-start | bytes 221192 | tf_op jit(solution)/shard_map/ppermute | solution.py:327
  13.5 1.3 %collective-permute-start.4 = (bf16[288,128]{1,0:T(8,128)(2,1)S(1)}, bf16[288,128]{1,0:T(8,128)(2,1)S(1)}, u32[]{:S(2)}, u32[]{:S(2)}) collective-permute-start(bf16[288,128]{1,0:T(8,128)(2,1)S(1)} %collective-permute-done.1.refs_1_), channel_id=1, source_target_pairs={{0,1},{1,0},{2,3},{3,2},{4,5},{5,4},{6,7},{7,6},{8,9},{9,8},{10,11... | collective-permute-start | bytes 221192 | tf_op jit(solution)/shard_map/ppermute | solution.py:327
  13.6 1.4 %collective-permute-start.5 = (bf16[288,128]{1,0:T(8,128)(2,1)S(1)}, bf16[288,128]{1,0:T(8,128)(2,1)S(1)}, u32[]{:S(2)}, u32[]{:S(2)}) collective-permute-start(bf16[288,128]{1,0:T(8,128)(2,1)S(1)} %collective-permute-done.2.refs_2_), channel_id=1, source_target_pairs={{0,1},{1,0},{2,3},{3,2},{4,5},{5,4},{6,7},{7,6},{8,9},{9,8},{10,11... | collective-permute-start | bytes 221192 | tf_op jit(solution)/shard_map/ppermute | solution.py:327
  15.0 1.9 %copy-start = (bf16[1,2048,768]{2,1,0:T(8,128)(2,1)S(1)}, bf16[1,2048,768]{2,1,0:T(8,128)(2,1)}, u32[]{:S(2)}) copy-start(bf16[1,2048,768]{2,1,0:T(8,128)(2,1)} %refs_8_.1) | copy-start | bytes 9437188
  16.9 1.9 %copy-start.1 = (bf16[1,2048,768]{2,1,0:T(8,128)(2,1)S(1)}, bf16[1,2048,768]{2,1,0:T(8,128)(2,1)}, u32[]{:S(2)}) copy-start(bf16[1,2048,768]{2,1,0:T(8,128)(2,1)} %refs_9_.1) | copy-start | bytes 9437188
  18.8 1.9 %copy-start.2 = (bf16[1,768,2048]{2,1,0:T(8,128)(2,1)S(1)}, bf16[1,768,2048]{2,1,0:T(8,128)(2,1)}, u32[]{:S(2)}) copy-start(bf16[1,768,2048]{2,1,0:T(8,128)(2,1)} %refs_10_.1) | copy-start | bytes 9437188
  22.4 1.3 %collective-permute-start.12 = (bf16[288,128]{1,0:T(8,128)(2,1)S(1)}, bf16[288,128]{1,0:T(8,128)(2,1)S(1)}, u32[]{:S(2)}, u32[]{:S(2)}) collective-permute-start(bf16[288,128]{1,0:T(8,128)(2,1)S(1)} %get-tuple-element.35), channel_id=1, source_target_pairs={{0,1},{1,0},{2,3},{3,2},{4,5},{5,4},{6,7},{7,6},{8,9},{9,8},{10,11... | collective-permute-start | bytes 221192 | tf_op jit(solution)/shard_map/ppermute | solution.py:394
  22.8 5.2 %collective-permute-start.16 = (bf16[288,128]{1,0:T(8,128)(2,1)S(1)}, bf16[288,128]{1,0:T(8,128)(2,1)S(1)}, u32[]{:S(2)}, u32[]{:S(2)}) collective-permute-start(bf16[288,128]{1,0:T(8,128)(2,1)S(1)} %get-tuple-element.37), channel_id=1, source_target_pairs={{0,1},{1,0},{2,3},{3,2},{4,5},{5,4},{6,7},{7,6},{8,9},{9,8},{10,11... | collective-permute-start | bytes 221192 | tf_op jit(solution)/shard_map/ppermute | solution.py:394
  23.0 1.4 %collective-permute-start.10 = (bf16[288,128]{1,0:T(8,128)(2,1)S(1)}, bf16[288,128]{1,0:T(8,128)(2,1)S(1)}, u32[]{:S(2)}, u32[]{:S(2)}) collective-permute-start(bf16[288,128]{1,0:T(8,128)(2,1)S(1)} %get-tuple-element.33), channel_id=1, source_target_pairs={{0,1},{1,0},{2,3},{3,2},{4,5},{5,4},{6,7},{7,6},{8,9},{9,8},{10,11... | collective-permute-start | bytes 221192 | tf_op jit(solution)/shard_map/ppermute | solution.py:394
  23.3 4.6 %collective-permute-start.7 = (bf16[288,128]{1,0:T(8,128)(2,1)S(1)}, bf16[288,128]{1,0:T(8,128)(2,1)S(1)}, u32[]{:S(2)}, u32[]{:S(2)}) collective-permute-start(bf16[288,128]{1,0:T(8,128)(2,1)S(1)} %get-tuple-element.28), channel_id=1, source_target_pairs={{0,1},{1,0},{2,3},{3,2},{4,5},{5,4},{6,7},{7,6},{8,9},{9,8},{10,11... | collective-permute-start | bytes 221192 | tf_op jit(solution)/shard_map/ppermute | solution.py:394
  23.8 5.3 %collective-permute-start.13 = (bf16[288,128]{1,0:T(8,128)(2,1)S(1)}, bf16[288,128]{1,0:T(8,128)(2,1)S(1)}, u32[]{:S(2)}, u32[]{:S(2)}) collective-permute-start(bf16[288,128]{1,0:T(8,128)(2,1)S(1)} %add_convert_fusion), channel_id=1, source_target_pairs={{0,4},{1,7},{2,6},{3,5},{4,0},{5,3},{6,2},{7,1},{8,12},{9,15},{10,... | collective-permute-start | bytes 221192 | tf_op jit(solution)/shard_map/ppermute | solution.py:325
  24.4 7.6 %collective-permute-start.11 = (bf16[288,128]{1,0:T(8,128)(2,1)S(1)}, bf16[288,128]{1,0:T(8,128)(2,1)S(1)}, u32[]{:S(2)}, u32[]{:S(2)}) collective-permute-start(bf16[288,128]{1,0:T(8,128)(2,1)S(1)} %add_convert_fusion.1), channel_id=1, source_target_pairs={{0,14},{1,13},{2,12},{3,15},{4,10},{5,9},{6,8},{7,11},{8,6},{9,5},... | collective-permute-start | bytes 221192 | tf_op jit(solution)/shard_map/ppermute | solution.py:325
  28.0 6.9 %collective-permute-start.8 = (bf16[288,128]{1,0:T(8,128)(2,1)S(1)}, bf16[288,128]{1,0:T(8,128)(2,1)S(1)}, u32[]{:S(2)}, u32[]{:S(2)}) collective-permute-start(bf16[288,128]{1,0:T(8,128)(2,1)S(1)} %add_convert_fusion.2), channel_id=1, source_target_pairs={{0,8},{1,11},{2,10},{3,9},{4,12},{5,15},{6,14},{7,13},{8,0},{9,3},... | collective-permute-start | bytes 221192 | tf_op jit(solution)/shard_map/ppermute | solution.py:325
  28.1 7.1 %collective-permute-start.17 = (bf16[144,128]{1,0:T(8,128)(2,1)S(1)}, bf16[144,128]{1,0:T(8,128)(2,1)S(1)}, u32[]{:S(2)}, u32[]{:S(2)}) collective-permute-start(bf16[144,128]{1,0:T(8,128)(2,1)S(1)} %get-tuple-element.40), channel_id=1, source_target_pairs={{0,2},{1,3},{2,0},{3,1},{4,6},{5,7},{6,4},{7,5},{8,10},{9,11},{10,... | collective-permute-start | bytes 110600 | tf_op jit(solution)/shard_map/ppermute | solution.py:325
  29.1 6.1 %collective-permute-start.15 = (bf16[288,128]{1,0:T(8,128)(2,1)S(1)}, bf16[288,128]{1,0:T(8,128)(2,1)S(1)}, u32[]{:S(2)}, u32[]{:S(2)}) collective-permute-start(bf16[288,128]{1,0:T(8,128)(2,1)S(1)} %collective-permute-done.13.refs_2_), channel_id=1, source_target_pairs={{0,1},{1,0},{2,3},{3,2},{4,5},{5,4},{6,7},{7,6},{8,9},{9,8},{10,11... | collective-permute-start | bytes 221192 | tf_op jit(solution)/shard_map/ppermute | solution.py:327
  32.0 3.2 %collective-permute-start.14 = (bf16[288,128]{1,0:T(8,128)(2,1)S(1)}, bf16[288,128]{1,0:T(8,128)(2,1)S(1)}, u32[]{:S(2)}, u32[]{:S(2)}) collective-permute-start(bf16[288,128]{1,0:T(8,128)(2,1)S(1)} %collective-permute-done.11.refs_0_), channel_id=1, source_target_pairs={{0,1},{1,0},{2,3},{3,2},{4,5},{5,4},{6,7},{7,6},{8,9},{9,8},{10,11... | collective-permute-start | bytes 221192 | tf_op jit(solution)/shard_map/ppermute | solution.py:327
  34.9 1.3 %collective-permute-start.9 = (bf16[288,128]{1,0:T(8,128)(2,1)S(1)}, bf16[288,128]{1,0:T(8,128)(2,1)S(1)}, u32[]{:S(2)}, u32[]{:S(2)}) collective-permute-start(bf16[288,128]{1,0:T(8,128)(2,1)S(1)} %collective-permute-done.8.refs_1_), channel_id=1, source_target_pairs={{0,1},{1,0},{2,3},{3,2},{4,5},{5,4},{6,7},{7,6},{8,9},{9,8},{10,11... | collective-permute-start | bytes 221192 | tf_op jit(solution)/shard_map/ppermute | solution.py:327

commit v7 on v6

--- a/solution.py
+++ b/solution.py
@@ -209,7 +209,7 @@
     slots = rows_ref.shape[1]
     half_slots, n_main, n_tail = split_slots(slots)
     lefts, (index_scr, weight_scr) = refs[:2], refs[2:]
-    out_rows = lefts[0].shape[0] // 3
+    out_rows = lefts[0].shape[0]
     core = lax.axis_index("tp")
     start = lax.axis_index("ep") * (2 * out_rows) + core * out_rows
     lane0 = core * half_slots
@@ -239,15 +239,15 @@
         for t in range(n_tail):
             at = jnp.full((padded, slots), n_main + t, jnp.int32) + lane0
             pieces.append(entry(pick(index, at), pick(weight, at)))
-        total = depth(len(members), slots)
-        pieces.append(jnp.zeros((cdiv(total, LANES) * LANES - total, pieces[0].shape[1]), F32))
-        pieces = [piece for piece in pieces if piece.shape[0]]
-        spread = jnp.concatenate(pieces, axis=0).T[:out_rows, :]
-        high = spread.astype(BF16)
-        rest = spread - high.astype(F32)
-        mid = rest.astype(BF16)
-        low = (rest - mid.astype(F32)).astype(BF16)
-        left_ref[...] = jnp.concatenate([high, mid, low], axis=0)[:, :total]
+        spread = jnp.concatenate(pieces, axis=0)
+        high = spread.astype(BF16).astype(F32)
+        mid = (spread - high).astype(BF16).astype(F32)
+        parts = [high, mid, spread - high - mid]
+        total = 3 * depth(len(members), slots)
+        missing = cdiv(total, LANES) * LANES - total
+        if missing:
+            parts.append(jnp.zeros((missing, spread.shape[1]), F32))
+        left_ref[...] = jnp.concatenate(parts, axis=0).T[:out_rows, :total].astype(BF16)
 
 
 def combine_kernel(*refs, members, slots, width, copies):
@@ -260,7 +260,6 @@
         before, out_hbm, row_scr, tail_scr, out_ref, sems = rest
     else:
         out_ref, row_scr, tail_scr = rest
-    out_rows = out_ref.shape[0]
     n_main, n_tail = split_slots(slots)[1:]
     blocks = width // LANES
     per_half = n_tail * blocks
@@ -299,8 +298,8 @@
     started = []
     for at in range(0, width, chunk):
         cols = slice(at, at + chunk)
-        got = jnp.dot(left, row_scr[:, cols].astype(BF16), preferred_element_type=F32)
-        got = got[:out_rows] + (got[out_rows : 2 * out_rows] + got[2 * out_rows :])
+        rows = row_scr[:, cols].astype(BF16)
+        got = jnp.dot(left, jnp.concatenate([rows] * 3, axis=0), preferred_element_type=F32)
         if before is not None:
             got = before[:, cols] + got
         out_ref[:, cols] = got.astype(out_ref.dtype)
@@ -363,7 +362,7 @@
     most = cdiv(len(members[0]), SUB) * SUB
     lefts = pl.pallas_call(
         functools.partial(route_kernel, far=far),
-        out_shape=[jax.ShapeDtypeStruct((3 * out_rows, d), BF16) for d in depths],
+        out_shape=[jax.ShapeDtypeStruct((out_rows, 3 * d), BF16) for d in depths],
         in_specs=[VMEM] * 2,
         out_specs=[VMEM] * 2,
         scratch_shapes=[pltpu.VMEM((most, slots), jnp.int32), pltpu.VMEM((most, slots), F32)],

time: 37.5 us -> 37.3 us (level)
  transfers between devices with their start and end apart: 18 -> 18, of which waited for: 8 -> 8; matrix products, arithmetic and copies ran while one was open for 0% -> 0% of each run, Pallas kernels for 2% -> 1%
where the time goes in v7:
time: 37.3 us; the launch traced here: 37.1 us
  starting transfers between devices  14.2 us (38%)
  waiting for transfers between devices  12.2 us (33%)
  local copies, waits for them, and re-layouts  5.67 us (15%)
  Pallas kernels  4.79 us (13%)
    ppermute x8, starting transfers between devices, exchange(): came.append(lax.ppermute(block, ('ep', 'tp'), pairs))  12.5 us
    ppermute x8, waiting for transfers between devices, exchange(): came.append(lax.ppermute(block, ('ep', 'tp'), pairs))  10.4 us
    unnamed x6, local copies, waits for them, and re-layouts  5.67 us
    pallas_call x1, Pallas kernels, local(): pl.pallas_call(functools.partial(expert_kernel, far=far, slots=slots), ou...  1.77 us
    pallas_call x1, Pallas kernels, local(): pl.pallas_call(functools.partial(dispatch_kernel, far=far), out_shape=[bl...  1.61 us
    ppermute x6, waiting for transfers between devices, exchange(): passed.append(lax.ppermute(block, 'tp', SWAP))  1.56 us
    pallas_call x2, Pallas kernels, local(): pl.pallas_call(functools.partial(combine_kernel, members=blocks_in, slots...  1.19 us
    ppermute x4, starting transfers between devices, local(): came.append(lax.ppermute(part, 'tp', SWAP))  1.09 us
  transfers between devices with their start and end apart: 18, of which 8 were waited for; matrix products, arithmetic and copies ran while one was open for 0% of the time, Pallas kernels for 1%

profile of v7, /device:TPU:0, one launch (start us, length us, event | category | flops | bytes accessed | tf_op | source)
XLA Modules:
  0.0 37.1 jit_solution(62854887801356998)
XLA Ops:
  0.0 1.6 %dispatch.1 = (bf16[288,128]{1,0:T(8,128)(2,1)S(1)}, bf16[288,128]{1,0:T(8,128)(2,1)S(1)}, bf16[288,128]{1,0:T(8,128)(2,1)S(1)}, bf16[288,128]{1,0:T(8,128)(2,1)...) custom-call(bf16[144,2048]{1,0:T(8,128)(2,1)} %refs_0_.1, bf16[16,128]{1,0:T(8,128)(2,1)} %bitcast.1, ...), custom_call_target="tpu_custom_call" | custom-call | tf_op jit(solution)/shard_map/dispatch/pallas_call | solution.py:341
  1.6 6.1 %collective-permute-start = (bf16[288,128]{1,0:T(8,128)(2,1)S(1)}, bf16[288,128]{1,0:T(8,128)(2,1)S(1)}, u32[]{:S(2)}, u32[]{:S(2)}) collective-permute-start(bf16[288,128]{1,0:T(8,128)(2,1)S(1)} %get-tuple-element.22), channel_id=1, source_target_pairs={{0,14},{1,13},{2,12},{3,15},{4,10},{5,9},{6,8},{7,11},{8,6},{9,5},... | collective-permute-start | bytes 221192 | tf_op jit(solution)/shard_map/ppermute | solution.py:324
  7.7 0.0 collective-permute-start.1
  7.7 0.8 %collective-permute-start.2 = (bf16[288,128]{1,0:T(8,128)(2,1)S(1)}, bf16[288,128]{1,0:T(8,128)(2,1)S(1)}, u32[]{:S(2)}, u32[]{:S(2)}) collective-permute-start(bf16[288,128]{1,0:T(8,128)(2,1)S(1)} %get-tuple-element.24), channel_id=1, source_target_pairs={{0,4},{1,7},{2,6},{3,5},{4,0},{5,3},{6,2},{7,1},{8,12},{9,15},{10,... | collective-permute-start | bytes 221192 | tf_op jit(solution)/shard_map/ppermute | solution.py:324
  8.5 0.4 %collective-permute-start.6 = (bf16[288,128]{1,0:T(8,128)(2,1)S(1)}, bf16[288,128]{1,0:T(8,128)(2,1)S(1)}, u32[]{:S(2)}, u32[]{:S(2)}) collective-permute-start(bf16[288,128]{1,0:T(8,128)(2,1)S(1)} %get-tuple-element.25), channel_id=1, source_target_pairs={{0,2},{1,3},{2,0},{3,1},{4,6},{5,7},{6,4},{7,5},{8,10},{9,11},{10,... | collective-permute-start | bytes 221192 | tf_op jit(solution)/shard_map/ppermute | solution.py:324
  8.9 1.5 %collective-permute-done.refs_0_ = bf16[288,128]{1,0:T(8,128)(2,1)S(1)} collective-permute-done((bf16[288,128]{1,0:T(8,128)(2,1)S(1)}, bf16[288,128]{1,0:T(8,128)(2,1)S(1)}, u32[]{:S(2)}, u32[]{:S(2)}) %collective-permute-start) | collective-permute-done | bytes 73760 | tf_op jit(solution)/shard_map/ppermute | solution.py:324
  10.5 0.0 collective-permute-start.3
  10.5 3.1 %collective-permute-done.1.refs_1_ = bf16[288,128]{1,0:T(8,128)(2,1)S(1)} collective-permute-done((bf16[288,128]{1,0:T(8,128)(2,1)S(1)}, bf16[288,128]{1,0:T(8,128)(2,1)S(1)}, u32[]{:S(2)}, u32[]{:S(2)}) %collective-permute-start.1) | collective-permute-done | bytes 73760 | tf_op jit(solution)/shard_map/ppermute | solution.py:324
  13.5 0.0 collective-permute-start.4
  13.6 0.0 collective-permute-done.2.refs_2_
  13.6 0.5 %collective-permute-start.5 = (bf16[288,128]{1,0:T(8,128)(2,1)S(1)}, bf16[288,128]{1,0:T(8,128)(2,1)S(1)}, u32[]{:S(2)}, u32[]{:S(2)}) collective-permute-start(bf16[288,128]{1,0:T(8,128)(2,1)S(1)} %collective-permute-done.2.refs_2_), channel_id=1, source_target_pairs={{0,1},{1,0},{2,3},{3,2},{4,5},{5,4},{6,7},{7,6},{8,9},{9,8},{10,11... | collective-permute-start | bytes 221192 | tf_op jit(solution)/shard_map/ppermute | solution.py:326
  14.1 0.0 collective-permute-done.6.refs_6_
  14.1 0.0 collective-permute-done.3.refs_3_
  14.1 0.7 %collective-permute-done.4.refs_4_ = bf16[288,128]{1,0:T(8,128)(2,1)S(1)} collective-permute-done((bf16[288,128]{1,0:T(8,128)(2,1)S(1)}, bf16[288,128]{1,0:T(8,128)(2,1)S(1)}, u32[]{:S(2)}, u32[]{:S(2)}) %collective-permute-start.4) | collective-permute-done | bytes 73760 | tf_op jit(solution)/shard_map/ppermute | solution.py:326
  14.8 0.2 collective-permute-done.5.refs_5_
  15.0 0.0 copy-start
  15.0 1.9 %copy-done = bf16[1,2048,768]{2,1,0:T(8,128)(2,1)S(1)} copy-done((bf16[1,2048,768]{2,1,0:T(8,128)(2,1)S(1)}, bf16[1,2048,768]{2,1,0:T(8,128)(2,1)}, u32[]{:S(2)}) %copy-start) | copy-done | bytes 3145752
  16.9 0.0 copy-start.1
  16.9 1.9 %copy-done.1 = bf16[1,2048,768]{2,1,0:T(8,128)(2,1)S(1)} copy-done((bf16[1,2048,768]{2,1,0:T(8,128)(2,1)S(1)}, bf16[1,2048,768]{2,1,0:T(8,128)(2,1)}, u32[]{:S(2)}) %copy-start.1) | copy-done | bytes 3145752
  18.8 0.0 copy-start.2
  18.8 1.9 %copy-done.2 = bf16[1,768,2048]{2,1,0:T(8,128)(2,1)S(1)} copy-done((bf16[1,768,2048]{2,1,0:T(8,128)(2,1)S(1)}, bf16[1,768,2048]{2,1,0:T(8,128)(2,1)}, u32[]{:S(2)}) %copy-start.2) | copy-done | bytes 3145752
  20.6 1.8 %expert.1 = (bf16[288,128]{1,0:T(8,128)(2,1)S(1)}, bf16[288,128]{1,0:T(8,128)(2,1)S(1)}, bf16[288,128]{1,0:T(8,128)(2,1)S(1)}, bf16[288,128]{1,0:T(8,128)(2,1)S(...) custom-call(bf16[288,128]{1,0:T(8,128)(2,1)S(1)} %collective-permute, ...), custom_call_target="tpu_custom_call" | custom-call | tf_op jit(solution)/shard_map/expert/pallas_call | solution.py:377
  22.4 0.4 %collective-permute-start.12 = (bf16[288,128]{1,0:T(8,128)(2,1)S(1)}, bf16[288,128]{1,0:T(8,128)(2,1)S(1)}, u32[]{:S(2)}, u32[]{:S(2)}) collective-permute-start(bf16[288,128]{1,0:T(8,128)(2,1)S(1)} %get-tuple-element.35), channel_id=1, source_target_pairs={{0,1},{1,0},{2,3},{3,2},{4,5},{5,4},{6,7},{7,6},{8,9},{9,8},{10,11... | collective-permute-start | bytes 221192 | tf_op jit(solution)/shard_map/ppermute | solution.py:393
  22.8 0.2 collective-permute-start.16
  23.0 0.3 collective-permute-start.10
  23.3 0.2 collective-permute-start.7
  23.5 0.2 collective-permute-done.12
  23.8 0.6 %collective-permute-start.13 = (bf16[288,128]{1,0:T(8,128)(2,1)S(1)}, bf16[288,128]{1,0:T(8,128)(2,1)S(1)}, u32[]{:S(2)}, u32[]{:S(2)}) collective-permute-start(bf16[288,128]{1,0:T(8,128)(2,1)S(1)} %add_convert_fusion), channel_id=1, source_target_pairs={{0,4},{1,7},{2,6},{3,5},{4,0},{5,3},{6,2},{7,1},{8,12},{9,15},{10,... | collective-permute-start | bytes 221192 | tf_op jit(solution)/shard_map/ppermute | solution.py:324
  24.4 0.0 collective-permute-done.10
  24.4 3.6 %collective-permute-start.11 = (bf16[288,128]{1,0:T(8,128)(2,1)S(1)}, bf16[288,128]{1,0:T(8,128)(2,1)S(1)}, u32[]{:S(2)}, u32[]{:S(2)}) collective-permute-start(bf16[288,128]{1,0:T(8,128)(2,1)S(1)} %add_convert_fusion.1), channel_id=1, source_target_pairs={{0,14},{1,13},{2,12},{3,15},{4,10},{5,9},{6,8},{7,11},{8,6},{9,5},... | collective-permute-start | bytes 221192 | tf_op jit(solution)/shard_map/ppermute | solution.py:324
  28.0 0.0 collective-permute-done.7
  28.0 0.1 collective-permute-start.8
  28.1 0.0 collective-permute-done.16
  28.1 1.0 %collective-permute-start.17 = (bf16[144,128]{1,0:T(8,128)(2,1)S(1)}, bf16[144,128]{1,0:T(8,128)(2,1)S(1)}, u32[]{:S(2)}, u32[]{:S(2)}) collective-permute-start(bf16[144,128]{1,0:T(8,128)(2,1)S(1)} %get-tuple-element.40), channel_id=1, source_target_pairs={{0,2},{1,3},{2,0},{3,1},{4,6},{5,7},{6,4},{7,5},{8,10},{9,11},{10,... | collective-permute-start | bytes 110600 | tf_op jit(solution)/shard_map/ppermute | solution.py:324
  29.1 0.0 collective-permute-done.13.refs_2_
  29.1 0.0 collective-permute-start.15
  29.1 2.9 %collective-permute-done.11.refs_0_ = bf16[288,128]{1,0:T(8,128)(2,1)S(1)} collective-permute-done((bf16[288,128]{1,0:T(8,128)(2,1)S(1)}, bf16[288,128]{1,0:T(8,128)(2,1)S(1)}, u32[]{:S(2)}, u32[]{:S(2)}) %collective-permute-start.11) | collective-permute-done | bytes 73760 | tf_op jit(solution)/shard_map/ppermute | solution.py:324
  32.0 0.0 collective-permute-start.14
  32.0 2.9 %collective-permute-done.8.refs_1_ = bf16[288,128]{1,0:T(8,128)(2,1)S(1)} collective-permute-done((bf16[288,128]{1,0:T(8,128)(2,1)S(1)}, bf16[288,128]{1,0:T(8,128)(2,1)S(1)}, u32[]{:S(2)}, u32[]{:S(2)}) %collective-permute-start.8) | collective-permute-done | bytes 73760 | tf_op jit(solution)/shard_map/ppermute | solution.py:324
  34.9 0.1 collective-permute-start.9
  35.0 0.2 route.1
  35.2 0.0 collective-permute-done.17.refs_5_
  35.2 0.0 collective-permute-done.15.refs_4_
  35.2 0.0 collective-permute-done.14.refs_3_
  35.2 0.3 shard_map.73.refs_2_
  35.5 0.6 %collective-permute-done.9.refs_0_ = bf16[288,128]{1,0:T(8,128)(2,1)S(1)} collective-permute-done((bf16[288,128]{1,0:T(8,128)(2,1)S(1)}, bf16[288,128]{1,0:T(8,128)(2,1)S(1)}, u32[]{:S(2)}, u32[]{:S(2)}) %collective-permute-start.9) | collective-permute-done | bytes 73760 | tf_op jit(solution)/shard_map/ppermute | solution.py:326
  36.2 0.9 %shard_map.74 = bf16[72,2048]{1,0:T(8,128)(2,1)} custom-call(bf16[288,128]{1,0:T(8,128)(2,1)S(1)} %collective-permute-done.9.refs_0_, bf16[72,48]{1,0:T(8,128)(2,1)S(1)} %get-tuple-element.31.refs_1_, f32[72,2048]{1,0:T(8,128)S(1)} %shard_map.73.refs_2_), custom_call_target="tpu_custom_call" | custom-call | tf_op jit(solution)/shard_map/pallas_call | solution.py:407
  (4 shorter events, 0.1 us)
Async XLA Ops:
  1.6 8.8 %collective-permute-start = (bf16[288,128]{1,0:T(8,128)(2,1)S(1)}, bf16[288,128]{1,0:T(8,128)(2,1)S(1)}, u32[]{:S(2)}, u32[]{:S(2)}) collective-permute-start(bf16[288,128]{1,0:T(8,128)(2,1)S(1)} %get-tuple-element.22), channel_id=1, source_target_pairs={{0,14},{1,13},{2,12},{3,15},{4,10},{5,9},{6,8},{7,11},{8,6},{9,5},... | collective-permute-start | bytes 221192 | tf_op jit(solution)/shard_map/ppermute | solution.py:324
  7.7 5.8 %collective-permute-start.1 = (bf16[288,128]{1,0:T(8,128)(2,1)S(1)}, bf16[288,128]{1,0:T(8,128)(2,1)S(1)}, u32[]{:S(2)}, u32[]{:S(2)}) collective-permute-start(bf16[288,128]{1,0:T(8,128)(2,1)S(1)} %get-tuple-element.23), channel_id=1, source_target_pairs={{0,8},{1,11},{2,10},{3,9},{4,12},{5,15},{6,14},{7,13},{8,0},{9,3},... | collective-permute-start | bytes 221192 | tf_op jit(solution)/shard_map/ppermute | solution.py:324
  7.7 5.8 %collective-permute-start.2 = (bf16[288,128]{1,0:T(8,128)(2,1)S(1)}, bf16[288,128]{1,0:T(8,128)(2,1)S(1)}, u32[]{:S(2)}, u32[]{:S(2)}) collective-permute-start(bf16[288,128]{1,0:T(8,128)(2,1)S(1)} %get-tuple-element.24), channel_id=1, source_target_pairs={{0,4},{1,7},{2,6},{3,5},{4,0},{5,3},{6,2},{7,1},{8,12},{9,15},{10,... | collective-permute-start | bytes 221192 | tf_op jit(solution)/shard_map/ppermute | solution.py:324
  8.5 5.5 %collective-permute-start.6 = (bf16[288,128]{1,0:T(8,128)(2,1)S(1)}, bf16[288,128]{1,0:T(8,128)(2,1)S(1)}, u32[]{:S(2)}, u32[]{:S(2)}) collective-permute-start(bf16[288,128]{1,0:T(8,128)(2,1)S(1)} %get-tuple-element.25), channel_id=1, source_target_pairs={{0,2},{1,3},{2,0},{3,1},{4,6},{5,7},{6,4},{7,5},{8,10},{9,11},{10,... | collective-permute-start | bytes 221192 | tf_op jit(solution)/shard_map/ppermute | solution.py:324
  10.5 3.6 %collective-permute-start.3 = (bf16[288,128]{1,0:T(8,128)(2,1)S(1)}, bf16[288,128]{1,0:T(8,128)(2,1)S(1)}, u32[]{:S(2)}, u32[]{:S(2)}) collective-permute-start(bf16[288,128]{1,0:T(8,128)(2,1)S(1)} %collective-permute-done.refs_0_), channel_id=1, source_target_pairs={{0,1},{1,0},{2,3},{3,2},{4,5},{5,4},{6,7},{7,6},{8,9},{9,8},{10,11... | collective-permute-start | bytes 221192 | tf_op jit(solution)/shard_map/ppermute | solution.py:326
  13.5 1.3 %collective-permute-start.4 = (bf16[288,128]{1,0:T(8,128)(2,1)S(1)}, bf16[288,128]{1,0:T(8,128)(2,1)S(1)}, u32[]{:S(2)}, u32[]{:S(2)}) collective-permute-start(bf16[288,128]{1,0:T(8,128)(2,1)S(1)} %collective-permute-done.1.refs_1_), channel_id=1, source_target_pairs={{0,1},{1,0},{2,3},{3,2},{4,5},{5,4},{6,7},{7,6},{8,9},{9,8},{10,11... | collective-permute-start | bytes 221192 | tf_op jit(solution)/shard_map/ppermute | solution.py:326
  13.6 1.4 %collective-permute-start.5 = (bf16[288,128]{1,0:T(8,128)(2,1)S(1)}, bf16[288,128]{1,0:T(8,128)(2,1)S(1)}, u32[]{:S(2)}, u32[]{:S(2)}) collective-permute-start(bf16[288,128]{1,0:T(8,128)(2,1)S(1)} %collective-permute-done.2.refs_2_), channel_id=1, source_target_pairs={{0,1},{1,0},{2,3},{3,2},{4,5},{5,4},{6,7},{7,6},{8,9},{9,8},{10,11... | collective-permute-start | bytes 221192 | tf_op jit(solution)/shard_map/ppermute | solution.py:326
  15.0 1.9 %copy-start = (bf16[1,2048,768]{2,1,0:T(8,128)(2,1)S(1)}, bf16[1,2048,768]{2,1,0:T(8,128)(2,1)}, u32[]{:S(2)}) copy-start(bf16[1,2048,768]{2,1,0:T(8,128)(2,1)} %refs_8_.1) | copy-start | bytes 9437188
  16.9 1.9 %copy-start.1 = (bf16[1,2048,768]{2,1,0:T(8,128)(2,1)S(1)}, bf16[1,2048,768]{2,1,0:T(8,128)(2,1)}, u32[]{:S(2)}) copy-start(bf16[1,2048,768]{2,1,0:T(8,128)(2,1)} %refs_9_.1) | copy-start | bytes 9437188
  18.8 1.9 %copy-start.2 = (bf16[1,768,2048]{2,1,0:T(8,128)(2,1)S(1)}, bf16[1,768,2048]{2,1,0:T(8,128)(2,1)}, u32[]{:S(2)}) copy-start(bf16[1,768,2048]{2,1,0:T(8,128)(2,1)} %refs_10_.1) | copy-start | bytes 9437188
  22.4 1.3 %collective-permute-start.12 = (bf16[288,128]{1,0:T(8,128)(2,1)S(1)}, bf16[288,128]{1,0:T(8,128)(2,1)S(1)}, u32[]{:S(2)}, u32[]{:S(2)}) collective-permute-start(bf16[288,128]{1,0:T(8,128)(2,1)S(1)} %get-tuple-element.35), channel_id=1, source_target_pairs={{0,1},{1,0},{2,3},{3,2},{4,5},{5,4},{6,7},{7,6},{8,9},{9,8},{10,11... | collective-permute-start | bytes 221192 | tf_op jit(solution)/shard_map/ppermute | solution.py:393
  22.8 5.2 %collective-permute-start.16 = (bf16[288,128]{1,0:T(8,128)(2,1)S(1)}, bf16[288,128]{1,0:T(8,128)(2,1)S(1)}, u32[]{:S(2)}, u32[]{:S(2)}) collective-permute-start(bf16[288,128]{1,0:T(8,128)(2,1)S(1)} %get-tuple-element.37), channel_id=1, source_target_pairs={{0,1},{1,0},{2,3},{3,2},{4,5},{5,4},{6,7},{7,6},{8,9},{9,8},{10,11... | collective-permute-start | bytes 221192 | tf_op jit(solution)/shard_map/ppermute | solution.py:393
  23.0 1.4 %collective-permute-start.10 = (bf16[288,128]{1,0:T(8,128)(2,1)S(1)}, bf16[288,128]{1,0:T(8,128)(2,1)S(1)}, u32[]{:S(2)}, u32[]{:S(2)}) collective-permute-start(bf16[288,128]{1,0:T(8,128)(2,1)S(1)} %get-tuple-element.33), channel_id=1, source_target_pairs={{0,1},{1,0},{2,3},{3,2},{4,5},{5,4},{6,7},{7,6},{8,9},{9,8},{10,11... | collective-permute-start | bytes 221192 | tf_op jit(solution)/shard_map/ppermute | solution.py:393
  23.3 4.6 %collective-permute-start.7 = (bf16[288,128]{1,0:T(8,128)(2,1)S(1)}, bf16[288,128]{1,0:T(8,128)(2,1)S(1)}, u32[]{:S(2)}, u32[]{:S(2)}) collective-permute-start(bf16[288,128]{1,0:T(8,128)(2,1)S(1)} %get-tuple-element.28), channel_id=1, source_target_pairs={{0,1},{1,0},{2,3},{3,2},{4,5},{5,4},{6,7},{7,6},{8,9},{9,8},{10,11... | collective-permute-start | bytes 221192 | tf_op jit(solution)/shard_map/ppermute | solution.py:393
  23.8 5.3 %collective-permute-start.13 = (bf16[288,128]{1,0:T(8,128)(2,1)S(1)}, bf16[288,128]{1,0:T(8,128)(2,1)S(1)}, u32[]{:S(2)}, u32[]{:S(2)}) collective-permute-start(bf16[288,128]{1,0:T(8,128)(2,1)S(1)} %add_convert_fusion), channel_id=1, source_target_pairs={{0,4},{1,7},{2,6},{3,5},{4,0},{5,3},{6,2},{7,1},{8,12},{9,15},{10,... | collective-permute-start | bytes 221192 | tf_op jit(solution)/shard_map/ppermute | solution.py:324
  24.4 7.6 %collective-permute-start.11 = (bf16[288,128]{1,0:T(8,128)(2,1)S(1)}, bf16[288,128]{1,0:T(8,128)(2,1)S(1)}, u32[]{:S(2)}, u32[]{:S(2)}) collective-permute-start(bf16[288,128]{1,0:T(8,128)(2,1)S(1)} %add_convert_fusion.1), channel_id=1, source_target_pairs={{0,14},{1,13},{2,12},{3,15},{4,10},{5,9},{6,8},{7,11},{8,6},{9,5},... | collective-permute-start | bytes 221192 | tf_op jit(solution)/shard_map/ppermute | solution.py:324
  28.0 6.9 %collective-permute-start.8 = (bf16[288,128]{1,0:T(8,128)(2,1)S(1)}, bf16[288,128]{1,0:T(8,128)(2,1)S(1)}, u32[]{:S(2)}, u32[]{:S(2)}) collective-permute-start(bf16[288,128]{1,0:T(8,128)(2,1)S(1)} %add_convert_fusion.2), channel_id=1, source_target_pairs={{0,8},{1,11},{2,10},{3,9},{4,12},{5,15},{6,14},{7,13},{8,0},{9,3},... | collective-permute-start | bytes 221192 | tf_op jit(solution)/shard_map/ppermute | solution.py:324
  28.1 7.1 %collective-permute-start.17 = (bf16[144,128]{1,0:T(8,128)(2,1)S(1)}, bf16[144,128]{1,0:T(8,128)(2,1)S(1)}, u32[]{:S(2)}, u32[]{:S(2)}) collective-permute-start(bf16[144,128]{1,0:T(8,128)(2,1)S(1)} %get-tuple-element.40), channel_id=1, source_target_pairs={{0,2},{1,3},{2,0},{3,1},{4,6},{5,7},{6,4},{7,5},{8,10},{9,11},{10,... | collective-permute-start | bytes 110600 | tf_op jit(solution)/shard_map/ppermute | solution.py:324
  29.1 6.1 %collective-permute-start.15 = (bf16[288,128]{1,0:T(8,128)(2,1)S(1)}, bf16[288,128]{1,0:T(8,128)(2,1)S(1)}, u32[]{:S(2)}, u32[]{:S(2)}) collective-permute-start(bf16[288,128]{1,0:T(8,128)(2,1)S(1)} %collective-permute-done.13.refs_2_), channel_id=1, source_target_pairs={{0,1},{1,0},{2,3},{3,2},{4,5},{5,4},{6,7},{7,6},{8,9},{9,8},{10,11... | collective-permute-start | bytes 221192 | tf_op jit(solution)/shard_map/ppermute | solution.py:326
  32.0 3.3 %collective-permute-start.14 = (bf16[288,128]{1,0:T(8,128)(2,1)S(1)}, bf16[288,128]{1,0:T(8,128)(2,1)S(1)}, u32[]{:S(2)}, u32[]{:S(2)}) collective-permute-start(bf16[288,128]{1,0:T(8,128)(2,1)S(1)} %collective-permute-done.11.refs_0_), channel_id=1, source_target_pairs={{0,1},{1,0},{2,3},{3,2},{4,5},{5,4},{6,7},{7,6},{8,9},{9,8},{10,11... | collective-permute-start | bytes 221192 | tf_op jit(solution)/shard_map/ppermute | solution.py:326
  34.9 1.3 %collective-permute-start.9 = (bf16[288,128]{1,0:T(8,128)(2,1)S(1)}, bf16[288,128]{1,0:T(8,128)(2,1)S(1)}, u32[]{:S(2)}, u32[]{:S(2)}) collective-permute-start(bf16[288,128]{1,0:T(8,128)(2,1)S(1)} %collective-permute-done.8.refs_1_), channel_id=1, source_target_pairs={{0,1},{1,0},{2,3},{3,2},{4,5},{5,4},{6,7},{7,6},{8,9},{9,8},{10,11... | collective-permute-start | bytes 221192 | tf_op jit(solution)/shard_map/ppermute | solution.py:326
